TPU v7x, 128 devices: a whole 4x4x4 slice. The times are simulated.
128 devices in a mesh: sp: 32 (over z, y, core), tp: 4 (over x).
Axes of the slice: x: 4, y: 4, z: 4, core: 2. Of those that a mesh axis runs over, the one named last changes fastest.
Arguments:
- stream: bfloat16 [8192, 2048], P(('sp', 'tp')), may hold values from -6 to 6
- queries: bfloat16 [8192, 2048], P('sp', 'tp'), may hold values from -147.07821 to 147.07821
- keys: bfloat16 [8192, 2048], P('sp', 'tp'), may hold values from -7 to 7
- values: bfloat16 [8192, 2048], P('sp', 'tp'), may hold values from -6 to 6
- head_lambda: float32 [8], P('tp'), may hold values from 0.3 to 0.8
- head_gain: float32 [256], replicated, may hold values from 0.1 to 1.9
- w_out: bfloat16 [2048, 2048], P('tp'), may hold values from -0.125 to 0.125
- norm_gain: float32 [2048], replicated, may hold values from 0.1 to 1.9
- w_gate: bfloat16 [2048, 5632], P('sp', 'tp'), may hold values from -0.125 to 0.125
- w_up: bfloat16 [2048, 5632], P('sp', 'tp'), may hold values from -0.125 to 0.125
- w_down: bfloat16 [5632, 2048], P('tp', 'sp'), may hold values from -0.078125 to 0.078125
Outputs:
- result: bfloat16 [8192, 2048], P(('sp', 'tp'))
All inputs are finite; a program needn't handle non-finite values.
Results may differ from a plain program's by a relative error of at most 0.013.
Values may be sent and summed in bfloat16 or wider, within the bound.
No kernel may reach another device: no remote copies, remote signals or barrier semaphores. Data moves between devices by JAX's collectives and lax.ppermute only.
A program may use at most 192 MiB of HBM per device.

v0:
```python
import functools

import jax
import jax.numpy as jnp
import numpy as np
from jax import lax
from jax.experimental import pallas as pl
from jax.experimental.pallas import tpu as pltpu
from jax.sharding import PartitionSpec as P


EPS = 1e-6
NEG = -1e30
F32 = jnp.float32
BF16 = jnp.bfloat16

STEP = {"zl": 4, "zh": 12, "yl": 1, "yh": 3}
KV_ORDERS = (("zl", "zh", "yh"), ("zh", "yh", "zl"), ("yh", "zl", "zh"))
KV_ROWS = (192, 160, 160)
KV_STARTS = (0, 96, 176)
W_ORDERS = (
    (("zl", "yl", "zh", "yh"), ("yl", "zl", "yh", "zh")),
    (("zh", "yh", "zl", "yl"), ("yh", "zh", "yl", "zl")),
)


def patterns(order):
    found = [0]
    for name in order:
        found = found + [p ^ STEP[name] for p in found]
    return found


def chip_swap(array, flip, core_flip=0):
    pairs = [(j * 2 + c, (j ^ flip) * 2 + (c ^ core_flip)) for j in range(16) for c in range(2)]
    return lax.ppermute(array, "sp", pairs)


def chip_swap_by_core(array, flips):
    pairs = [(j * 2 + c, (j ^ flips[c]) * 2 + c) for j in range(16) for c in range(2)]
    return lax.ppermute(array, "sp", pairs)


def core_swap(array):
    return chip_swap(array, 0, 1)


def shift_x(array, d):
    return lax.ppermute(array, "tp", [(i, (i + d) % 4) for i in range(4)])


def meta_layout():
    rows = [[(0, 0, 0, 0, 0)] * 2]
    for core_flip in (0, 1):
        rows.append([(0, 0, core_flip, 256, 0), (STEP["yl"],) * 2 + (core_flip, 256, 0)])
    for far in (0, 1):
        for t in range(3):
            for p in patterns(KV_ORDERS[t])[4 * far : 4 * far + 4]:
                rows.append(
                    [(p, p, 0, 256, KV_STARTS[t]), (p ^ STEP["yl"],) * 2 + (0, 256, KV_STARTS[t])]
                )
    for h in range(2):
        rows.append(
            [(a, b, h, 64, 0) for a, b in zip(patterns(W_ORDERS[0][h]), patterns(W_ORDERS[1][h]))]
        )
    return np.array([entry for row in rows for entry in row], np.int32)


META_Q, META_K, META_W = 2, 6, 54


def meta_table(head, x, chip, core):
    flip0, flip1, core_flip, factor, addend = (jnp.asarray(v) for v in meta_layout().T)
    flip = jnp.where(core == 0, flip0, flip1)
    table = ((chip ^ flip) * 2 + (core ^ core_flip)) * factor + addend
    place = jnp.arange(table.shape[0])
    table = jnp.where(place == 0, head, jnp.where(place == 1, x, table))
    return table.astype(jnp.int32)


def after(value, *others):
    return lax.optimization_barrier((value, others))[0]


def whole(shape):
    return pl.BlockSpec(shape, lambda *_: (0,) * len(shape))


def cost(us):
    return pl.CostEstimate(flops=int(us * 1e9), bytes_accessed=int(1e5), transcendentals=0)


def vmem_params(mib=24, **kw):
    return pltpu.CompilerParams(vmem_limit_bytes=mib << 20, **kw)


def pack_kernel(meta, keys, values, queries, own_ref, given_ref, ins, outs, sem):
    second, x = meta[0], meta[1]
    loads = [
        pltpu.make_async_copy(ref, ins.at[k], sem.at[k])
        for k, ref in enumerate((keys, values, queries))
    ]
    stores = [
        pltpu.make_async_copy(outs.at[k], ref, sem.at[3 + k])
        for k, ref in enumerate((given_ref, own_ref))
    ]
    for load in loads:
        load.start()
    for load in loads:
        load.wait()
    for k, turn in enumerate((1 - second, second)):
        cols = pl.ds(pl.multiple_of(turn * 256, 256), 256)
        outs[k, :, :256] = ins[0, :, cols]
        outs[k, :, 256:512] = ins[1, :, cols]
        for j in range(4):
            rows = pl.ds(pl.multiple_of(lax.rem(x + j, 4) * 64, 64), 64)
            outs[k, 64 * j : 64 * j + 64, 512:] = ins[2, rows, cols]
        stores[k].start()
    for store in stores:
        store.wait()


def pack(meta, keys, values, queries):
    in_hbm = pl.BlockSpec(memory_space=pltpu.HBM)
    return pl.pallas_call(
        pack_kernel,
        in_specs=[pl.BlockSpec(memory_space=pltpu.SMEM)] + [in_hbm] * 3,
        out_specs=[in_hbm] * 2,
        out_shape=[jax.ShapeDtypeStruct((256, 768), BF16)] * 2,
        scratch_shapes=[
            pltpu.VMEM((3, 256, 512), BF16),
            pltpu.VMEM((2, 256, 768), BF16),
            pltpu.SemaphoreType.DMA((5,)),
        ],
        compiler_params=vmem_params(16),
        cost_estimate=cost(1),
        name="pack",
    )(meta, keys, values, queries)


def weights_kernel(meta, gate, up, down, own_ref, given_ref):
    first = lax.rem(meta[META_Q] // 256, 2) == 0
    for k in range(2):
        cols = slice(704 * k, 704 * k + 704)
        block = jnp.concatenate(
            [gate[:, cols], up[:, cols], down[cols, :].T, jnp.zeros((64, 64), BF16)], axis=1
        )

        @pl.when(first == (k == 0))
        def _():
            own_ref[0] = block

        @pl.when(first != (k == 0))
        def _():
            given_ref[0] = block


def split_weights(meta, gate, up, down):
    return pl.pallas_call(
        weights_kernel,
        grid=(1,),
        in_specs=[pl.BlockSpec(memory_space=pltpu.SMEM)]
        + [whole((64, 1408))] * 2
        + [whole((1408, 64))],
        out_specs=[whole((1, 64, 2176))] * 2,
        out_shape=[jax.ShapeDtypeStruct((1, 64, 2176), BF16)] * 2,
        compiler_params=vmem_params(),
        cost_estimate=cost(2),
        name="weights",
    )(meta, gate, up, down)


def thirds_kernel(own, taken, *outs):
    for t in range(3):
        half, start = KV_ROWS[t] // 2, KV_STARTS[t]
        outs[t][0, :half] = own[start : start + half, :512]
        outs[t][0, half:] = taken[start : start + half, :512]
    outs[3][:256] = own[:, 512:]
    outs[3][256:] = taken[:, 512:]


def thirds(own, taken):
    shapes = [(1, n, 512) for n in KV_ROWS] + [(512, 256)]
    return pl.pallas_call(
        thirds_kernel,
        grid=(1,),
        in_specs=[whole((256, 768))] * 2,
        out_specs=[whole(shape) for shape in shapes],
        out_shape=[jax.ShapeDtypeStruct(shape, BF16) for shape in shapes],
        compiler_params=vmem_params(16),
        cost_estimate=cost(1),
        name="thirds",
    )(own, taken)


def join_kernel(count, *refs):
    for k in range(count):
        n = refs[k].shape[0]
        refs[2 * count + k][:n] = refs[k][...]
        refs[2 * count + k][n:] = refs[count + k][...]


def join(held, far):
    shapes = [(2 * a.shape[0], *a.shape[1:]) for a in held]
    return pl.pallas_call(
        functools.partial(join_kernel, len(held)),
        grid=(1,),
        in_specs=[whole(a.shape) for a in (*held, *far)],
        out_specs=[whole(shape) for shape in shapes],
        out_shape=[jax.ShapeDtypeStruct(shape, BF16) for shape in shapes],
        compiler_params=vmem_params(),
        cost_estimate=cost(1),
        name="join",
    )(*held, *far)


def flash_kernel(group, far, scale, meta, *refs):
    q_ref, kv_refs, rest = refs[0], refs[1:4], refs[4:]
    out_ref = rest[-1]
    step = pl.program_id(0)
    row = lax.broadcasted_iota(jnp.int32, (256, 1), 0)
    qpos = meta[META_Q + group + step] + ((meta[1] + (row >> 6)) & 3) * 64 + (row & 63)
    state = []
    for s in range(2):
        if far:
            st = rest[0]
            state.append(
                (st[:, 512 + s : 513 + s], st[:, 514 + s : 515 + s], st[:, 256 * s : 256 * s + 256])
            )
        else:
            state.append(
                (jnp.full((256, 1), NEG, F32), jnp.zeros((256, 1), F32), jnp.zeros((256, 256), F32))
            )
    for t in range(3):
        kv_ref, half = kv_refs[t], KV_ROWS[t] // 2
        key = lax.broadcasted_iota(jnp.int32, (1, 8 * half), 1)
        kpos = key
        for k in range(8):
            base = meta[META_K + 24 * far + 8 * t + k]
            kpos = jnp.where(key >= k * half, base + key - k * half, kpos)
        visible = kpos <= qpos
        for s in range(2):
            top, total, acc = state[s]
            scores = lax.dot_general(
                q_ref[:, 128 * s : 128 * s + 128],
                kv_ref[:, 128 * s : 128 * s + 128],
                (((1,), (1,)), ((), ())),
                preferred_element_type=F32,
            )
            scores = jnp.where(visible, scores, NEG)
            new_top = jnp.maximum(top, jnp.max(scores, axis=1, keepdims=True))
            weights = jnp.exp2((scores - new_top) * scale)
            fade = jnp.exp2((top - new_top) * scale)
            total = total * fade + jnp.sum(weights, axis=1, keepdims=True)
            acc = acc * fade + jnp.dot(
                weights.astype(BF16), kv_ref[:, 256:512], preferred_element_type=F32
            )
            state[s] = (new_top, total, acc)
    lane = lax.broadcasted_iota(jnp.int32, (256, 128), 1)
    tail = jnp.zeros((256, 128), F32)
    for s in range(2):
        top, total, acc = state[s]
        out_ref[:, 256 * s : 256 * s + 256] = acc
        tail = jnp.where(lane == s, top, tail)
        tail = jnp.where(lane == 2 + s, total, tail)
    out_ref[:, 512:640] = tail


def flash(meta, q, kvs, group, far, state, us):
    scale = float(128**-0.5 * np.log2(np.e))
    row_block = lambda width: pl.BlockSpec((256, width), lambda i: (i, 0))
    kvs = [a.reshape(-1, 512) for a in kvs]
    return pl.pallas_call(
        functools.partial(flash_kernel, group, far, scale),
        grid=(2,),
        in_specs=[pl.BlockSpec(memory_space=pltpu.SMEM), row_block(256)]
        + [pl.BlockSpec(a.shape, lambda i: (0, 0)) for a in kvs]
        + [row_block(640)] * far,
        out_specs=row_block(640),
        out_shape=jax.ShapeDtypeStruct((512, 640), F32),
        compiler_params=vmem_params(),
        cost_estimate=cost(us),
        name="flash",
    )(meta, q, *kvs, *([state] if far else []))


def merge_kernel(meta, lam, mine_ref, other_ref, gain_ref, out_ref):
    scale = float(128**-0.5 * np.log2(np.e))
    maps = []
    for s in range(2):
        top_a, top_b = mine_ref[:, 512 + s : 513 + s], other_ref[:, 512 + s : 513 + s]
        top = jnp.maximum(top_a, top_b)
        fade_a, fade_b = jnp.exp2((top_a - top) * scale), jnp.exp2((top_b - top) * scale)
        total = mine_ref[:, 514 + s : 515 + s] * fade_a + other_ref[:, 514 + s : 515 + s] * fade_b
        cols = slice(256 * s, 256 * s + 256)
        maps.append((mine_ref[:, cols] * fade_a + other_ref[:, cols] * fade_b) / total)
    contrast = maps[0] - lax.select(meta[0] == 1, lam[1], lam[0]) * maps[1]
    power = jnp.mean(contrast * contrast, axis=-1, keepdims=True)
    out_ref[0] = (contrast * lax.rsqrt(power + EPS) * gain_ref[...]).astype(BF16)


def merge(meta, lam, mine, other, gain):
    return pl.pallas_call(
        merge_kernel,
        grid=(2,),
        in_specs=[
            pl.BlockSpec(memory_space=pltpu.SMEM),
            pl.BlockSpec(memory_space=pltpu.SMEM),
            pl.BlockSpec((256, 640), lambda i: (i, 0)),
            pl.BlockSpec((256, 640), lambda i: (i, 0)),
            pl.BlockSpec((1, 256), lambda i: (0, 0)),
        ],
        out_specs=pl.BlockSpec((1, 256, 256), lambda i: (i, 0, 0)),
        out_shape=jax.ShapeDtypeStruct((2, 256, 256), BF16),
        compiler_params=vmem_params(),
        cost_estimate=cost(2),
        name="merge",
    )(meta, lam, mine, other, gain)


def middle_kernel(meta, *refs):
    owns, passes, weights, streams = refs[0:4], refs[4:8], refs[8:16], refs[16:20]
    gain_ref, normed_ref, own_ref, scratch, power = refs[20:]
    step = pl.program_id(0)
    total = jnp.concatenate([streams[d][...] for d in (0, 3, 2, 1)], axis=0).astype(F32)
    straight = (meta[META_Q] // 256) % 2 == 0
    for d in range(4):
        own, passed = owns[d][...], passes[d][...]
        for half in range(2):
            block = jnp.where(straight, *((own, passed) if half == 0 else (passed, own)))
            if d:
                block = jnp.concatenate([block[64 * d :], block[: 64 * d]], axis=0)
            total += jnp.dot(block, weights[2 * d + half][...], preferred_element_type=F32)
    squares = jnp.sum(total * total, axis=-1, keepdims=True)

    @pl.when(step == 0)
    def _():
        power[...] = jnp.broadcast_to(squares, power.shape)

    @pl.when(step > 0)
    def _():
        power[...] += jnp.broadcast_to(squares, power.shape)

    scratch[step] = total
    own_ref[...] = total[:64]

    @pl.when(step == 3)
    def _():
        root = lax.rsqrt(power[:, :1] * (1.0 / 2048) + EPS)
        for k in range(4):
            cols = slice(512 * k, 512 * k + 512)
            normed_ref[:, cols] = (scratch[k] * root * gain_ref[:, cols]).astype(BF16)


def middle_call(meta, owns, passes, weights, streams, gain):
    return pl.pallas_call(
        middle_kernel,
        grid=(4,),
        in_specs=[pl.BlockSpec(memory_space=pltpu.SMEM)]
        + [pl.BlockSpec((256, 256), lambda i: (0, 0))] * 8
        + [pl.BlockSpec((256, 512), lambda i: (0, i))] * 8
        + [pl.BlockSpec((64, 512), lambda i: (0, i))] * 4
        + [pl.BlockSpec((1, 2048), lambda i: (0, 0))],
        out_specs=[
            pl.BlockSpec((256, 2048), lambda i: (0, 0)),
            pl.BlockSpec((64, 512), lambda i: (0, i)),
        ],
        out_shape=[jax.ShapeDtypeStruct((256, 2048), BF16), jax.ShapeDtypeStruct((64, 2048), F32)],
        scratch_shapes=[pltpu.VMEM((4, 256, 512), F32), pltpu.VMEM((256, 128), F32)],
        compiler_params=vmem_params(),
        cost_estimate=cost(4),
        name="middle",
    )(meta, *owns, *passes, *weights, *streams, gain)


def ffn_kernel(table, mine_ref, other_ref, *refs):
    pieces = refs[:8]
    keep_ref, send_ref = refs[8:10]
    gu, down, both, hidden, sem = refs[10:]
    for k in range(8):

        def body(i, _, w=pieces[k], base=4 * k):
            row = pl.ds(pl.multiple_of(table[META_W + base + i], 64), 64)
            for n, (start, width) in enumerate(((0, 768), (768, 640))):
                pltpu.make_async_copy(
                    w.at[i, :, pl.ds(start, width)], gu.at[row, pl.ds(start, width)], sem.at[n]
                ).start()
            pltpu.make_async_copy(w.at[i, :, pl.ds(1408, 768)], down.at[row], sem.at[2]).start()
            return 0

        lax.fori_loop(0, 4, body, 0)

    def gate_up(cols):
        both[:256, cols] = jnp.dot(other_ref[...], gu[:, cols], preferred_element_type=F32)
        both[256:, cols] = jnp.dot(mine_ref[...], gu[:, cols], preferred_element_type=F32)

    def gate_up_pair(k, _):
        gate_up(pl.ds(pl.multiple_of(k * 256, 256), 256))
        return 0

    first, second = gu.at[:, pl.ds(0, 768)], gu.at[:, pl.ds(768, 640)]
    pltpu.make_async_copy(first, first, sem.at[0]).wait()
    lax.fori_loop(0, 3, gate_up_pair, 0)
    pltpu.make_async_copy(second, second, sem.at[1]).wait()
    lax.fori_loop(3, 5, gate_up_pair, 0)
    gate_up(pl.ds(1280, 128))

    def activate(k, _):
        rows = pl.ds(pl.multiple_of(k * 64, 64), 64)
        gate, up = both[rows, :704], both[rows, 704:]
        hidden[rows, :704] = (gate / (1.0 + jnp.exp(-gate)) * up).astype(BF16)
        hidden[rows, 704:] = jnp.zeros((64, 64), BF16)
        return 0

    lax.fori_loop(0, 8, activate, 0)
    pltpu.make_async_copy(down, down, sem.at[2]).wait()

    def project(k, _):
        rows = pl.ds(pl.multiple_of(k * 256, 256), 256)
        part = lax.dot_general(
            hidden[...], down[rows, :], (((1,), (1,)), ((), ())), preferred_element_type=F32
        )
        send_ref[:, rows] = part[:256].astype(BF16)
        keep_ref[:, rows] = part[256:]
        return 0

    lax.fori_loop(0, 8, project, 0)


def ffn(table, mine, other, pieces):
    any_space = pl.BlockSpec(memory_space=pl.ANY)
    in_vmem = pl.BlockSpec(memory_space=pltpu.VMEM)
    return pl.pallas_call(
        ffn_kernel,
        in_specs=[pl.BlockSpec(memory_space=pltpu.SMEM), in_vmem, in_vmem] + [any_space] * 8,
        out_specs=[in_vmem] * 2,
        out_shape=[jax.ShapeDtypeStruct((256, 2048), F32), jax.ShapeDtypeStruct((256, 2048), BF16)],
        scratch_shapes=[
            pltpu.VMEM((2048, 1408), BF16),
            pltpu.VMEM((2048, 768), BF16),
            pltpu.VMEM((512, 1408), F32),
            pltpu.VMEM((512, 768), BF16),
            pltpu.SemaphoreType.DMA((3,)),
        ],
        compiler_params=vmem_params(),
        cost_estimate=cost(9),
        name="ffn",
    )(table, mine, other, *pieces)


def add_kernel(mine_ref, came_ref, middle_ref, own_ref, *sent):
    total = mine_ref[...] + came_ref[...].astype(F32)
    own_ref[...] = total[:64] + middle_ref[...]
    for d in range(3):
        sent[d][...] = total[64 * d + 64 : 64 * d + 128].astype(BF16)


def add_parts(mine, came, middle):
    in_vmem = pl.BlockSpec(memory_space=pltpu.VMEM)
    return pl.pallas_call(
        add_kernel,
        in_specs=[in_vmem] * 3,
        out_specs=[in_vmem] * 4,
        out_shape=[jax.ShapeDtypeStruct((64, 2048), F32)]
        + [jax.ShapeDtypeStruct((64, 2048), BF16)] * 3,
        compiler_params=vmem_params(),
        cost_estimate=cost(1),
        name="add",
    )(mine, came, middle)


def layer(
    stream, queries, keys, values, head_lambda, head_gain, w_out, norm_gain, w_gate, w_up, w_down
):
    sp = lax.axis_index("sp")
    x = lax.axis_index("tp")
    core = sp % 2
    chip = sp // 2
    y = chip % 4
    second = jnp.logical_or(y == 1, y == 2)
    head = second.astype(jnp.int32)

    meta = meta_table(head, x, chip, core)
    own, given = pack(meta, keys, values, queries)
    *kv_held, q_mine = thirds(own, chip_swap(given, STEP["yl"]))
    q_other = core_swap(q_mine)

    w_own, w_given = split_weights(meta, w_gate, w_up, w_down)
    w_held = [w_own, core_swap(w_given)]

    own_rows = (head ^ core) * 256
    w_mine = lax.dynamic_slice(w_out, (own_rows, 0), (256, 2048))
    w_other = lax.dynamic_slice(w_out, (256 - own_rows, 0), (256, 2048))

    streams = [stream] + [shift_x(stream, d) for d in (1, 2, 3)]
    w_mines = [w_mine] + [shift_x(w_mine, d) for d in (1, 2, 3)]
    for s in range(3):
        kv_far = [chip_swap(kv_held[t], STEP[KV_ORDERS[t][s]]) for t in range(3)]
        if s < 2:
            kv_held = join(kv_held, kv_far)
        w_far = [
            chip_swap_by_core(w_held[h], [STEP[W_ORDERS[c][h][s]] for c in range(2)])
            for h in range(2)
        ]
        if s < 2:
            w_held = join(w_held, w_far)
    w_others = [w_other] + [core_swap(after(w, *kv_far)) for w in w_mines[1:]]

    state_other = flash(meta, q_other, kv_held, 2, 0, None, 5)
    state_mine = flash(meta, q_mine, kv_held, 0, 0, None, 5)
    last = [[STEP[W_ORDERS[c][h][3]] for c in range(2)] for h in range(2)]
    w_last = [chip_swap_by_core(after(w_held[h], *kv_far), last[h]) for h in range(2)]
    sent = flash(meta, q_other, kv_far, 2, 1, after(state_other, state_mine), 5)
    came = core_swap(sent)
    w_tail = [chip_swap_by_core(after(w_far[h], sent), last[h]) for h in range(2)]
    kept = flash(meta, q_mine, kv_far, 0, 1, state_mine, 5)
    head_out = merge(meta, head_lambda, kept, came, head_gain[None])
    mine_out, pair_out = head_out[0], head_out[1]
    passed = chip_swap(pair_out, STEP["yl"])
    owns = [mine_out] + [shift_x(mine_out, d) for d in (1, 2, 3)]
    passes = [passed] + [shift_x(passed, d) for d in (1, 2, 3)]

    weights = [w for pair in zip(w_mines, w_others) for w in pair]
    normed, middle = middle_call(meta, owns, passes, weights, streams, norm_gain[None])
    other_normed = core_swap(normed)
    kept_part, sent_part = ffn(
        meta,
        normed,
        other_normed,
        [w_held[0], w_far[0], w_last[0], w_tail[0], w_held[1], w_far[1], w_last[1], w_tail[1]],
    )
    result, *parts = add_parts(kept_part, core_swap(sent_part), middle)
    for d in (1, 2, 3):
        result = result + shift_x(parts[d - 1], d).astype(F32)
    return result.astype(BF16)


def solution(mesh):
    placed = (
        P(("sp", "tp"), None),
        P("sp", "tp"),
        P("sp", "tp"),
        P("sp", "tp"),
        P("tp"),
        P(),
        P("tp", None),
        P(),
        P("sp", "tp"),
        P("sp", "tp"),
        P("tp", "sp"),
    )
    return jax.shard_map(
        layer, mesh=mesh, in_specs=placed, out_specs=P(("sp", "tp"), None), check_vma=False
    )
```

profile of v0, /device:TPU:0, one launch (start us, length us, event | category | flops | bytes accessed | tf_op | source)
XLA Modules:
  0.0 212.4 jit_solution(7284564200983725522)
XLA Ops:
  6.7 8.9 %collective-permute-done.taken = bf16[256,768]{1,0:T(8,128)(2,1)S(1)} collective-permute-done((bf16[256,768]{1,0:T(8,128)(2,1)S(1)}, bf16[256,768]{1,0:T(8,128)(2,1)S(1)}, u32[]{:S(2)}, u32[]{:S(2)}) %collective-permute-start) | collective-permute-done | bytes 393248 | tf_op jit(solution)/shard_map/ppermute | solution.py:36
  19.4 2.6 %collective-permute-start.2 = (bf16[1,160,512]{2,1,0:T(8,128)(2,1)S(1)}, bf16[1,160,512]{2,1,0:T(8,128)(2,1)S(1)}, u32[]{:S(2)}, u32[]{:S(2)}) collective-permute-start(bf16[1,160,512]{2,1,0:T(8,128)(2,1)S(1)} %get-tuple-element.43.refs_1_), channel_id=1, source_target_pairs={{0,96},{4,100},{8,104},{12,108},{16,112},{20,116},{24,120},{28,124... | collective-permute-start | bytes 491528 | tf_op jit(solution)/shard_map/ppermute | solution.py:36
  22.0 3.0 %collective-permute-start.3 = (bf16[1,160,512]{2,1,0:T(8,128)(2,1)S(1)}, bf16[1,160,512]{2,1,0:T(8,128)(2,1)S(1)}, u32[]{:S(2)}, u32[]{:S(2)}) collective-permute-start(bf16[1,160,512]{2,1,0:T(8,128)(2,1)S(1)} %get-tuple-element.44.refs_2_), channel_id=1, source_target_pairs={{0,24},{4,28},{8,16},{12,20},{16,8},{20,12},{24,0},{28,4},{32,56},... | collective-permute-start | bytes 491528 | tf_op jit(solution)/shard_map/ppermute | solution.py:36
  25.0 2.2 %collective-permute-done.2.refs_4_ = bf16[1,160,512]{2,1,0:T(8,128)(2,1)S(1)} collective-permute-done((bf16[1,160,512]{2,1,0:T(8,128)(2,1)S(1)}, bf16[1,160,512]{2,1,0:T(8,128)(2,1)S(1)}, u32[]{:S(2)}, u32[]{:S(2)}) %collective-permute-start.2) | collective-permute-done | bytes 163872 | tf_op jit(solution)/shard_map/ppermute | solution.py:36
  27.2 2.3 %collective-permute-done.3.refs_5_ = bf16[1,160,512]{2,1,0:T(8,128)(2,1)S(1)} collective-permute-done((bf16[1,160,512]{2,1,0:T(8,128)(2,1)S(1)}, bf16[1,160,512]{2,1,0:T(8,128)(2,1)S(1)}, u32[]{:S(2)}, u32[]{:S(2)}) %collective-permute-start.3) | collective-permute-done | bytes 163872 | tf_op jit(solution)/shard_map/ppermute | solution.py:36
  31.4 2.5 %collective-permute-start.5 = (bf16[2,160,512]{2,1,0:T(8,128)(2,1)S(1)}, bf16[2,160,512]{2,1,0:T(8,128)(2,1)S(1)}, u32[]{:S(2)}, u32[]{:S(2)}) collective-permute-start(bf16[2,160,512]{2,1,0:T(8,128)(2,1)S(1)} %get-tuple-element.46.refs_1_), channel_id=1, source_target_pairs={{0,24},{4,28},{8,16},{12,20},{16,8},{20,12},{24,0},{28,4},{32,56},... | collective-permute-start | bytes 983048 | tf_op jit(solution)/shard_map/ppermute | solution.py:36
  38.4 6.8 %collective-permute-start.10 = (bf16[512,256]{1,0:T(8,128)(2,1)}, bf16[512,256]{1,0:T(8,128)(2,1)S(1)}, u32[]{:S(2)}, u32[]{:S(2)}) collective-permute-start(bf16[512,256]{1,0:T(8,128)(2,1)} %copy-done.4), channel_id=1, source_target_pairs={{0,4},{4,0},{8,12},{12,8},{16,20},{20,16},{24,28},{28,24},{32,36},... | collective-permute-start | bytes 786440 | tf_op jit(solution)/shard_map/ppermute | solution.py:36
  45.5 3.0 %collective-permute-start.7 = (bf16[4,192,512]{2,1,0:T(8,128)(2,1)S(1)}, bf16[4,192,512]{2,1,0:T(8,128)(2,1)S(1)}, u32[]{:S(2)}, u32[]{:S(2)}) collective-permute-start(bf16[4,192,512]{2,1,0:T(8,128)(2,1)S(1)} %get-tuple-element.48), channel_id=1, source_target_pairs={{0,24},{4,28},{8,16},{12,20},{16,8},{20,12},{24,0},{28,4},{32,56},... | collective-permute-start | bytes 2359304 | tf_op jit(solution)/shard_map/ppermute | solution.py:36
  50.0 4.8 %flash.4.refs_4_ = f32[512,640]{1,0:T(8,128)S(1)} custom-call(s32[86]{0:T(128)S(1)} %compare_select_fusion.1.meta.table, bf16[512,256]{1,0:T(8,128)(2,1)S(1)} %copy-done.5, bf16[768,512]{1,0:T(8,128)(2,1)S(1)} %bitcast.14, bf16[640,512]{1,0:T(8,128)(2,1)S(1)} %bitcast.22, bf16[640,512]{1,0:T(8,128)(2,1)S(1)} %bitcast.20), custom_call_target="tpu_custom_call" | custom-call | flops 5000000000 | bytes 100000 | tf_op jit(solution)/shard_map/flash/pallas_call | solution.py:273
  54.9 3.1 %collective-permute-start.26 = (bf16[64,2048]{1,0:T(8,128)(2,1)S(1)}, bf16[64,2048]{1,0:T(8,128)(2,1)S(1)}, u32[]{:S(2)}, u32[]{:S(2)}) collective-permute-start(bf16[64,2048]{1,0:T(8,128)(2,1)S(1)} %copy-done.3), channel_id=1, source_target_pairs={{0,2},{1,3},{2,0},{3,1},{4,6},{5,7},{6,4},{7,5},{8,10},{9,11},{10,... | collective-permute-start | bytes 786440 | tf_op jit(solution)/shard_map/ppermute | solution.py:49
  58.0 4.8 %flash.6.refs_4_ = f32[512,640]{1,0:T(8,128)S(1)} custom-call(s32[86]{0:T(128)S(1)} %compare_select_fusion.1.meta.table, bf16[512,256]{1,0:T(8,128)(2,1)S(1)} %collective-permute-done.10.refs_0_, bf16[768,512]{1,0:T(8,128)(2,1)S(1)} %bitcast.15, bf16[640,512]{1,0:T(8,128)(2,1)S(1)} %bitcast.23, bf16[640,512]{1,0:T(8,128)(2,1)S(1)} %bitcast.21), custom_call_target="tpu_custom_call" | custom-call | flops 5000000000 | bytes 100000 | tf_op jit(solution)/shard_map/flash/pallas_call | solution.py:273
  66.4 6.6 %flash.7 = f32[512,640]{1,0:T(8,128)S(1)} custom-call(s32[86]{0:T(128)S(1)} %compare_select_fusion.1.meta.table, bf16[512,256]{1,0:T(8,128)(2,1)S(1)} %collective-permute-done.10.refs_0_, bf16[768,512]{1,0:T(8,128)(2,1)S(1)} %bitcast.12, bf16[640,512]{1,0:T(8,128)(2,1)S(1)} %bitcast.16, bf16[640,512]{1,0:T(8,128)(2,1)S(1)} %bitcast.18, ...), custom_call_target="tpu_custom_call" | custom-call | flops 5000000000 | bytes 100000 | tf_op jit(solution)/shard_map/flash/pallas_call | solution.py:273
  74.9 2.5 %collective-permute-start.21 = (bf16[256,2048]{1,0:T(8,128)(2,1)S(1)}, bf16[256,2048]{1,0:T(8,128)(2,1)S(1)}, u32[]{:S(2)}, u32[]{:S(2)}) collective-permute-start(bf16[256,2048]{1,0:T(8,128)(2,1)S(1)} %get-tuple-element.74.refs_8_), channel_id=1, source_target_pairs={{0,2},{1,3},{2,0},{3,1},{4,6},{5,7},{6,4},{7,5},{8,10},{9,11},{10,... | collective-permute-start | bytes 3145736 | tf_op jit(solution)/shard_map/ppermute | solution.py:49
  79.2 9.2 %collective-permute-done.33.refs_3_ = bf16[2,64,2176]{2,1,0:T(8,128)(2,1)S(1)} collective-permute-done((bf16[2,64,2176]{2,1,0:T(8,128)(2,1)S(1)}, bf16[2,64,2176]{2,1,0:T(8,128)(2,1)S(1)}, u32[]{:S(2)}, u32[]{:S(2)}) %collective-permute-start.33) | collective-permute-done | bytes 557088 | tf_op jit(solution)/shard_map/ppermute | solution.py:41
  88.7 11.5 %collective-permute-done.19.refs_10_ = bf16[256,2048]{1,0:T(8,128)(2,1)S(1)} collective-permute-done((bf16[256,2048]{1,0:T(8,128)(2,1)S(1)}, bf16[256,2048]{1,0:T(8,128)(2,1)S(1)}, u32[]{:S(2)}, u32[]{:S(2)}) %collective-permute-start.19) | collective-permute-done | bytes 1048608 | tf_op jit(solution)/shard_map/ppermute | solution.py:49
  101.3 22.1 %collective-permute-done.21.refs_12_ = bf16[256,2048]{1,0:T(8,128)(2,1)S(1)} collective-permute-done((bf16[256,2048]{1,0:T(8,128)(2,1)S(1)}, bf16[256,2048]{1,0:T(8,128)(2,1)S(1)}, u32[]{:S(2)}, u32[]{:S(2)}) %collective-permute-start.21) | collective-permute-done | bytes 1048608 | tf_op jit(solution)/shard_map/ppermute | solution.py:49
  123.4 3.2 %collective-permute-start.37 = (bf16[4,64,2176]{2,1,0:T(8,128)(2,1)S(1)}, bf16[4,64,2176]{2,1,0:T(8,128)(2,1)S(1)}, u32[]{:S(2)}, u32[]{:S(2)}) collective-permute-start(bf16[4,64,2176]{2,1,0:T(8,128)(2,1)S(1)} %get-tuple-element.64.refs_4_), channel_id=1, source_target_pairs={{0,24},{4,12},{8,16},{12,4},{16,8},{20,28},{24,0},{28,20},{32,56},... | collective-permute-start | bytes 3342344 | tf_op jit(solution)/shard_map/ppermute | solution.py:41
  126.6 2.3 %collective-permute-done.27.refs_19_ = bf16[64,2048]{1,0:T(8,128)(2,1)S(1)} collective-permute-done((bf16[64,2048]{1,0:T(8,128)(2,1)S(1)}, bf16[64,2048]{1,0:T(8,128)(2,1)S(1)}, u32[]{:S(2)}, u32[]{:S(2)}) %collective-permute-start.27) | collective-permute-done | bytes 262176 | tf_op jit(solution)/shard_map/ppermute | solution.py:49
  129.5 6.7 %flash.5.mine_ref = f32[512,640]{1,0:T(8,128)S(1)} custom-call(s32[86]{0:T(128)S(1)} %compare_select_fusion.1.meta.table, bf16[512,256]{1,0:T(8,128)(2,1)S(1)} %copy-done.5, bf16[768,512]{1,0:T(8,128)(2,1)S(1)} %bitcast.13, bf16[640,512]{1,0:T(8,128)(2,1)S(1)} %bitcast.17, bf16[640,512]{1,0:T(8,128)(2,1)S(1)} %bitcast.19, f32[512,640]{1,0:T(8,128)S(1)} %flash.4.refs_4_), custom_call_target="tpu_custom_call" | custom-call | flops 5000000000 | bytes 100000 | tf_op jit(solution)/shard_map/flash/pallas_call | solution.py:273
  140.1 2.3 %collective-permute-start.13 = (bf16[256,256]{1,0:T(8,128)(2,1)S(1)}, bf16[256,256]{1,0:T(8,128)(2,1)S(1)}, u32[]{:S(2)}, u32[]{:S(2)}) collective-permute-start(bf16[256,256]{1,0:T(8,128)(2,1)S(1)} %get-tuple-element.76.refs_0_), channel_id=1, source_target_pairs={{0,2},{1,3},{2,0},{3,1},{4,6},{5,7},{6,4},{7,5},{8,10},{9,11},{10,... | collective-permute-start | bytes 393224 | tf_op jit(solution)/shard_map/ppermute | solution.py:49
  145.4 2.4 %collective-permute-start.17 = (bf16[256,256]{1,0:T(8,128)(2,1)S(1)}, bf16[256,256]{1,0:T(8,128)(2,1)S(1)}, u32[]{:S(2)}, u32[]{:S(2)}) collective-permute-start(bf16[256,256]{1,0:T(8,128)(2,1)S(1)} %collective-permute-done.15.refs_4_), channel_id=1, source_target_pairs={{0,2},{1,3},{2,0},{3,1},{4,6},{5,7},{6,4},{7,5},{8,10},{9,11},{10,... | collective-permute-start | bytes 393224 | tf_op jit(solution)/shard_map/ppermute | solution.py:49
  149.7 3.2 %collective-permute-start.35 = (bf16[4,64,2176]{2,1,0:T(8,128)(2,1)S(1)}, bf16[4,64,2176]{2,1,0:T(8,128)(2,1)S(1)}, u32[]{:S(2)}, u32[]{:S(2)}) collective-permute-start(bf16[4,64,2176]{2,1,0:T(8,128)(2,1)S(1)} %get-tuple-element.61.refs_0_), channel_id=1, source_target_pairs={{0,24},{4,12},{8,16},{12,4},{16,8},{20,28},{24,0},{28,20},{32,56},... | collective-permute-start | bytes 3342344 | tf_op jit(solution)/shard_map/ppermute | solution.py:41
  155.8 4.0 %collective-permute-start.39 = (bf16[4,64,2176]{2,1,0:T(8,128)(2,1)S(1)}, bf16[4,64,2176]{2,1,0:T(8,128)(2,1)S(1)}, u32[]{:S(2)}, u32[]{:S(2)}) collective-permute-start(bf16[4,64,2176]{2,1,0:T(8,128)(2,1)S(1)} %collective-permute-done.37.refs_5_), channel_id=1, source_target_pairs={{0,96},{4,36},{8,104},{12,44},{16,112},{20,52},{24,120},{28,60},{3... | collective-permute-start | bytes 3342344 | tf_op jit(solution)/shard_map/ppermute | solution.py:41
  159.8 4.9 %middle.1 = (bf16[256,2048]{1,0:T(8,128)(2,1)S(1)}, f32[64,2048]{1,0:T(8,128)S(1)}) custom-call(s32[86]{0:T(128)S(1)} %compare_select_fusion.1.meta.table, bf16[256,256]{1,0:T(8,128)(2,1)S(1)} %get-tuple-element.76.refs_0_, bf16[256,256]{1,0:T(8,128)(2,1)S(1)} %collective-permute-done.12.refs_1_, bf16[256,256]{1,0:T(8,128)(2,1)S(1)} %collective-permute-done.13.refs_2_, ...), custom_call_target="tpu_custom_call" | custom-call | flops 4000000000 | bytes 100000 | tf_op jit(solution)/shard_map/middle/pallas_call | solution.py:356
  166.4 3.2 %collective-permute-done.38.refs_6_ = bf16[4,64,2176]{2,1,0:T(8,128)(2,1)S(1)} collective-permute-done((bf16[4,64,2176]{2,1,0:T(8,128)(2,1)S(1)}, bf16[4,64,2176]{2,1,0:T(8,128)(2,1)S(1)}, u32[]{:S(2)}, u32[]{:S(2)}) %collective-permute-start.38) | collective-permute-done | bytes 1114144 | tf_op jit(solution)/shard_map/ppermute | solution.py:41
  169.6 8.7 %collective-permute-done.36.refs_3_ = bf16[4,64,2176]{2,1,0:T(8,128)(2,1)S(1)} collective-permute-done((bf16[4,64,2176]{2,1,0:T(8,128)(2,1)S(1)}, bf16[4,64,2176]{2,1,0:T(8,128)(2,1)S(1)}, u32[]{:S(2)}, u32[]{:S(2)}) %collective-permute-start.36) | collective-permute-done | bytes 1114144 | tf_op jit(solution)/shard_map/ppermute | solution.py:41
  178.3 3.2 %collective-permute-done.39.refs_7_ = bf16[4,64,2176]{2,1,0:T(8,128)(2,1)S(1)} collective-permute-done((bf16[4,64,2176]{2,1,0:T(8,128)(2,1)S(1)}, bf16[4,64,2176]{2,1,0:T(8,128)(2,1)S(1)}, u32[]{:S(2)}, u32[]{:S(2)}) %collective-permute-start.39) | collective-permute-done | bytes 1114144 | tf_op jit(solution)/shard_map/ppermute | solution.py:41
  181.6 10.8 %ffn.1 = (f32[256,2048]{1,0:T(8,128)S(1)}, bf16[256,2048]{1,0:T(8,128)(2,1)S(1)}) custom-call(s32[86]{0:T(128)S(1)} %compare_select_fusion.1.meta.table, bf16[256,2048]{1,0:T(8,128)(2,1)S(1)} %get-tuple-element.55.mine_ref, bf16[256,2048]{1,0:T(8,128)(2,1)S(1)} %collective-permute-done.28.other_ref, bf16[4,64,2176]{2,1,0:T(8,128)(2,1)S(1)} %get-tuple-element.61.refs_0_, ...), custom_call_target="tpu_custom_call" | custom-call | flops 8999999488 | bytes 100000 | tf_op jit(solution)/shard_map/ffn/pallas_call | solution.py:433
  192.4 2.6 %collective-permute-done.40.came_ref = bf16[256,2048]{1,0:T(8,128)(2,1)S(1)} collective-permute-done((bf16[256,2048]{1,0:T(8,128)(2,1)S(1)}, bf16[256,2048]{1,0:T(8,128)(2,1)S(1)}, u32[]{:S(2)}, u32[]{:S(2)}) %collective-permute-start.40) | collective-permute-done | bytes 1048608 | tf_op jit(solution)/shard_map/ppermute | solution.py:36
  198.0 6.5 %collective-permute-done.43 = bf16[64,2048]{1,0:T(8,128)(2,1)S(1)} collective-permute-done((bf16[64,2048]{1,0:T(8,128)(2,1)S(1)}, bf16[64,2048]{1,0:T(8,128)(2,1)S(1)}, u32[]{:S(2)}, u32[]{:S(2)}) %collective-permute-start.43) | collective-permute-done | bytes 262176 | tf_op jit(solution)/shard_map/ppermute | solution.py:49
  204.5 2.6 %collective-permute-done.42 = bf16[64,2048]{1,0:T(8,128)(2,1)S(1)} collective-permute-done((bf16[64,2048]{1,0:T(8,128)(2,1)S(1)}, bf16[64,2048]{1,0:T(8,128)(2,1)S(1)}, u32[]{:S(2)}, u32[]{:S(2)}) %collective-permute-start.42) | collective-permute-done | bytes 262176 | tf_op jit(solution)/shard_map/ppermute | solution.py:49
  207.1 4.5 %collective-permute-done.41 = bf16[64,2048]{1,0:T(8,128)(2,1)S(1)} collective-permute-done((bf16[64,2048]{1,0:T(8,128)(2,1)S(1)}, bf16[64,2048]{1,0:T(8,128)(2,1)S(1)}, u32[]{:S(2)}, u32[]{:S(2)}) %collective-permute-start.41) | collective-permute-done | bytes 262176 | tf_op jit(solution)/shard_map/ppermute | solution.py:49
  (102 shorter events, 45.2 us)
Async XLA Ops:
  4.7 10.9 %collective-permute-start = (bf16[256,768]{1,0:T(8,128)(2,1)S(1)}, bf16[256,768]{1,0:T(8,128)(2,1)S(1)}, u32[]{:S(2)}, u32[]{:S(2)}) collective-permute-start(bf16[256,768]{1,0:T(8,128)(2,1)S(1)} %get-tuple-element.40), channel_id=1, source_target_pairs={{0,8},{4,12},{8,0},{12,4},{16,24},{20,28},{24,16},{28,20},{32,40},... | collective-permute-start | bytes 1179656 | tf_op jit(solution)/shard_map/ppermute | solution.py:36
  16.3 13.2 %collective-permute-start.1 = (bf16[1,192,512]{2,1,0:T(8,128)(2,1)S(1)}, bf16[1,192,512]{2,1,0:T(8,128)(2,1)S(1)}, u32[]{:S(2)}, u32[]{:S(2)}) collective-permute-start(bf16[1,192,512]{2,1,0:T(8,128)(2,1)S(1)} %get-tuple-element.42.refs_0_), channel_id=1, source_target_pairs={{0,32},{4,36},{8,40},{12,44},{16,48},{20,52},{24,56},{28,60},{32,0... | collective-permute-start | bytes 589832 | tf_op jit(solution)/shard_map/ppermute | solution.py:36
  19.3 11.7 %collective-permute-start.29 = (bf16[1,64,2176]{2,1,0:T(8,128)(2,1)S(1)}, bf16[1,64,2176]{2,1,0:T(8,128)(2,1)S(1)}, u32[]{:S(2)}, u32[]{:S(2)}) collective-permute-start(bf16[1,64,2176]{2,1,0:T(8,128)(2,1)S(1)} %get-tuple-element.57), channel_id=1, source_target_pairs={{0,4},{4,0},{8,12},{12,8},{16,20},{20,16},{24,28},{28,24},{32,36},... | collective-permute-start | bytes 835592 | tf_op jit(solution)/shard_map/ppermute | solution.py:36
  29.5 15.8 %collective-permute-start.4 = (bf16[2,192,512]{2,1,0:T(8,128)(2,1)S(1)}, bf16[2,192,512]{2,1,0:T(8,128)(2,1)S(1)}, u32[]{:S(2)}, u32[]{:S(2)}) collective-permute-start(bf16[2,192,512]{2,1,0:T(8,128)(2,1)S(1)} %get-tuple-element.45.refs_0_), channel_id=1, source_target_pairs={{0,96},{4,100},{8,104},{12,108},{16,112},{20,116},{24,120},{28,124... | collective-permute-start | bytes 1179656 | tf_op jit(solution)/shard_map/ppermute | solution.py:36
  31.4 13.9 %collective-permute-start.5 = (bf16[2,160,512]{2,1,0:T(8,128)(2,1)S(1)}, bf16[2,160,512]{2,1,0:T(8,128)(2,1)S(1)}, u32[]{:S(2)}, u32[]{:S(2)}) collective-permute-start(bf16[2,160,512]{2,1,0:T(8,128)(2,1)S(1)} %get-tuple-element.46.refs_1_), channel_id=1, source_target_pairs={{0,24},{4,28},{8,16},{12,20},{16,8},{20,12},{24,0},{28,4},{32,56},... | collective-permute-start | bytes 983048 | tf_op jit(solution)/shard_map/ppermute | solution.py:36
  33.9 11.4 %collective-permute-start.6 = (bf16[2,160,512]{2,1,0:T(8,128)(2,1)S(1)}, bf16[2,160,512]{2,1,0:T(8,128)(2,1)S(1)}, u32[]{:S(2)}, u32[]{:S(2)}) collective-permute-start(bf16[2,160,512]{2,1,0:T(8,128)(2,1)S(1)} %get-tuple-element.47.refs_2_), channel_id=1, source_target_pairs={{0,32},{4,36},{8,40},{12,44},{16,48},{20,52},{24,56},{28,60},{32,0... | collective-permute-start | bytes 983048 | tf_op jit(solution)/shard_map/ppermute | solution.py:36
  36.9 38.0 %collective-permute-start.25 = (bf16[64,2048]{1,0:T(8,128)(2,1)S(1)}, bf16[64,2048]{1,0:T(8,128)(2,1)S(1)}, u32[]{:S(2)}, u32[]{:S(2)}) collective-permute-start(bf16[64,2048]{1,0:T(8,128)(2,1)S(1)} %copy-done.3), channel_id=1, source_target_pairs={{0,1},{1,2},{2,3},{3,0},{4,5},{5,6},{6,7},{7,4},{8,9},{9,10},{10,1... | collective-permute-start | bytes 786440 | tf_op jit(solution)/shard_map/ppermute | solution.py:49
  38.4 16.5 %collective-permute-start.10 = (bf16[512,256]{1,0:T(8,128)(2,1)}, bf16[512,256]{1,0:T(8,128)(2,1)S(1)}, u32[]{:S(2)}, u32[]{:S(2)}) collective-permute-start(bf16[512,256]{1,0:T(8,128)(2,1)} %copy-done.4), channel_id=1, source_target_pairs={{0,4},{4,0},{8,12},{12,8},{16,20},{20,16},{24,28},{28,24},{32,36},... | collective-permute-start | bytes 786440 | tf_op jit(solution)/shard_map/ppermute | solution.py:36
  45.5 20.9 %collective-permute-start.7 = (bf16[4,192,512]{2,1,0:T(8,128)(2,1)S(1)}, bf16[4,192,512]{2,1,0:T(8,128)(2,1)S(1)}, u32[]{:S(2)}, u32[]{:S(2)}) collective-permute-start(bf16[4,192,512]{2,1,0:T(8,128)(2,1)S(1)} %get-tuple-element.48), channel_id=1, source_target_pairs={{0,24},{4,28},{8,16},{12,20},{16,8},{20,12},{24,0},{28,4},{32,56},... | collective-permute-start | bytes 2359304 | tf_op jit(solution)/shard_map/ppermute | solution.py:36
  48.5 16.4 %collective-permute-start.8 = (bf16[4,160,512]{2,1,0:T(8,128)(2,1)S(1)}, bf16[4,160,512]{2,1,0:T(8,128)(2,1)S(1)}, u32[]{:S(2)}, u32[]{:S(2)}) collective-permute-start(bf16[4,160,512]{2,1,0:T(8,128)(2,1)S(1)} %get-tuple-element.49), channel_id=1, source_target_pairs={{0,32},{4,36},{8,40},{12,44},{16,48},{20,52},{24,56},{28,60},{32,0... | collective-permute-start | bytes 1966088 | tf_op jit(solution)/shard_map/ppermute | solution.py:36
  48.6 17.5 %collective-permute-start.9 = (bf16[4,160,512]{2,1,0:T(8,128)(2,1)S(1)}, bf16[4,160,512]{2,1,0:T(8,128)(2,1)S(1)}, u32[]{:S(2)}, u32[]{:S(2)}) collective-permute-start(bf16[4,160,512]{2,1,0:T(8,128)(2,1)S(1)} %get-tuple-element.50), channel_id=1, source_target_pairs={{0,96},{4,100},{8,104},{12,108},{16,112},{20,116},{24,120},{28,124... | collective-permute-start | bytes 1966088 | tf_op jit(solution)/shard_map/ppermute | solution.py:36
  54.9 22.5 %collective-permute-start.26 = (bf16[64,2048]{1,0:T(8,128)(2,1)S(1)}, bf16[64,2048]{1,0:T(8,128)(2,1)S(1)}, u32[]{:S(2)}, u32[]{:S(2)}) collective-permute-start(bf16[64,2048]{1,0:T(8,128)(2,1)S(1)} %copy-done.3), channel_id=1, source_target_pairs={{0,2},{1,3},{2,0},{3,1},{4,6},{5,7},{6,4},{7,5},{8,10},{9,11},{10,... | collective-permute-start | bytes 786440 | tf_op jit(solution)/shard_map/ppermute | solution.py:49
  64.8 14.0 %collective-permute-start.32 = (bf16[2,64,2176]{2,1,0:T(8,128)(2,1)S(1)}, bf16[2,64,2176]{2,1,0:T(8,128)(2,1)S(1)}, u32[]{:S(2)}, u32[]{:S(2)}) collective-permute-start(bf16[2,64,2176]{2,1,0:T(8,128)(2,1)S(1)} %get-tuple-element.58.refs_0_), channel_id=1, source_target_pairs={{0,8},{4,28},{8,0},{12,20},{16,24},{20,12},{24,16},{28,4},{32,40},... | collective-permute-start | bytes 1671176 | tf_op jit(solution)/shard_map/ppermute | solution.py:41
  73.0 56.4 %collective-permute-start.11 = (f32[512,640]{1,0:T(8,128)S(1)}, f32[512,640]{1,0:T(8,128)S(1)}, u32[]{:S(2)}, u32[]{:S(2)}) collective-permute-start(f32[512,640]{1,0:T(8,128)S(1)} %flash.7), channel_id=1, source_target_pairs={{0,4},{4,0},{8,12},{12,8},{16,20},{20,16},{24,28},{28,24},{32,36},... | collective-permute-start | bytes 3932168 | tf_op jit(solution)/shard_map/ppermute | solution.py:36
  73.3 26.8 %collective-permute-start.19 = (bf16[256,2048]{1,0:T(8,128)(2,1)S(1)}, bf16[256,2048]{1,0:T(8,128)(2,1)S(1)}, u32[]{:S(2)}, u32[]{:S(2)}) collective-permute-start(bf16[256,2048]{1,0:T(8,128)(2,1)S(1)} %get-tuple-element.74.refs_8_), channel_id=1, source_target_pairs={{0,1},{1,2},{2,3},{3,0},{4,5},{5,6},{6,7},{7,4},{8,9},{9,10},{10,1... | collective-permute-start | bytes 3145736 | tf_op jit(solution)/shard_map/ppermute | solution.py:49
  74.9 48.5 %collective-permute-start.21 = (bf16[256,2048]{1,0:T(8,128)(2,1)S(1)}, bf16[256,2048]{1,0:T(8,128)(2,1)S(1)}, u32[]{:S(2)}, u32[]{:S(2)}) collective-permute-start(bf16[256,2048]{1,0:T(8,128)(2,1)S(1)} %get-tuple-element.74.refs_8_), channel_id=1, source_target_pairs={{0,2},{1,3},{2,0},{3,1},{4,6},{5,7},{6,4},{7,5},{8,10},{9,11},{10,... | collective-permute-start | bytes 3145736 | tf_op jit(solution)/shard_map/ppermute | solution.py:49
  77.4 51.5 %collective-permute-start.23 = (bf16[256,2048]{1,0:T(8,128)(2,1)S(1)}, bf16[256,2048]{1,0:T(8,128)(2,1)S(1)}, u32[]{:S(2)}, u32[]{:S(2)}) collective-permute-start(bf16[256,2048]{1,0:T(8,128)(2,1)S(1)} %get-tuple-element.74.refs_8_), channel_id=1, source_target_pairs={{0,3},{1,0},{2,1},{3,2},{4,7},{5,4},{6,5},{7,6},{8,11},{9,8},{10,9... | collective-permute-start | bytes 3145736 | tf_op jit(solution)/shard_map/ppermute | solution.py:49
  88.4 40.5 %collective-permute-start.27 = (bf16[64,2048]{1,0:T(8,128)(2,1)S(1)}, bf16[64,2048]{1,0:T(8,128)(2,1)S(1)}, u32[]{:S(2)}, u32[]{:S(2)}) collective-permute-start(bf16[64,2048]{1,0:T(8,128)(2,1)S(1)} %copy-done.3), channel_id=1, source_target_pairs={{0,3},{1,0},{2,1},{3,2},{4,7},{5,4},{6,5},{7,6},{8,11},{9,8},{10,9... | collective-permute-start | bytes 786440 | tf_op jit(solution)/shard_map/ppermute | solution.py:49
  100.2 37.6 %collective-permute-start.34 = (bf16[4,64,2176]{2,1,0:T(8,128)(2,1)S(1)}, bf16[4,64,2176]{2,1,0:T(8,128)(2,1)S(1)}, u32[]{:S(2)}, u32[]{:S(2)}) collective-permute-start(bf16[4,64,2176]{2,1,0:T(8,128)(2,1)S(1)} %get-tuple-element.61.refs_0_), channel_id=1, source_target_pairs={{0,96},{4,36},{8,104},{12,44},{16,112},{20,52},{24,120},{28,60},{3... | collective-permute-start | bytes 3342344 | tf_op jit(solution)/shard_map/ppermute | solution.py:41
  123.4 16.7 %collective-permute-start.37 = (bf16[4,64,2176]{2,1,0:T(8,128)(2,1)S(1)}, bf16[4,64,2176]{2,1,0:T(8,128)(2,1)S(1)}, u32[]{:S(2)}, u32[]{:S(2)}) collective-permute-start(bf16[4,64,2176]{2,1,0:T(8,128)(2,1)S(1)} %get-tuple-element.64.refs_4_), channel_id=1, source_target_pairs={{0,24},{4,12},{8,16},{12,4},{16,8},{20,28},{24,0},{28,20},{32,56},... | collective-permute-start | bytes 3342344 | tf_op jit(solution)/shard_map/ppermute | solution.py:41
  128.9 11.2 %collective-permute-start.20 = (bf16[256,2048]{1,0:T(8,128)(2,1)S(1)}, bf16[256,2048]{1,0:T(8,128)(2,1)S(1)}, u32[]{:S(2)}, u32[]{:S(2)}) collective-permute-start(bf16[256,2048]{1,0:T(8,128)(2,1)S(1)} %collective-permute-done.19.refs_10_), channel_id=1, source_target_pairs={{0,4},{4,0},{8,12},{12,8},{16,20},{20,16},{24,28},{28,24},{32,36},... | collective-permute-start | bytes 3145736 | tf_op jit(solution)/shard_map/ppermute | solution.py:36
  128.9 13.6 %collective-permute-start.22 = (bf16[256,2048]{1,0:T(8,128)(2,1)S(1)}, bf16[256,2048]{1,0:T(8,128)(2,1)S(1)}, u32[]{:S(2)}, u32[]{:S(2)}) collective-permute-start(bf16[256,2048]{1,0:T(8,128)(2,1)S(1)} %collective-permute-done.21.refs_12_), channel_id=1, source_target_pairs={{0,4},{4,0},{8,12},{12,8},{16,20},{20,16},{24,28},{28,24},{32,36},... | collective-permute-start | bytes 3145736 | tf_op jit(solution)/shard_map/ppermute | solution.py:36
  129.4 16.0 %collective-permute-start.24 = (bf16[256,2048]{1,0:T(8,128)(2,1)S(1)}, bf16[256,2048]{1,0:T(8,128)(2,1)S(1)}, u32[]{:S(2)}, u32[]{:S(2)}) collective-permute-start(bf16[256,2048]{1,0:T(8,128)(2,1)S(1)} %collective-permute-done.23.refs_14_), channel_id=1, source_target_pairs={{0,4},{4,0},{8,12},{12,8},{16,20},{20,16},{24,28},{28,24},{32,36},... | collective-permute-start | bytes 3145736 | tf_op jit(solution)/shard_map/ppermute | solution.py:36
  144.2 10.5 %collective-permute-start.16 = (bf16[256,256]{1,0:T(8,128)(2,1)S(1)}, bf16[256,256]{1,0:T(8,128)(2,1)S(1)}, u32[]{:S(2)}, u32[]{:S(2)}) collective-permute-start(bf16[256,256]{1,0:T(8,128)(2,1)S(1)} %collective-permute-done.15.refs_4_), channel_id=1, source_target_pairs={{0,1},{1,2},{2,3},{3,0},{4,5},{5,6},{6,7},{7,4},{8,9},{9,10},{10,1... | collective-permute-start | bytes 393224 | tf_op jit(solution)/shard_map/ppermute | solution.py:49
  148.9 10.9 %collective-permute-start.18 = (bf16[256,256]{1,0:T(8,128)(2,1)S(1)}, bf16[256,256]{1,0:T(8,128)(2,1)S(1)}, u32[]{:S(2)}, u32[]{:S(2)}) collective-permute-start(bf16[256,256]{1,0:T(8,128)(2,1)S(1)} %collective-permute-done.15.refs_4_), channel_id=1, source_target_pairs={{0,3},{1,0},{2,1},{3,2},{4,7},{5,4},{6,5},{7,6},{8,11},{9,8},{10,9... | collective-permute-start | bytes 393224 | tf_op jit(solution)/shard_map/ppermute | solution.py:49
  149.7 16.7 %collective-permute-start.35 = (bf16[4,64,2176]{2,1,0:T(8,128)(2,1)S(1)}, bf16[4,64,2176]{2,1,0:T(8,128)(2,1)S(1)}, u32[]{:S(2)}, u32[]{:S(2)}) collective-permute-start(bf16[4,64,2176]{2,1,0:T(8,128)(2,1)S(1)} %get-tuple-element.61.refs_0_), channel_id=1, source_target_pairs={{0,24},{4,12},{8,16},{12,4},{16,8},{20,28},{24,0},{28,20},{32,56},... | collective-permute-start | bytes 3342344 | tf_op jit(solution)/shard_map/ppermute | solution.py:41
  152.9 16.7 %collective-permute-start.38 = (bf16[4,64,2176]{2,1,0:T(8,128)(2,1)S(1)}, bf16[4,64,2176]{2,1,0:T(8,128)(2,1)S(1)}, u32[]{:S(2)}, u32[]{:S(2)}) collective-permute-start(bf16[4,64,2176]{2,1,0:T(8,128)(2,1)S(1)} %get-tuple-element.64.refs_4_), channel_id=1, source_target_pairs={{0,96},{4,36},{8,104},{12,44},{16,112},{20,52},{24,120},{28,60},{3... | collective-permute-start | bytes 3342344 | tf_op jit(solution)/shard_map/ppermute | solution.py:41
  154.7 23.6 %collective-permute-start.36 = (bf16[4,64,2176]{2,1,0:T(8,128)(2,1)S(1)}, bf16[4,64,2176]{2,1,0:T(8,128)(2,1)S(1)}, u32[]{:S(2)}, u32[]{:S(2)}) collective-permute-start(bf16[4,64,2176]{2,1,0:T(8,128)(2,1)S(1)} %collective-permute-done.34.refs_1_), channel_id=1, source_target_pairs={{0,24},{4,12},{8,16},{12,4},{16,8},{20,28},{24,0},{28,20},{32,56},... | collective-permute-start | bytes 3342344 | tf_op jit(solution)/shard_map/ppermute | solution.py:41
  155.8 25.7 %collective-permute-start.39 = (bf16[4,64,2176]{2,1,0:T(8,128)(2,1)S(1)}, bf16[4,64,2176]{2,1,0:T(8,128)(2,1)S(1)}, u32[]{:S(2)}, u32[]{:S(2)}) collective-permute-start(bf16[4,64,2176]{2,1,0:T(8,128)(2,1)S(1)} %collective-permute-done.37.refs_5_), channel_id=1, source_target_pairs={{0,96},{4,36},{8,104},{12,44},{16,112},{20,52},{24,120},{28,60},{3... | collective-permute-start | bytes 3342344 | tf_op jit(solution)/shard_map/ppermute | solution.py:41
  164.7 16.9 %collective-permute-start.28 = (bf16[256,2048]{1,0:T(8,128)(2,1)S(1)}, bf16[256,2048]{1,0:T(8,128)(2,1)S(1)}, u32[]{:S(2)}, u32[]{:S(2)}) collective-permute-start(bf16[256,2048]{1,0:T(8,128)(2,1)S(1)} %get-tuple-element.55.mine_ref), channel_id=1, source_target_pairs={{0,4},{4,0},{8,12},{12,8},{16,20},{20,16},{24,28},{28,24},{32,36},... | collective-permute-start | bytes 3145736 | tf_op jit(solution)/shard_map/ppermute | solution.py:36
  196.4 10.7 %collective-permute-start.42 = (bf16[64,2048]{1,0:T(8,128)(2,1)S(1)}, bf16[64,2048]{1,0:T(8,128)(2,1)S(1)}, u32[]{:S(2)}, u32[]{:S(2)}) collective-permute-start(bf16[64,2048]{1,0:T(8,128)(2,1)S(1)} %get-tuple-element.71), channel_id=1, source_target_pairs={{0,2},{1,3},{2,0},{3,1},{4,6},{5,7},{6,4},{7,5},{8,10},{9,11},{10,... | collective-permute-start | bytes 786440 | tf_op jit(solution)/shard_map/ppermute | solution.py:49
  198.0 13.5 %collective-permute-start.41 = (bf16[64,2048]{1,0:T(8,128)(2,1)S(1)}, bf16[64,2048]{1,0:T(8,128)(2,1)S(1)}, u32[]{:S(2)}, u32[]{:S(2)}) collective-permute-start(bf16[64,2048]{1,0:T(8,128)(2,1)S(1)} %get-tuple-element.70), channel_id=1, source_target_pairs={{0,1},{1,2},{2,3},{3,0},{4,5},{5,6},{6,7},{7,4},{8,9},{9,10},{10,1... | collective-permute-start | bytes 786440 | tf_op jit(solution)/shard_map/ppermute | solution.py:49
  (25 other events, 184.1 us)
where the time goes:
time: 214 us; the launch traced here: 212 us
  waiting for transfers between devices  99.6 us (47%)
  starting transfers between devices  64.1 us (30%)
  Pallas kernels  42.7 us (20%)
  local copies, waits for them, and re-layouts  4.09 us (2%)
    ppermute x15, waiting for transfers between devices, shift_x(): return lax.ppermute(array, 'tp', [(i, (i + d) % 4) for i in range(4)])  51 us
    ppermute x10, waiting for transfers between devices, chip_swap_by_core(): return lax.ppermute(array, 'sp', pairs)  29 us
    ppermute x19, starting transfers between devices, chip_swap(): return lax.ppermute(array, 'sp', pairs)  27.3 us
    pallas_call x4, Pallas kernels, flash(): pl.pallas_call(functools.partial(flash_kernel, group, far, scale), grid=(...  22.9 us
    ppermute x15, starting transfers between devices, shift_x(): return lax.ppermute(array, 'tp', [(i, (i + d) % 4) for i in range(4)])  20.9 us
    ppermute x19, waiting for transfers between devices, chip_swap(): return lax.ppermute(array, 'sp', pairs)  19.6 us
    ppermute x10, starting transfers between devices, chip_swap_by_core(): return lax.ppermute(array, 'sp', pairs)  15.9 us
    pallas_call x1, Pallas kernels, ffn(): pl.pallas_call(ffn_kernel, in_specs=[pl.BlockSpec(memory_space=pltpu.SMEM...  10.8 us
  transfers between devices with their start and end apart: 44, of which 22 were waited for; matrix products, arithmetic and copies ran while one was open for 0% of the time, Pallas kernels for 14%

commit v1 on v0

--- a/solution.py
+++ b/solution.py
@@ -90,7 +90,7 @@
     return pl.CostEstimate(flops=int(us * 1e9), bytes_accessed=int(1e5), transcendentals=0)
 
 
-def vmem_params(mib=24, **kw):
+def vmem_params(mib=16, **kw):
     return pltpu.CompilerParams(vmem_limit_bytes=mib << 20, **kw)
 
 
@@ -132,7 +132,7 @@
             pltpu.VMEM((2, 256, 768), BF16),
             pltpu.SemaphoreType.DMA((5,)),
         ],
-        compiler_params=vmem_params(16),
+        compiler_params=vmem_params(63),
         cost_estimate=cost(1),
         name="pack",
     )(meta, keys, values, queries)
@@ -143,7 +143,7 @@
     for k in range(2):
         cols = slice(704 * k, 704 * k + 704)
         block = jnp.concatenate(
-            [gate[:, cols], up[:, cols], down[cols, :].T, jnp.zeros((64, 64), BF16)], axis=1
+            [gate[:, cols], up[:, cols], down[:, cols], jnp.zeros((64, 64), BF16)], axis=1
         )
 
         @pl.when(first == (k == 0))
@@ -159,15 +159,42 @@
     return pl.pallas_call(
         weights_kernel,
         grid=(1,),
-        in_specs=[pl.BlockSpec(memory_space=pltpu.SMEM)]
-        + [whole((64, 1408))] * 2
-        + [whole((1408, 64))],
+        in_specs=[pl.BlockSpec(memory_space=pltpu.SMEM)] + [whole((64, 1408))] * 3,
         out_specs=[whole((1, 64, 2176))] * 2,
         out_shape=[jax.ShapeDtypeStruct((1, 64, 2176), BF16)] * 2,
-        compiler_params=vmem_params(),
+        compiler_params=vmem_params(63),
         cost_estimate=cost(2),
         name="weights",
     )(meta, gate, up, down)
+
+
+def lines_kernel(meta, w_out, stream, out_ref, held, sem):
+    half = pl.multiple_of((meta[0] ^ lax.rem(meta[META_Q] // 256, 2)) * 256, 256)
+    loads = [
+        pltpu.make_async_copy(w_out.at[pl.ds(half, 256)], held.at[pl.ds(0, 256)], sem.at[0]),
+        pltpu.make_async_copy(stream, held.at[pl.ds(256, 64)], sem.at[1]),
+    ]
+    for load in loads:
+        load.start()
+    for load in loads:
+        load.wait()
+    store = pltpu.make_async_copy(held, out_ref, sem.at[2])
+    store.start()
+    store.wait()
+
+
+def lines(meta, w_out, stream):
+    in_hbm = pl.BlockSpec(memory_space=pltpu.HBM)
+    return pl.pallas_call(
+        lines_kernel,
+        in_specs=[pl.BlockSpec(memory_space=pltpu.SMEM)] + [in_hbm] * 2,
+        out_specs=in_hbm,
+        out_shape=jax.ShapeDtypeStruct((320, 2048), BF16),
+        scratch_shapes=[pltpu.VMEM((320, 2048), BF16), pltpu.SemaphoreType.DMA((3,))],
+        compiler_params=vmem_params(63),
+        cost_estimate=cost(2),
+        name="lines",
+    )(meta, w_out, stream)
 
 
 def thirds_kernel(own, taken, *outs):
@@ -214,23 +241,19 @@
     )(*held, *far)
 
 
-def flash_kernel(group, far, scale, meta, *refs):
-    q_ref, kv_refs, rest = refs[0], refs[1:4], refs[4:]
-    out_ref = rest[-1]
+def flash_kernel(block, far, scale, meta, *refs):
+    kv_refs, rest = refs[2:5], refs[5:]
     step = pl.program_id(0)
     row = lax.broadcasted_iota(jnp.int32, (256, 1), 0)
-    qpos = meta[META_Q + group + step] + ((meta[1] + (row >> 6)) & 3) * 64 + (row & 63)
+    qpos = (
+        meta[META_Q + block + 2 * step] + ((meta[1] + (row >> 6)) & 3) * 64 + (row & 63)
+    )
+    queries = jnp.where(step == 0, refs[0][...], refs[1][...])
     state = []
-    for s in range(2):
-        if far:
-            st = rest[0]
-            state.append(
-                (st[:, 512 + s : 513 + s], st[:, 514 + s : 515 + s], st[:, 256 * s : 256 * s + 256])
-            )
-        else:
-            state.append(
-                (jnp.full((256, 1), NEG, F32), jnp.zeros((256, 1), F32), jnp.zeros((256, 256), F32))
-            )
+    for _ in range(2):
+        state.append(
+            (jnp.full((256, 1), NEG, F32), jnp.zeros((256, 1), F32), jnp.zeros((256, 256), F32))
+        )
     for t in range(3):
         kv_ref, half = kv_refs[t], KV_ROWS[t] // 2
         key = lax.broadcasted_iota(jnp.int32, (1, 8 * half), 1)
@@ -242,7 +265,7 @@
         for s in range(2):
             top, total, acc = state[s]
             scores = lax.dot_general(
-                q_ref[:, 128 * s : 128 * s + 128],
+                queries[:, 128 * s : 128 * s + 128],
                 kv_ref[:, 128 * s : 128 * s + 128],
                 (((1,), (1,)), ((), ())),
                 preferred_element_type=F32,
@@ -259,29 +282,50 @@
     lane = lax.broadcasted_iota(jnp.int32, (256, 128), 1)
     tail = jnp.zeros((256, 128), F32)
     for s in range(2):
-        top, total, acc = state[s]
-        out_ref[:, 256 * s : 256 * s + 256] = acc
-        tail = jnp.where(lane == s, top, tail)
-        tail = jnp.where(lane == 2 + s, total, tail)
-    out_ref[:, 512:640] = tail
-
-
-def flash(meta, q, kvs, group, far, state, us):
+        tail = jnp.where(lane == s, state[s][0], tail)
+        tail = jnp.where(lane == 2 + s, state[s][1], tail)
+    for k in range(2):
+
+        @pl.when(step == k)
+        def _():
+            out_ref = rest[k - 2]
+            if not far:
+                for s in range(2):
+                    out_ref[:, 256 * s : 256 * s + 256] = state[s][2]
+                out_ref[:, 512:640] = tail
+            else:
+                near = rest[k]
+                ends = jnp.zeros((256, 128), F32)
+                for s in range(2):
+                    top, total, acc = state[s]
+                    near_top = near[:, 512 + s : 513 + s]
+                    both_top = jnp.maximum(top, near_top)
+                    fade = jnp.exp2((top - both_top) * scale)
+                    near_fade = jnp.exp2((near_top - both_top) * scale)
+                    total = total * fade + near[:, 514 + s : 515 + s] * near_fade
+                    cols = slice(256 * s, 256 * s + 256)
+                    out_ref[:, cols] = acc * fade + near[:, cols] * near_fade
+                    ends = jnp.where(lane == s, both_top, ends)
+                    ends = jnp.where(lane == 2 + s, total, ends)
+                out_ref[:, 512:640] = ends
+
+
+def flash(meta, block, q_mine, q_other, kvs, far, states, us):
     scale = float(128**-0.5 * np.log2(np.e))
-    row_block = lambda width: pl.BlockSpec((256, width), lambda i: (i, 0))
     kvs = [a.reshape(-1, 512) for a in kvs]
     return pl.pallas_call(
-        functools.partial(flash_kernel, group, far, scale),
+        functools.partial(flash_kernel, block, far, scale),
         grid=(2,),
-        in_specs=[pl.BlockSpec(memory_space=pltpu.SMEM), row_block(256)]
-        + [pl.BlockSpec(a.shape, lambda i: (0, 0)) for a in kvs]
-        + [row_block(640)] * far,
-        out_specs=row_block(640),
-        out_shape=jax.ShapeDtypeStruct((512, 640), F32),
+        in_specs=[pl.BlockSpec(memory_space=pltpu.SMEM)]
+        + [pl.BlockSpec((256, 256), lambda i: (block, 0))] * 2
+        + [whole(a.shape) for a in kvs]
+        + [whole((256, 640))] * len(states),
+        out_specs=[whole((256, 640))] * 2,
+        out_shape=[jax.ShapeDtypeStruct((256, 640), F32)] * 2,
         compiler_params=vmem_params(),
         cost_estimate=cost(us),
         name="flash",
-    )(meta, q, *kvs, *([state] if far else []))
+    )(meta, q_mine, q_other, *kvs, *states)
 
 
 def merge_kernel(meta, lam, mine_ref, other_ref, gain_ref, out_ref):
@@ -296,41 +340,65 @@
         maps.append((mine_ref[:, cols] * fade_a + other_ref[:, cols] * fade_b) / total)
     contrast = maps[0] - lax.select(meta[0] == 1, lam[1], lam[0]) * maps[1]
     power = jnp.mean(contrast * contrast, axis=-1, keepdims=True)
-    out_ref[0] = (contrast * lax.rsqrt(power + EPS) * gain_ref[...]).astype(BF16)
+    out_ref[...] = (contrast * lax.rsqrt(power + EPS) * gain_ref[...]).astype(BF16)
 
 
 def merge(meta, lam, mine, other, gain):
     return pl.pallas_call(
         merge_kernel,
-        grid=(2,),
-        in_specs=[
-            pl.BlockSpec(memory_space=pltpu.SMEM),
-            pl.BlockSpec(memory_space=pltpu.SMEM),
-            pl.BlockSpec((256, 640), lambda i: (i, 0)),
-            pl.BlockSpec((256, 640), lambda i: (i, 0)),
-            pl.BlockSpec((1, 256), lambda i: (0, 0)),
-        ],
-        out_specs=pl.BlockSpec((1, 256, 256), lambda i: (i, 0, 0)),
-        out_shape=jax.ShapeDtypeStruct((2, 256, 256), BF16),
+        grid=(1,),
+        in_specs=[pl.BlockSpec(memory_space=pltpu.SMEM)] * 2
+        + [whole((256, 640))] * 2
+        + [whole((1, 256))],
+        out_specs=whole((256, 256)),
+        out_shape=jax.ShapeDtypeStruct((256, 256), BF16),
         compiler_params=vmem_params(),
-        cost_estimate=cost(2),
+        cost_estimate=cost(1),
         name="merge",
     )(meta, lam, mine, other, gain)
 
 
+def merge_last_kernel(meta, lam, mine_ref, other_ref, gain_ref, passed_ref, out_ref, own):
+    merge_kernel(meta, lam, mine_ref, other_ref, gain_ref, own)
+    straight = lax.rem(meta[META_Q] // 256, 2) == 0
+    out_ref[:, :256] = jnp.where(straight, own[...], passed_ref[...])
+    out_ref[:, 256:] = jnp.where(straight, passed_ref[...], own[...])
+
+
+def merge_last(meta, lam, mine, other, gain, passed):
+    return pl.pallas_call(
+        merge_last_kernel,
+        grid=(1,),
+        in_specs=[pl.BlockSpec(memory_space=pltpu.SMEM)] * 2
+        + [whole((256, 640))] * 2
+        + [whole((1, 256)), whole((256, 256))],
+        out_specs=whole((256, 512)),
+        out_shape=jax.ShapeDtypeStruct((256, 512), BF16),
+        scratch_shapes=[pltpu.VMEM((256, 256), BF16)],
+        compiler_params=vmem_params(),
+        cost_estimate=cost(1),
+        name="merge_last",
+    )(meta, lam, mine, other, gain, passed)
+
+
 def middle_kernel(meta, *refs):
-    owns, passes, weights, streams = refs[0:4], refs[4:8], refs[8:16], refs[16:20]
-    gain_ref, normed_ref, own_ref, scratch, power = refs[20:]
+    blocks, mines, others = refs[0:4], refs[4:8], refs[8:11]
+    local, gain_ref, normed_ref, own_ref, scratch, power = refs[11:]
     step = pl.program_id(0)
-    total = jnp.concatenate([streams[d][...] for d in (0, 3, 2, 1)], axis=0).astype(F32)
-    straight = (meta[META_Q] // 256) % 2 == 0
+    total = jnp.concatenate([mines[d][256:] for d in (0, 3, 2, 1)], axis=0).astype(F32)
+    core = lax.rem(meta[META_Q] // 256, 2)
+    rest = pl.ds(pl.multiple_of((1 - (meta[0] ^ core)) * 256, 256), 256)
     for d in range(4):
-        own, passed = owns[d][...], passes[d][...]
+        rows = blocks[d][...]
+        if d:
+            rows = jnp.concatenate([rows[64 * d :], rows[: 64 * d]], axis=0)
         for half in range(2):
-            block = jnp.where(straight, *((own, passed) if half == 0 else (passed, own)))
-            if d:
-                block = jnp.concatenate([block[64 * d :], block[: 64 * d]], axis=0)
-            total += jnp.dot(block, weights[2 * d + half][...], preferred_element_type=F32)
+            block = rows[:, 256 * half : 256 * half + 256]
+            if half == 0:
+                weights = mines[d][:256]
+            else:
+                weights = others[d - 1][:256] if d else local[rest, :]
+            total += jnp.dot(block, weights, preferred_element_type=F32)
     squares = jnp.sum(total * total, axis=-1, keepdims=True)
 
     @pl.when(step == 0)
@@ -352,14 +420,14 @@
             normed_ref[:, cols] = (scratch[k] * root * gain_ref[:, cols]).astype(BF16)
 
 
-def middle_call(meta, owns, passes, weights, streams, gain):
+def middle_call(meta, blocks, mines, others, w_out, gain):
     return pl.pallas_call(
         middle_kernel,
         grid=(4,),
         in_specs=[pl.BlockSpec(memory_space=pltpu.SMEM)]
-        + [pl.BlockSpec((256, 256), lambda i: (0, 0))] * 8
-        + [pl.BlockSpec((256, 512), lambda i: (0, i))] * 8
-        + [pl.BlockSpec((64, 512), lambda i: (0, i))] * 4
+        + [pl.BlockSpec((256, 512), lambda i: (0, 0))] * 4
+        + [pl.BlockSpec((320, 512), lambda i: (0, i))] * 7
+        + [pl.BlockSpec((512, 512), lambda i: (0, i))]
         + [pl.BlockSpec((1, 2048), lambda i: (0, 0))],
         out_specs=[
             pl.BlockSpec((256, 2048), lambda i: (0, 0)),
@@ -370,7 +438,7 @@
         compiler_params=vmem_params(),
         cost_estimate=cost(4),
         name="middle",
-    )(meta, *owns, *passes, *weights, *streams, gain)
+    )(meta, *blocks, *mines, *others, w_out, gain)
 
 
 def ffn_kernel(table, mine_ref, other_ref, *refs):
@@ -394,29 +462,24 @@
         both[:256, cols] = jnp.dot(other_ref[...], gu[:, cols], preferred_element_type=F32)
         both[256:, cols] = jnp.dot(mine_ref[...], gu[:, cols], preferred_element_type=F32)
 
-    def gate_up_pair(k, _):
-        gate_up(pl.ds(pl.multiple_of(k * 256, 256), 256))
-        return 0
-
     first, second = gu.at[:, pl.ds(0, 768)], gu.at[:, pl.ds(768, 640)]
     pltpu.make_async_copy(first, first, sem.at[0]).wait()
-    lax.fori_loop(0, 3, gate_up_pair, 0)
+    gate_up(pl.ds(0, 768))
     pltpu.make_async_copy(second, second, sem.at[1]).wait()
-    lax.fori_loop(3, 5, gate_up_pair, 0)
-    gate_up(pl.ds(1280, 128))
+    gate_up(pl.ds(768, 640))
 
     def activate(k, _):
-        rows = pl.ds(pl.multiple_of(k * 64, 64), 64)
+        rows = pl.ds(pl.multiple_of(k * 128, 128), 128)
         gate, up = both[rows, :704], both[rows, 704:]
         hidden[rows, :704] = (gate / (1.0 + jnp.exp(-gate)) * up).astype(BF16)
-        hidden[rows, 704:] = jnp.zeros((64, 64), BF16)
+        hidden[rows, 704:] = jnp.zeros((128, 64), BF16)
         return 0
 
-    lax.fori_loop(0, 8, activate, 0)
+    lax.fori_loop(0, 4, activate, 0)
     pltpu.make_async_copy(down, down, sem.at[2]).wait()
 
     def project(k, _):
-        rows = pl.ds(pl.multiple_of(k * 256, 256), 256)
+        rows = pl.ds(pl.multiple_of(k * 512, 512), 512)
         part = lax.dot_general(
             hidden[...], down[rows, :], (((1,), (1,)), ((), ())), preferred_element_type=F32
         )
@@ -424,7 +487,7 @@
         keep_ref[:, rows] = part[256:]
         return 0
 
-    lax.fori_loop(0, 8, project, 0)
+    lax.fori_loop(0, 4, project, 0)
 
 
 def ffn(table, mine, other, pieces):
@@ -442,7 +505,7 @@
             pltpu.VMEM((512, 768), BF16),
             pltpu.SemaphoreType.DMA((3,)),
         ],
-        compiler_params=vmem_params(),
+        compiler_params=vmem_params(28),
         cost_estimate=cost(9),
         name="ffn",
     )(table, mine, other, *pieces)
@@ -485,43 +548,41 @@
     *kv_held, q_mine = thirds(own, chip_swap(given, STEP["yl"]))
     q_other = core_swap(q_mine)
 
-    w_own, w_given = split_weights(meta, w_gate, w_up, w_down)
+    w_own, w_given = split_weights(meta, w_gate, w_up, w_down.T)
     w_held = [w_own, core_swap(w_given)]
 
-    own_rows = (head ^ core) * 256
-    w_mine = lax.dynamic_slice(w_out, (own_rows, 0), (256, 2048))
-    w_other = lax.dynamic_slice(w_out, (256 - own_rows, 0), (256, 2048))
-
-    streams = [stream] + [shift_x(stream, d) for d in (1, 2, 3)]
-    w_mines = [w_mine] + [shift_x(w_mine, d) for d in (1, 2, 3)]
+    line = lines(meta, w_out, stream)
+    w_mines = [line] + [shift_x(line, d) for d in (1, 2, 3)]
     for s in range(3):
         kv_far = [chip_swap(kv_held[t], STEP[KV_ORDERS[t][s]]) for t in range(3)]
         if s < 2:
             kv_held = join(kv_held, kv_far)
-        w_far = [
-            chip_swap_by_core(w_held[h], [STEP[W_ORDERS[c][h][s]] for c in range(2)])
-            for h in range(2)
-        ]
-        if s < 2:
-            w_held = join(w_held, w_far)
-    w_others = [w_other] + [core_swap(after(w, *kv_far)) for w in w_mines[1:]]
-
-    state_other = flash(meta, q_other, kv_held, 2, 0, None, 5)
-    state_mine = flash(meta, q_mine, kv_held, 0, 0, None, 5)
-    last = [[STEP[W_ORDERS[c][h][3]] for c in range(2)] for h in range(2)]
-    w_last = [chip_swap_by_core(after(w_held[h], *kv_far), last[h]) for h in range(2)]
-    sent = flash(meta, q_other, kv_far, 2, 1, after(state_other, state_mine), 5)
+    states_p = flash(meta, 1, q_mine, q_other, kv_held, 0, [], 5)
+    states_o = flash(meta, 0, after(q_mine, *states_p), q_other, kv_held, 0, [], 5)
+
+    def w_step(s, h, array):
+        return chip_swap_by_core(array, [STEP[W_ORDERS[c][h][s]] for c in range(2)])
+
+    w_far = [w_step(0, h, w_held[h]) for h in range(2)]
+    w_held = join(w_held, w_far)
+    w_far = [w_step(1, h, after(w_held[h], *states_p)) for h in range(2)]
+
+    kept, sent = flash(meta, 1, after(q_mine, *states_o), q_other, kv_far, 1, states_p, 5)
     came = core_swap(sent)
-    w_tail = [chip_swap_by_core(after(w_far[h], sent), last[h]) for h in range(2)]
-    kept = flash(meta, q_mine, kv_far, 0, 1, state_mine, 5)
-    head_out = merge(meta, head_lambda, kept, came, head_gain[None])
-    mine_out, pair_out = head_out[0], head_out[1]
+    w_held = join([after(w, sent) for w in w_held], w_far)
+    w_far = [w_step(2, h, w_held[h]) for h in range(2)]
+    w_last1 = w_step(3, 1, w_held[1])
+    pair_out = merge(meta, head_lambda, kept, came, head_gain[None])
     passed = chip_swap(pair_out, STEP["yl"])
-    owns = [mine_out] + [shift_x(mine_out, d) for d in (1, 2, 3)]
-    passes = [passed] + [shift_x(passed, d) for d in (1, 2, 3)]
-
-    weights = [w for pair in zip(w_mines, w_others) for w in pair]
-    normed, middle = middle_call(meta, owns, passes, weights, streams, norm_gain[None])
+    w_last0 = w_step(3, 0, after(w_held[0], pair_out))
+    kept, sent = flash(meta, 0, after(q_mine, pair_out), q_other, kv_far, 1, states_o, 5)
+    came = core_swap(sent)
+    block = merge_last(meta, head_lambda, kept, came, head_gain[None], passed)
+    blocks = [block] + [shift_x(block, d) for d in (1, 2, 3)]
+    w_others = [core_swap(after(w, block)) for w in w_mines[1:]]
+    w_tail = [w_step(3, h, after(w_far[h], block)) for h in range(2)]
+    w_last = [w_last0, w_last1]
+    normed, middle = middle_call(meta, blocks, w_mines, w_others, w_out, norm_gain[None])
     other_normed = core_swap(normed)
     kept_part, sent_part = ffn(
         meta,

time: 214 us -> 211 us (0.986)
  starting transfers between devices: 64.1 us -> 55 us
  Pallas kernels: 42.7 us -> 49.7 us
    ppermute x19 -> x20, waiting for transfers between devices: 19.6 us -> 29.7 us  [chip_swap(): return lax.ppermute(array, 'sp', pairs)]
    ppermute x10, waiting for transfers between devices: 29 us -> 18.9 us  [chip_swap_by_core(): return lax.ppermute(array, 'sp', pairs)]
    ppermute x15 -> x9, starting transfers between devices: 20.9 us -> 14.8 us  [shift_x(): return lax.ppermute(array, 'tp', [(i, (i + d) % 4) for i in range(4)])]
    pallas_call x5 -> x7, Pallas kernels: 24.5 us -> 28.9 us  [the longest x4 22.9 us: flash(): pl.pallas_call(functools.partial(flash_kernel, block, far, scale), grid=(...]
    ppermute x19 -> x20, starting transfers between devices: 27.3 us -> 25.9 us  [chip_swap(): return lax.ppermute(array, 'sp', pairs)]
    ppermute x15 -> x9, waiting for transfers between devices: 51 us -> 49.8 us  [shift_x(): return lax.ppermute(array, 'tp', [(i, (i + d) % 4) for i in range(4)])]
  transfers between devices with their start and end apart: 44 -> 39, of which waited for: 22 -> 20; matrix products, arithmetic and copies ran while one was open for 0% -> 0% of each run, Pallas kernels for 14% -> 15%
where the time goes in v1:
time: 211 us; the launch traced here: 209 us
  waiting for transfers between devices  98.4 us (47%)
  starting transfers between devices  55 us (26%)
  Pallas kernels  49.7 us (24%)
  local copies, waits for them, and re-layouts  3.92 us (2%)
  other arithmetic  2.11 us (1%)
    ppermute x9, waiting for transfers between devices, shift_x(): return lax.ppermute(array, 'tp', [(i, (i + d) % 4) for i in range(4)])  49.8 us
    ppermute x20, waiting for transfers between devices, chip_swap(): return lax.ppermute(array, 'sp', pairs)  29.7 us
    ppermute x20, starting transfers between devices, chip_swap(): return lax.ppermute(array, 'sp', pairs)  25.9 us
    pallas_call x4, Pallas kernels, flash(): pl.pallas_call(functools.partial(flash_kernel, block, far, scale), grid=(...  22.9 us
    ppermute x10, waiting for transfers between devices, chip_swap_by_core(): return lax.ppermute(array, 'sp', pairs)  18.9 us
    ppermute x9, starting transfers between devices, shift_x(): return lax.ppermute(array, 'tp', [(i, (i + d) % 4) for i in range(4)])  14.8 us
    ppermute x10, starting transfers between devices, chip_swap_by_core(): return lax.ppermute(array, 'sp', pairs)  14.3 us
    pallas_call x1, Pallas kernels, ffn(): pl.pallas_call(ffn_kernel, in_specs=[pl.BlockSpec(memory_space=pltpu.SMEM...  9.1 us
  transfers between devices with their start and end apart: 39, of which 20 were waited for; matrix products, arithmetic and copies ran while one was open for 0% of the time, Pallas kernels for 15%

profile of v1, /device:TPU:0, one launch (start us, length us, event | category | flops | bytes accessed | tf_op | source)
XLA Modules:
  0.0 209.4 jit_solution(7459461053703197020)
XLA Ops:
  1.3 2.8 %pack.1 = (bf16[256,768]{1,0:T(8,128)(2,1)}, bf16[256,768]{1,0:T(8,128)(2,1)}) custom-call(s32[86]{0:T(128)} %compare_select_fusion.1.meta.table, bf16[256,512]{1,0:T(8,128)(2,1)} %keys.1, bf16[256,512]{1,0:T(8,128)(2,1)} %values.1, bf16[256,512]{1,0:T(8,128)(2,1)} %queries.1), custom_call_target="tpu_custom_call" | custom-call | flops 1000000000 | bytes 100000 | tf_op jit(solution)/shard_map/pack/pallas_call | solution.py:125
  5.8 9.3 %collective-permute-done.taken = bf16[256,768]{1,0:T(8,128)(2,1)S(1)} collective-permute-done((bf16[256,768]{1,0:T(8,128)(2,1)}, bf16[256,768]{1,0:T(8,128)(2,1)S(1)}, u32[]{:S(2)}, u32[]{:S(2)}) %collective-permute-start) | collective-permute-done | bytes 393248 | tf_op jit(solution)/shard_map/ppermute | solution.py:36
  16.2 2.2 %collective-permute-start.2 = (bf16[1,192,512]{2,1,0:T(8,128)(2,1)S(1)}, bf16[1,192,512]{2,1,0:T(8,128)(2,1)S(1)}, u32[]{:S(2)}, u32[]{:S(2)}) collective-permute-start(bf16[1,192,512]{2,1,0:T(8,128)(2,1)S(1)} %get-tuple-element.55.refs_0_), channel_id=1, source_target_pairs={{0,32},{4,36},{8,40},{12,44},{16,48},{20,52},{24,56},{28,60},{32,0... | collective-permute-start | bytes 589832 | tf_op jit(solution)/shard_map/ppermute | solution.py:36
  18.4 2.5 %collective-permute-start.3 = (bf16[1,160,512]{2,1,0:T(8,128)(2,1)S(1)}, bf16[1,160,512]{2,1,0:T(8,128)(2,1)S(1)}, u32[]{:S(2)}, u32[]{:S(2)}) collective-permute-start(bf16[1,160,512]{2,1,0:T(8,128)(2,1)S(1)} %get-tuple-element.56.refs_1_), channel_id=1, source_target_pairs={{0,96},{4,100},{8,104},{12,108},{16,112},{20,116},{24,120},{28,124... | collective-permute-start | bytes 491528 | tf_op jit(solution)/shard_map/ppermute | solution.py:36
  20.9 3.0 %collective-permute-start.4 = (bf16[1,160,512]{2,1,0:T(8,128)(2,1)S(1)}, bf16[1,160,512]{2,1,0:T(8,128)(2,1)S(1)}, u32[]{:S(2)}, u32[]{:S(2)}) collective-permute-start(bf16[1,160,512]{2,1,0:T(8,128)(2,1)S(1)} %get-tuple-element.57.refs_2_), channel_id=1, source_target_pairs={{0,24},{4,28},{8,16},{12,20},{16,8},{20,12},{24,0},{28,4},{32,56},... | collective-permute-start | bytes 491528 | tf_op jit(solution)/shard_map/ppermute | solution.py:36
  24.9 2.5 %collective-permute-done.4.refs_5_ = bf16[1,160,512]{2,1,0:T(8,128)(2,1)S(1)} collective-permute-done((bf16[1,160,512]{2,1,0:T(8,128)(2,1)S(1)}, bf16[1,160,512]{2,1,0:T(8,128)(2,1)S(1)}, u32[]{:S(2)}, u32[]{:S(2)}) %collective-permute-start.4) | collective-permute-done | bytes 163872 | tf_op jit(solution)/shard_map/ppermute | solution.py:36
  28.3 3.0 %collective-permute-start.6 = (bf16[2,160,512]{2,1,0:T(8,128)(2,1)S(1)}, bf16[2,160,512]{2,1,0:T(8,128)(2,1)S(1)}, u32[]{:S(2)}, u32[]{:S(2)}) collective-permute-start(bf16[2,160,512]{2,1,0:T(8,128)(2,1)S(1)} %get-tuple-element.59.refs_1_), channel_id=1, source_target_pairs={{0,24},{4,28},{8,16},{12,20},{16,8},{20,12},{24,0},{28,4},{32,56},... | collective-permute-start | bytes 983048 | tf_op jit(solution)/shard_map/ppermute | solution.py:36
  31.7 4.9 %collective-permute-done.6.refs_4_ = bf16[2,160,512]{2,1,0:T(8,128)(2,1)S(1)} collective-permute-done((bf16[2,160,512]{2,1,0:T(8,128)(2,1)S(1)}, bf16[2,160,512]{2,1,0:T(8,128)(2,1)S(1)}, u32[]{:S(2)}, u32[]{:S(2)}) %collective-permute-start.6) | collective-permute-done | bytes 327712 | tf_op jit(solution)/shard_map/ppermute | solution.py:36
  40.6 2.3 %collective-permute-start.10 = (bf16[4,160,512]{2,1,0:T(8,128)(2,1)S(1)}, bf16[4,160,512]{2,1,0:T(8,128)(2,1)S(1)}, u32[]{:S(2)}, u32[]{:S(2)}) collective-permute-start(bf16[4,160,512]{2,1,0:T(8,128)(2,1)S(1)} %get-tuple-element.63), channel_id=1, source_target_pairs={{0,96},{4,100},{8,104},{12,108},{16,112},{20,116},{24,120},{28,124... | collective-permute-start | bytes 1966088 | tf_op jit(solution)/shard_map/ppermute | solution.py:36
  42.9 5.0 %flash.4 = (f32[256,640]{1,0:T(8,128)S(1)}, f32[256,640]{1,0:T(8,128)S(1)}) custom-call(s32[86]{0:T(128)S(1)} %copy-done, bf16[512,256]{1,0:T(8,128)(2,1)S(1)} %get-tuple-element.72.refs_0_, bf16[512,256]{1,0:T(8,128)(2,1)S(1)} %collective-permute-done.1.refs_1_, bf16[768,512]{1,0:T(8,128)(2,1)S(1)} %bitcast.11, bf16[640,512]{1,0:T(8,128)(2,1)S(1)} %bitcast.19, ...), custom_call_target="tpu_custom_call" | custom-call | flops 5000000000 | bytes 100000 | tf_op jit(solution)/shard_map/flash/pallas_call | solution.py:316
  47.9 5.0 %flash.5 = (f32[256,640]{1,0:T(8,128)S(1)}, f32[256,640]{1,0:T(8,128)S(1)}) custom-call(s32[86]{0:T(128)S(1)} %copy-done, bf16[512,256]{1,0:T(8,128)(2,1)S(1)} %get-tuple-element.72.refs_0_, bf16[512,256]{1,0:T(8,128)(2,1)S(1)} %collective-permute-done.1.refs_1_, bf16[768,512]{1,0:T(8,128)(2,1)S(1)} %bitcast.12, bf16[640,512]{1,0:T(8,128)(2,1)S(1)} %bitcast.20, ...), custom_call_target="tpu_custom_call" | custom-call | flops 5000000000 | bytes 100000 | tf_op jit(solution)/shard_map/flash/pallas_call | solution.py:316
  55.1 6.9 %flash.6 = (f32[256,640]{1,0:T(8,128)S(1)}, f32[256,640]{1,0:T(8,128)}) custom-call(s32[86]{0:T(128)S(1)} %copy-done, bf16[512,256]{1,0:T(8,128)(2,1)S(1)} %get-tuple-element.72.refs_0_, bf16[512,256]{1,0:T(8,128)(2,1)S(1)} %collective-permute-done.1.refs_1_, bf16[768,512]{1,0:T(8,128)(2,1)S(1)} %bitcast.9, bf16[640,512]{1,0:T(8,128)(2,1)S(1)} %bitcast.13, ...), custom_call_target="tpu_custom_call" | custom-call | flops 5000000000 | bytes 100000 | tf_op jit(solution)/shard_map/flash/pallas_call | solution.py:316
  62.9 2.2 %weights.1 = (bf16[1,64,2176]{2,1,0:T(8,128)(2,1)}, bf16[1,64,2176]{2,1,0:T(8,128)(2,1)}) custom-call(s32[86]{0:T(128)} %compare_select_fusion.1.meta.table, bf16[64,1408]{1,0:T(8,128)(2,1)} %gate.1, bf16[64,1408]{1,0:T(8,128)(2,1)} %up.1, bf16[64,1408]{1,0:T(8,128)(2,1)} %bitcast.24), custom_call_target="tpu_custom_call" | custom-call | flops 2000000000 | bytes 100000 | tf_op jit(solution)/shard_map/weights/pallas_call | solution.py:159
  67.1 3.2 %lines.1.refs_4_ = bf16[320,2048]{1,0:T(8,128)(2,1)} custom-call(s32[86]{0:T(128)} %compare_select_fusion.1.meta.table, bf16[512,2048]{1,0:T(8,128)(2,1)} %refs_11_.1, bf16[64,2048]{1,0:T(8,128)(2,1)} %stream.1), custom_call_target="tpu_custom_call" | custom-call | flops 2000000000 | bytes 100000 | tf_op jit(solution)/shard_map/lines/pallas_call | solution.py:188
  71.9 2.7 %collective-permute-start.18 = (bf16[320,2048]{1,0:T(8,128)(2,1)}, bf16[320,2048]{1,0:T(8,128)(2,1)S(1)}, u32[]{:S(2)}, u32[]{:S(2)}) collective-permute-start(bf16[320,2048]{1,0:T(8,128)(2,1)} %lines.1.refs_4_), channel_id=1, source_target_pairs={{0,2},{1,3},{2,0},{3,1},{4,6},{5,7},{6,4},{7,5},{8,10},{9,11},{10,... | collective-permute-start | bytes 3932168 | tf_op jit(solution)/shard_map/ppermute | solution.py:49
  83.1 6.0 %flash.7 = (f32[256,640]{1,0:T(8,128)S(1)}, f32[256,640]{1,0:T(8,128)S(1)}) custom-call(s32[86]{0:T(128)S(1)} %copy-done.1, bf16[512,256]{1,0:T(8,128)(2,1)S(1)} %copy-done.10, bf16[512,256]{1,0:T(8,128)(2,1)S(1)} %copy-done.12, bf16[768,512]{1,0:T(8,128)(2,1)S(1)} %bitcast.10, bf16[640,512]{1,0:T(8,128)(2,1)S(1)} %bitcast.14, ...), custom_call_target="tpu_custom_call" | custom-call | flops 5000000000 | bytes 100000 | tf_op jit(solution)/shard_map/flash/pallas_call | solution.py:316
  91.4 5.3 %collective-permute-done.13.passed_ref = bf16[256,256]{1,0:T(8,128)(2,1)S(1)} collective-permute-done((bf16[256,256]{1,0:T(8,128)(2,1)S(1)}, bf16[256,256]{1,0:T(8,128)(2,1)S(1)}, u32[]{:S(2)}, u32[]{:S(2)}) %collective-permute-start.13) | collective-permute-done | bytes 131104 | tf_op jit(solution)/shard_map/ppermute | solution.py:36
  101.5 3.1 %collective-permute-start.20 = (bf16[320,2048]{1,0:T(8,128)(2,1)S(1)}, bf16[320,2048]{1,0:T(8,128)(2,1)S(1)}, u32[]{:S(2)}, u32[]{:S(2)}) collective-permute-start(bf16[320,2048]{1,0:T(8,128)(2,1)S(1)} %collective-permute-done.17.refs_5_), channel_id=1, source_target_pairs={{0,4},{4,0},{8,12},{12,8},{16,20},{20,16},{24,28},{28,24},{32,36},... | collective-permute-start | bytes 3932168 | tf_op jit(solution)/shard_map/ppermute | solution.py:36
  104.6 26.0 %collective-permute-done.18.refs_6_ = bf16[320,2048]{1,0:T(8,128)(2,1)S(1)} collective-permute-done((bf16[320,2048]{1,0:T(8,128)(2,1)}, bf16[320,2048]{1,0:T(8,128)(2,1)S(1)}, u32[]{:S(2)}, u32[]{:S(2)}) %collective-permute-start.18) | collective-permute-done | bytes 1310752 | tf_op jit(solution)/shard_map/ppermute | solution.py:49
  134.3 2.3 %collective-permute-start.15 = (bf16[256,512]{1,0:T(8,128)(2,1)S(1)}, bf16[256,512]{1,0:T(8,128)(2,1)S(1)}, u32[]{:S(2)}, u32[]{:S(2)}) collective-permute-start(bf16[256,512]{1,0:T(8,128)(2,1)S(1)} %merge_last.1.refs_0_), channel_id=1, source_target_pairs={{0,2},{1,3},{2,0},{3,1},{4,6},{5,7},{6,4},{7,5},{8,10},{9,11},{10,... | collective-permute-start | bytes 786440 | tf_op jit(solution)/shard_map/ppermute | solution.py:49
  136.6 5.7 %collective-permute-done.14.refs_1_ = bf16[256,512]{1,0:T(8,128)(2,1)S(1)} collective-permute-done((bf16[256,512]{1,0:T(8,128)(2,1)S(1)}, bf16[256,512]{1,0:T(8,128)(2,1)S(1)}, u32[]{:S(2)}, u32[]{:S(2)}) %collective-permute-start.14) | collective-permute-done | bytes 262176 | tf_op jit(solution)/shard_map/ppermute | solution.py:49
  144.3 4.5 %collective-permute-done.15.refs_2_ = bf16[256,512]{1,0:T(8,128)(2,1)S(1)} collective-permute-done((bf16[256,512]{1,0:T(8,128)(2,1)S(1)}, bf16[256,512]{1,0:T(8,128)(2,1)S(1)}, u32[]{:S(2)}, u32[]{:S(2)}) %collective-permute-start.15) | collective-permute-done | bytes 262176 | tf_op jit(solution)/shard_map/ppermute | solution.py:49
  148.8 2.9 %collective-permute-start.33 = (bf16[4,64,2176]{2,1,0:T(8,128)(2,1)S(1)}, bf16[4,64,2176]{2,1,0:T(8,128)(2,1)S(1)}, u32[]{:S(2)}, u32[]{:S(2)}) collective-permute-start(bf16[4,64,2176]{2,1,0:T(8,128)(2,1)S(1)} %get-tuple-element.90.refs_4_), channel_id=1, source_target_pairs={{0,96},{4,36},{8,104},{12,44},{16,112},{20,52},{24,120},{28,60},{3... | collective-permute-start | bytes 3342344 | tf_op jit(solution)/shard_map/ppermute | solution.py:41
  156.2 4.9 %middle.1 = (bf16[256,2048]{1,0:T(8,128)(2,1)S(1)}, f32[64,2048]{1,0:T(8,128)S(1)}) custom-call(s32[86]{0:T(128)S(1)} %copy-done.1, bf16[256,512]{1,0:T(8,128)(2,1)S(1)} %merge_last.1.refs_0_, bf16[256,512]{1,0:T(8,128)(2,1)S(1)} %collective-permute-done.14.refs_1_, bf16[256,512]{1,0:T(8,128)(2,1)S(1)} %collective-permute-done.15.refs_2_, ...), custom_call_target="tpu_custom_call" | custom-call | flops 4000000000 | bytes 100000 | tf_op jit(solution)/shard_map/middle/pallas_call | solution.py:424
  161.4 4.0 %collective-permute-done.33.refs_6_ = bf16[4,64,2176]{2,1,0:T(8,128)(2,1)S(1)} collective-permute-done((bf16[4,64,2176]{2,1,0:T(8,128)(2,1)S(1)}, bf16[4,64,2176]{2,1,0:T(8,128)(2,1)S(1)}, u32[]{:S(2)}, u32[]{:S(2)}) %collective-permute-start.33) | collective-permute-done | bytes 1114144 | tf_op jit(solution)/shard_map/ppermute | solution.py:41
  165.5 2.9 %collective-permute-done.30.refs_2_ = bf16[4,64,2176]{2,1,0:T(8,128)(2,1)S(1)} collective-permute-done((bf16[4,64,2176]{2,1,0:T(8,128)(2,1)S(1)}, bf16[4,64,2176]{2,1,0:T(8,128)(2,1)S(1)}, u32[]{:S(2)}, u32[]{:S(2)}) %collective-permute-start.30) | collective-permute-done | bytes 1114144 | tf_op jit(solution)/shard_map/ppermute | solution.py:41
  168.4 11.9 %collective-permute-done.31.refs_3_ = bf16[4,64,2176]{2,1,0:T(8,128)(2,1)S(1)} collective-permute-done((bf16[4,64,2176]{2,1,0:T(8,128)(2,1)S(1)}, bf16[4,64,2176]{2,1,0:T(8,128)(2,1)S(1)}, u32[]{:S(2)}, u32[]{:S(2)}) %collective-permute-start.31) | collective-permute-done | bytes 1114144 | tf_op jit(solution)/shard_map/ppermute | solution.py:41
  180.3 9.1 %ffn.1 = (f32[256,2048]{1,0:T(8,128)S(1)}, bf16[256,2048]{1,0:T(8,128)(2,1)S(1)}) custom-call(s32[86]{0:T(128)S(1)} %copy-done.1, bf16[256,2048]{1,0:T(8,128)(2,1)S(1)} %get-tuple-element.78.mine_ref, bf16[256,2048]{1,0:T(8,128)(2,1)S(1)} %collective-permute-done.23.other_ref, bf16[4,64,2176]{2,1,0:T(8,128)(2,1)S(1)} %get-tuple-element.88.refs_0_, ...), custom_call_target="tpu_custom_call" | custom-call | flops 8999999488 | bytes 100000 | tf_op jit(solution)/shard_map/ffn/pallas_call | solution.py:496
  189.5 2.6 %collective-permute-done.35.came_ref = bf16[256,2048]{1,0:T(8,128)(2,1)S(1)} collective-permute-done((bf16[256,2048]{1,0:T(8,128)(2,1)S(1)}, bf16[256,2048]{1,0:T(8,128)(2,1)S(1)}, u32[]{:S(2)}, u32[]{:S(2)}) %collective-permute-start.35) | collective-permute-done | bytes 1048608 | tf_op jit(solution)/shard_map/ppermute | solution.py:36
  195.2 6.4 %collective-permute-done.38 = bf16[64,2048]{1,0:T(8,128)(2,1)S(1)} collective-permute-done((bf16[64,2048]{1,0:T(8,128)(2,1)S(1)}, bf16[64,2048]{1,0:T(8,128)(2,1)S(1)}, u32[]{:S(2)}, u32[]{:S(2)}) %collective-permute-start.38) | collective-permute-done | bytes 262176 | tf_op jit(solution)/shard_map/ppermute | solution.py:49
  201.6 2.5 %collective-permute-done.37 = bf16[64,2048]{1,0:T(8,128)(2,1)S(1)} collective-permute-done((bf16[64,2048]{1,0:T(8,128)(2,1)S(1)}, bf16[64,2048]{1,0:T(8,128)(2,1)S(1)}, u32[]{:S(2)}, u32[]{:S(2)}) %collective-permute-start.37) | collective-permute-done | bytes 262176 | tf_op jit(solution)/shard_map/ppermute | solution.py:49
  204.2 4.5 %collective-permute-done.36 = bf16[64,2048]{1,0:T(8,128)(2,1)S(1)} collective-permute-done((bf16[64,2048]{1,0:T(8,128)(2,1)S(1)}, bf16[64,2048]{1,0:T(8,128)(2,1)S(1)}, u32[]{:S(2)}, u32[]{:S(2)}) %collective-permute-start.36) | collective-permute-done | bytes 262176 | tf_op jit(solution)/shard_map/ppermute | solution.py:49
  (111 shorter events, 46.9 us)
Async XLA Ops:
  4.0 11.1 %collective-permute-start = (bf16[256,768]{1,0:T(8,128)(2,1)}, bf16[256,768]{1,0:T(8,128)(2,1)S(1)}, u32[]{:S(2)}, u32[]{:S(2)}) collective-permute-start(bf16[256,768]{1,0:T(8,128)(2,1)} %get-tuple-element.53), channel_id=1, source_target_pairs={{0,8},{4,12},{8,0},{12,4},{16,24},{20,28},{24,16},{28,20},{32,40},... | collective-permute-start | bytes 1179656 | tf_op jit(solution)/shard_map/ppermute | solution.py:36
  16.2 11.2 %collective-permute-start.2 = (bf16[1,192,512]{2,1,0:T(8,128)(2,1)S(1)}, bf16[1,192,512]{2,1,0:T(8,128)(2,1)S(1)}, u32[]{:S(2)}, u32[]{:S(2)}) collective-permute-start(bf16[1,192,512]{2,1,0:T(8,128)(2,1)S(1)} %get-tuple-element.55.refs_0_), channel_id=1, source_target_pairs={{0,32},{4,36},{8,40},{12,44},{16,48},{20,52},{24,56},{28,60},{32,0... | collective-permute-start | bytes 589832 | tf_op jit(solution)/shard_map/ppermute | solution.py:36
  27.5 10.9 %collective-permute-start.5 = (bf16[2,192,512]{2,1,0:T(8,128)(2,1)S(1)}, bf16[2,192,512]{2,1,0:T(8,128)(2,1)S(1)}, u32[]{:S(2)}, u32[]{:S(2)}) collective-permute-start(bf16[2,192,512]{2,1,0:T(8,128)(2,1)S(1)} %get-tuple-element.58.refs_0_), channel_id=1, source_target_pairs={{0,96},{4,100},{8,104},{12,108},{16,112},{20,116},{24,120},{28,124... | collective-permute-start | bytes 1179656 | tf_op jit(solution)/shard_map/ppermute | solution.py:36
  31.7 11.2 %collective-permute-start.1 = (bf16[512,256]{1,0:T(8,128)(2,1)S(1)}, bf16[512,256]{1,0:T(8,128)(2,1)S(1)}, u32[]{:S(2)}, u32[]{:S(2)}) collective-permute-start(bf16[512,256]{1,0:T(8,128)(2,1)S(1)} %get-tuple-element.72.refs_0_), channel_id=1, source_target_pairs={{0,4},{4,0},{8,12},{12,8},{16,20},{20,16},{24,28},{28,24},{32,36},... | collective-permute-start | bytes 786440 | tf_op jit(solution)/shard_map/ppermute | solution.py:36
  38.5 16.6 %collective-permute-start.8 = (bf16[4,192,512]{2,1,0:T(8,128)(2,1)S(1)}, bf16[4,192,512]{2,1,0:T(8,128)(2,1)S(1)}, u32[]{:S(2)}, u32[]{:S(2)}) collective-permute-start(bf16[4,192,512]{2,1,0:T(8,128)(2,1)S(1)} %get-tuple-element.61), channel_id=1, source_target_pairs={{0,24},{4,28},{8,16},{12,20},{16,8},{20,12},{24,0},{28,4},{32,56},... | collective-permute-start | bytes 2359304 | tf_op jit(solution)/shard_map/ppermute | solution.py:36
  40.6 13.2 %collective-permute-start.9 = (bf16[4,160,512]{2,1,0:T(8,128)(2,1)S(1)}, bf16[4,160,512]{2,1,0:T(8,128)(2,1)S(1)}, u32[]{:S(2)}, u32[]{:S(2)}) collective-permute-start(bf16[4,160,512]{2,1,0:T(8,128)(2,1)S(1)} %get-tuple-element.62), channel_id=1, source_target_pairs={{0,32},{4,36},{8,40},{12,44},{16,48},{20,52},{24,56},{28,60},{32,0... | collective-permute-start | bytes 1966088 | tf_op jit(solution)/shard_map/ppermute | solution.py:36
  40.6 14.3 %collective-permute-start.10 = (bf16[4,160,512]{2,1,0:T(8,128)(2,1)S(1)}, bf16[4,160,512]{2,1,0:T(8,128)(2,1)S(1)}, u32[]{:S(2)}, u32[]{:S(2)}) collective-permute-start(bf16[4,160,512]{2,1,0:T(8,128)(2,1)S(1)} %get-tuple-element.63), channel_id=1, source_target_pairs={{0,96},{4,100},{8,104},{12,108},{16,112},{20,116},{24,120},{28,124... | collective-permute-start | bytes 1966088 | tf_op jit(solution)/shard_map/ppermute | solution.py:36
  62.9 17.5 %collective-permute-start.11 = (f32[256,640]{1,0:T(8,128)}, f32[256,640]{1,0:T(8,128)}, u32[]{:S(2)}, u32[]{:S(2)}) collective-permute-start(f32[256,640]{1,0:T(8,128)} %get-tuple-element.71), channel_id=1, source_target_pairs={{0,4},{4,0},{8,12},{12,8},{16,20},{20,16},{24,28},{28,24},{32,36},... | collective-permute-start | bytes 1966088 | tf_op jit(solution)/shard_map/ppermute | solution.py:36
  65.6 9.0 %collective-permute-start.25 = (bf16[1,64,2176]{2,1,0:T(8,128)(2,1)}, bf16[1,64,2176]{2,1,0:T(8,128)(2,1)}, u32[]{:S(2)}, u32[]{:S(2)}) collective-permute-start(bf16[1,64,2176]{2,1,0:T(8,128)(2,1)} %get-tuple-element.79.refs_0_), channel_id=1, source_target_pairs={{0,32},{4,100},{8,40},{12,108},{16,48},{20,116},{24,56},{28,124},{... | collective-permute-start | bytes 835592 | tf_op jit(solution)/shard_map/ppermute | solution.py:41
  67.1 8.9 %collective-permute-start.26 = (bf16[1,64,2176]{2,1,0:T(8,128)(2,1)}, bf16[1,64,2176]{2,1,0:T(8,128)(2,1)}, u32[]{:S(2)}, u32[]{:S(2)}) collective-permute-start(bf16[1,64,2176]{2,1,0:T(8,128)(2,1)} %collective-permute-done.24.refs_1_), channel_id=1, source_target_pairs={{0,8},{4,28},{8,0},{12,20},{16,24},{20,12},{24,16},{28,4},{32,40},... | collective-permute-start | bytes 835592 | tf_op jit(solution)/shard_map/ppermute | solution.py:41
  70.3 31.2 %collective-permute-start.17 = (bf16[320,2048]{1,0:T(8,128)(2,1)}, bf16[320,2048]{1,0:T(8,128)(2,1)S(1)}, u32[]{:S(2)}, u32[]{:S(2)}) collective-permute-start(bf16[320,2048]{1,0:T(8,128)(2,1)} %lines.1.refs_4_), channel_id=1, source_target_pairs={{0,1},{1,2},{2,3},{3,0},{4,5},{5,6},{6,7},{7,4},{8,9},{9,10},{10,1... | collective-permute-start | bytes 3932168 | tf_op jit(solution)/shard_map/ppermute | solution.py:49
  71.9 58.7 %collective-permute-start.18 = (bf16[320,2048]{1,0:T(8,128)(2,1)}, bf16[320,2048]{1,0:T(8,128)(2,1)S(1)}, u32[]{:S(2)}, u32[]{:S(2)}) collective-permute-start(bf16[320,2048]{1,0:T(8,128)(2,1)} %lines.1.refs_4_), channel_id=1, source_target_pairs={{0,2},{1,3},{2,0},{3,1},{4,6},{5,7},{6,4},{7,5},{8,10},{9,11},{10,... | collective-permute-start | bytes 3932168 | tf_op jit(solution)/shard_map/ppermute | solution.py:49
  74.6 57.7 %collective-permute-start.19 = (bf16[320,2048]{1,0:T(8,128)(2,1)}, bf16[320,2048]{1,0:T(8,128)(2,1)S(1)}, u32[]{:S(2)}, u32[]{:S(2)}) collective-permute-start(bf16[320,2048]{1,0:T(8,128)(2,1)} %lines.1.refs_4_), channel_id=1, source_target_pairs={{0,3},{1,0},{2,1},{3,2},{4,7},{5,4},{6,5},{7,6},{8,11},{9,8},{10,9... | collective-permute-start | bytes 3932168 | tf_op jit(solution)/shard_map/ppermute | solution.py:49
  78.3 10.8 %collective-permute-start.27 = (bf16[2,64,2176]{2,1,0:T(8,128)(2,1)S(1)}, bf16[2,64,2176]{2,1,0:T(8,128)(2,1)S(1)}, u32[]{:S(2)}, u32[]{:S(2)}) collective-permute-start(bf16[2,64,2176]{2,1,0:T(8,128)(2,1)S(1)} %get-tuple-element.85.refs_0_), channel_id=1, source_target_pairs={{0,8},{4,28},{8,0},{12,20},{16,24},{20,12},{24,16},{28,4},{32,40},... | collective-permute-start | bytes 1671176 | tf_op jit(solution)/shard_map/ppermute | solution.py:41
  80.4 10.8 %collective-permute-start.28 = (bf16[2,64,2176]{2,1,0:T(8,128)(2,1)S(1)}, bf16[2,64,2176]{2,1,0:T(8,128)(2,1)S(1)}, u32[]{:S(2)}, u32[]{:S(2)}) collective-permute-start(bf16[2,64,2176]{2,1,0:T(8,128)(2,1)S(1)} %get-tuple-element.86.refs_1_), channel_id=1, source_target_pairs={{0,32},{4,100},{8,40},{12,108},{16,48},{20,116},{24,56},{28,124},{... | collective-permute-start | bytes 1671176 | tf_op jit(solution)/shard_map/ppermute | solution.py:41
  89.1 9.6 %collective-permute-start.12 = (f32[256,640]{1,0:T(8,128)S(1)}, f32[256,640]{1,0:T(8,128)S(1)}, u32[]{:S(2)}, u32[]{:S(2)}) collective-permute-start(f32[256,640]{1,0:T(8,128)S(1)} %get-tuple-element.74), channel_id=1, source_target_pairs={{0,4},{4,0},{8,12},{12,8},{16,20},{20,16},{24,28},{28,24},{32,36},... | collective-permute-start | bytes 1966088 | tf_op jit(solution)/shard_map/ppermute | solution.py:36
  96.7 35.6 %collective-permute-start.29 = (bf16[4,64,2176]{2,1,0:T(8,128)(2,1)S(1)}, bf16[4,64,2176]{2,1,0:T(8,128)(2,1)S(1)}, u32[]{:S(2)}, u32[]{:S(2)}) collective-permute-start(bf16[4,64,2176]{2,1,0:T(8,128)(2,1)S(1)} %get-tuple-element.88.refs_0_), channel_id=1, source_target_pairs={{0,96},{4,36},{8,104},{12,44},{16,112},{20,52},{24,120},{28,60},{3... | collective-permute-start | bytes 3342344 | tf_op jit(solution)/shard_map/ppermute | solution.py:41
  98.7 35.6 %collective-permute-start.32 = (bf16[4,64,2176]{2,1,0:T(8,128)(2,1)S(1)}, bf16[4,64,2176]{2,1,0:T(8,128)(2,1)S(1)}, u32[]{:S(2)}, u32[]{:S(2)}) collective-permute-start(bf16[4,64,2176]{2,1,0:T(8,128)(2,1)S(1)} %get-tuple-element.90.refs_4_), channel_id=1, source_target_pairs={{0,24},{4,12},{8,16},{12,4},{16,8},{20,28},{24,0},{28,20},{32,56},... | collective-permute-start | bytes 3342344 | tf_op jit(solution)/shard_map/ppermute | solution.py:41
  101.5 51.7 %collective-permute-start.20 = (bf16[320,2048]{1,0:T(8,128)(2,1)S(1)}, bf16[320,2048]{1,0:T(8,128)(2,1)S(1)}, u32[]{:S(2)}, u32[]{:S(2)}) collective-permute-start(bf16[320,2048]{1,0:T(8,128)(2,1)S(1)} %collective-permute-done.17.refs_5_), channel_id=1, source_target_pairs={{0,4},{4,0},{8,12},{12,8},{16,20},{20,16},{24,28},{28,24},{32,36},... | collective-permute-start | bytes 3932168 | tf_op jit(solution)/shard_map/ppermute | solution.py:36
  130.6 24.4 %collective-permute-start.21 = (bf16[320,2048]{1,0:T(8,128)(2,1)S(1)}, bf16[320,2048]{1,0:T(8,128)(2,1)S(1)}, u32[]{:S(2)}, u32[]{:S(2)}) collective-permute-start(bf16[320,2048]{1,0:T(8,128)(2,1)S(1)} %collective-permute-done.18.refs_6_), channel_id=1, source_target_pairs={{0,4},{4,0},{8,12},{12,8},{16,20},{20,16},{24,28},{28,24},{32,36},... | collective-permute-start | bytes 3932168 | tf_op jit(solution)/shard_map/ppermute | solution.py:36
  132.4 23.8 %collective-permute-start.22 = (bf16[320,2048]{1,0:T(8,128)(2,1)S(1)}, bf16[320,2048]{1,0:T(8,128)(2,1)S(1)}, u32[]{:S(2)}, u32[]{:S(2)}) collective-permute-start(bf16[320,2048]{1,0:T(8,128)(2,1)S(1)} %collective-permute-done.19.refs_7_), channel_id=1, source_target_pairs={{0,4},{4,0},{8,12},{12,8},{16,20},{20,16},{24,28},{28,24},{32,36},... | collective-permute-start | bytes 3932168 | tf_op jit(solution)/shard_map/ppermute | solution.py:36
  132.4 9.9 %collective-permute-start.14 = (bf16[256,512]{1,0:T(8,128)(2,1)S(1)}, bf16[256,512]{1,0:T(8,128)(2,1)S(1)}, u32[]{:S(2)}, u32[]{:S(2)}) collective-permute-start(bf16[256,512]{1,0:T(8,128)(2,1)S(1)} %merge_last.1.refs_0_), channel_id=1, source_target_pairs={{0,1},{1,2},{2,3},{3,0},{4,5},{5,6},{6,7},{7,4},{8,9},{9,10},{10,1... | collective-permute-start | bytes 786440 | tf_op jit(solution)/shard_map/ppermute | solution.py:49
  134.3 14.5 %collective-permute-start.15 = (bf16[256,512]{1,0:T(8,128)(2,1)S(1)}, bf16[256,512]{1,0:T(8,128)(2,1)S(1)}, u32[]{:S(2)}, u32[]{:S(2)}) collective-permute-start(bf16[256,512]{1,0:T(8,128)(2,1)S(1)} %merge_last.1.refs_0_), channel_id=1, source_target_pairs={{0,2},{1,3},{2,0},{3,1},{4,6},{5,7},{6,4},{7,5},{8,10},{9,11},{10,... | collective-permute-start | bytes 786440 | tf_op jit(solution)/shard_map/ppermute | solution.py:49
  142.3 9.4 %collective-permute-start.16 = (bf16[256,512]{1,0:T(8,128)(2,1)S(1)}, bf16[256,512]{1,0:T(8,128)(2,1)S(1)}, u32[]{:S(2)}, u32[]{:S(2)}) collective-permute-start(bf16[256,512]{1,0:T(8,128)(2,1)S(1)} %merge_last.1.refs_0_), channel_id=1, source_target_pairs={{0,3},{1,0},{2,1},{3,2},{4,7},{5,4},{6,5},{7,6},{8,11},{9,8},{10,9... | collective-permute-start | bytes 786440 | tf_op jit(solution)/shard_map/ppermute | solution.py:49
  148.8 16.7 %collective-permute-start.33 = (bf16[4,64,2176]{2,1,0:T(8,128)(2,1)S(1)}, bf16[4,64,2176]{2,1,0:T(8,128)(2,1)S(1)}, u32[]{:S(2)}, u32[]{:S(2)}) collective-permute-start(bf16[4,64,2176]{2,1,0:T(8,128)(2,1)S(1)} %get-tuple-element.90.refs_4_), channel_id=1, source_target_pairs={{0,96},{4,36},{8,104},{12,44},{16,112},{20,52},{24,120},{28,60},{3... | collective-permute-start | bytes 3342344 | tf_op jit(solution)/shard_map/ppermute | solution.py:41
  151.7 16.7 %collective-permute-start.30 = (bf16[4,64,2176]{2,1,0:T(8,128)(2,1)S(1)}, bf16[4,64,2176]{2,1,0:T(8,128)(2,1)S(1)}, u32[]{:S(2)}, u32[]{:S(2)}) collective-permute-start(bf16[4,64,2176]{2,1,0:T(8,128)(2,1)S(1)} %get-tuple-element.88.refs_0_), channel_id=1, source_target_pairs={{0,24},{4,12},{8,16},{12,4},{16,8},{20,28},{24,0},{28,20},{32,56},... | collective-permute-start | bytes 3342344 | tf_op jit(solution)/shard_map/ppermute | solution.py:41
  153.2 27.2 %collective-permute-start.31 = (bf16[4,64,2176]{2,1,0:T(8,128)(2,1)S(1)}, bf16[4,64,2176]{2,1,0:T(8,128)(2,1)S(1)}, u32[]{:S(2)}, u32[]{:S(2)}) collective-permute-start(bf16[4,64,2176]{2,1,0:T(8,128)(2,1)S(1)} %collective-permute-done.29.refs_1_), channel_id=1, source_target_pairs={{0,24},{4,12},{8,16},{12,4},{16,8},{20,28},{24,0},{28,20},{32,56},... | collective-permute-start | bytes 3342344 | tf_op jit(solution)/shard_map/ppermute | solution.py:41
  154.9 25.4 %collective-permute-start.34 = (bf16[4,64,2176]{2,1,0:T(8,128)(2,1)S(1)}, bf16[4,64,2176]{2,1,0:T(8,128)(2,1)S(1)}, u32[]{:S(2)}, u32[]{:S(2)}) collective-permute-start(bf16[4,64,2176]{2,1,0:T(8,128)(2,1)S(1)} %collective-permute-done.32.refs_5_), channel_id=1, source_target_pairs={{0,96},{4,36},{8,104},{12,44},{16,112},{20,52},{24,120},{28,60},{3... | collective-permute-start | bytes 3342344 | tf_op jit(solution)/shard_map/ppermute | solution.py:41
  161.1 19.2 %collective-permute-start.23 = (bf16[256,2048]{1,0:T(8,128)(2,1)S(1)}, bf16[256,2048]{1,0:T(8,128)(2,1)S(1)}, u32[]{:S(2)}, u32[]{:S(2)}) collective-permute-start(bf16[256,2048]{1,0:T(8,128)(2,1)S(1)} %get-tuple-element.78.mine_ref), channel_id=1, source_target_pairs={{0,4},{4,0},{8,12},{12,8},{16,20},{20,16},{24,28},{28,24},{32,36},... | collective-permute-start | bytes 3145736 | tf_op jit(solution)/shard_map/ppermute | solution.py:36
  192.4 9.2 %collective-permute-start.38 = (bf16[64,2048]{1,0:T(8,128)(2,1)S(1)}, bf16[64,2048]{1,0:T(8,128)(2,1)S(1)}, u32[]{:S(2)}, u32[]{:S(2)}) collective-permute-start(bf16[64,2048]{1,0:T(8,128)(2,1)S(1)} %get-tuple-element.98), channel_id=1, source_target_pairs={{0,3},{1,0},{2,1},{3,2},{4,7},{5,4},{6,5},{7,6},{8,11},{9,8},{10,9... | collective-permute-start | bytes 786440 | tf_op jit(solution)/shard_map/ppermute | solution.py:49
  193.4 10.7 %collective-permute-start.37 = (bf16[64,2048]{1,0:T(8,128)(2,1)S(1)}, bf16[64,2048]{1,0:T(8,128)(2,1)S(1)}, u32[]{:S(2)}, u32[]{:S(2)}) collective-permute-start(bf16[64,2048]{1,0:T(8,128)(2,1)S(1)} %get-tuple-element.97), channel_id=1, source_target_pairs={{0,2},{1,3},{2,0},{3,1},{4,6},{5,7},{6,4},{7,5},{8,10},{9,11},{10,... | collective-permute-start | bytes 786440 | tf_op jit(solution)/shard_map/ppermute | solution.py:49
  193.9 14.7 %collective-permute-start.36 = (bf16[64,2048]{1,0:T(8,128)(2,1)S(1)}, bf16[64,2048]{1,0:T(8,128)(2,1)S(1)}, u32[]{:S(2)}, u32[]{:S(2)}) collective-permute-start(bf16[64,2048]{1,0:T(8,128)(2,1)S(1)} %get-tuple-element.96), channel_id=1, source_target_pairs={{0,1},{1,2},{2,3},{3,0},{4,5},{5,6},{6,7},{7,4},{8,9},{9,10},{10,1... | collective-permute-start | bytes 786440 | tf_op jit(solution)/shard_map/ppermute | solution.py:49
  (30 other events, 350.0 us)

commit v2 on v1

--- a/solution.py
+++ b/solution.py
@@ -94,8 +94,9 @@
     return pltpu.CompilerParams(vmem_limit_bytes=mib << 20, **kw)
 
 
-def pack_kernel(meta, keys, values, queries, own_ref, given_ref, ins, outs, sem):
-    second, x = meta[0], meta[1]
+def pack_kernel(keys, values, queries, own_ref, given_ref, ins, outs, sem):
+    y, x = lax.rem(lax.axis_index("sp") // 2, 4), lax.axis_index("tp")
+    second = jnp.where((y == 1) | (y == 2), 1, 0)
     loads = [
         pltpu.make_async_copy(ref, ins.at[k], sem.at[k])
         for k, ref in enumerate((keys, values, queries))
@@ -120,11 +121,11 @@
         store.wait()
 
 
-def pack(meta, keys, values, queries):
+def pack(keys, values, queries):
     in_hbm = pl.BlockSpec(memory_space=pltpu.HBM)
     return pl.pallas_call(
         pack_kernel,
-        in_specs=[pl.BlockSpec(memory_space=pltpu.SMEM)] + [in_hbm] * 3,
+        in_specs=[in_hbm] * 3,
         out_specs=[in_hbm] * 2,
         out_shape=[jax.ShapeDtypeStruct((256, 768), BF16)] * 2,
         scratch_shapes=[
@@ -135,7 +136,7 @@
         compiler_params=vmem_params(63),
         cost_estimate=cost(1),
         name="pack",
-    )(meta, keys, values, queries)
+    )(keys, values, queries)
 
 
 def weights_kernel(meta, gate, up, down, own_ref, given_ref):
@@ -241,25 +242,26 @@
     )(*held, *far)
 
 
-def flash_kernel(block, far, scale, meta, *refs):
+def flash_first_kernel(block, scale, meta, *refs):
     kv_refs, rest = refs[2:5], refs[5:]
-    step = pl.program_id(0)
-    row = lax.broadcasted_iota(jnp.int32, (256, 1), 0)
+    row = lax.broadcasted_iota(jnp.int32, (512, 1), 0)
     qpos = (
-        meta[META_Q + block + 2 * step] + ((meta[1] + (row >> 6)) & 3) * 64 + (row & 63)
+        jnp.where(row < 256, meta[META_Q + block], meta[META_Q + block + 2])
+        + ((meta[1] + (row >> 6)) & 3) * 64
+        + (row & 63)
     )
-    queries = jnp.where(step == 0, refs[0][...], refs[1][...])
+    queries = jnp.concatenate([refs[0][...], refs[1][...]], axis=0)
     state = []
     for _ in range(2):
         state.append(
-            (jnp.full((256, 1), NEG, F32), jnp.zeros((256, 1), F32), jnp.zeros((256, 256), F32))
+            (jnp.full((512, 1), NEG, F32), jnp.zeros((512, 1), F32), jnp.zeros((512, 256), F32))
         )
     for t in range(3):
         kv_ref, half = kv_refs[t], KV_ROWS[t] // 2
         key = lax.broadcasted_iota(jnp.int32, (1, 8 * half), 1)
         kpos = key
         for k in range(8):
-            base = meta[META_K + 24 * far + 8 * t + k]
+            base = meta[META_K + 8 * t + k]
             kpos = jnp.where(key >= k * half, base + key - k * half, kpos)
         visible = kpos <= qpos
         for s in range(2):
@@ -280,42 +282,85 @@
             )
             state[s] = (new_top, total, acc)
     lane = lax.broadcasted_iota(jnp.int32, (256, 128), 1)
-    tail = jnp.zeros((256, 128), F32)
-    for s in range(2):
-        tail = jnp.where(lane == s, state[s][0], tail)
-        tail = jnp.where(lane == 2 + s, state[s][1], tail)
+    for k in range(2):
+        out_ref = rest[k - 2]
+        rows = slice(256 * k, 256 * k + 256)
+        tail = jnp.zeros((256, 128), F32)
+        for s in range(2):
+            top, total, acc = (part[rows] for part in state[s])
+            cols = slice(256 * s, 256 * s + 256)
+            out_ref[:, cols] = acc
+            tail = jnp.where(lane == s, top, tail)
+            tail = jnp.where(lane == 2 + s, total, tail)
+        out_ref[:, 512:640] = tail
+
+
+def flash_last_kernel(block, scale, meta, *refs):
+    kv_refs, rest = refs[2:5], refs[5:]
+    step = pl.program_id(0)
+    row = lax.broadcasted_iota(jnp.int32, (256, 1), 0)
+    qpos = (
+        meta[META_Q + block + 2 * step] + ((meta[1] + (row >> 6)) & 3) * 64 + (row & 63)
+    )
+    queries = jnp.where(step == 0, refs[0][...], refs[1][...])
+    state = []
+    for _ in range(2):
+        state.append(
+            (jnp.full((256, 1), NEG, F32), jnp.zeros((256, 1), F32), jnp.zeros((256, 256), F32))
+        )
+    for t in range(3):
+        kv_ref, half = kv_refs[t], KV_ROWS[t] // 2
+        key = lax.broadcasted_iota(jnp.int32, (1, 8 * half), 1)
+        kpos = key
+        for k in range(8):
+            base = meta[META_K + 24 + 8 * t + k]
+            kpos = jnp.where(key >= k * half, base + key - k * half, kpos)
+        visible = kpos <= qpos
+        for s in range(2):
+            top, total, acc = state[s]
+            scores = lax.dot_general(
+                queries[:, 128 * s : 128 * s + 128],
+                kv_ref[:, 128 * s : 128 * s + 128],
+                (((1,), (1,)), ((), ())),
+                preferred_element_type=F32,
+            )
+            scores = jnp.where(visible, scores, NEG)
+            new_top = jnp.maximum(top, jnp.max(scores, axis=1, keepdims=True))
+            weights = jnp.exp2((scores - new_top) * scale)
+            fade = jnp.exp2((top - new_top) * scale)
+            total = total * fade + jnp.sum(weights, axis=1, keepdims=True)
+            acc = acc * fade + jnp.dot(
+                weights.astype(BF16), kv_ref[:, 256:512], preferred_element_type=F32
+            )
+            state[s] = (new_top, total, acc)
+    lane = lax.broadcasted_iota(jnp.int32, (256, 128), 1)
     for k in range(2):
 
         @pl.when(step == k)
         def _():
             out_ref = rest[k - 2]
-            if not far:
-                for s in range(2):
-                    out_ref[:, 256 * s : 256 * s + 256] = state[s][2]
-                out_ref[:, 512:640] = tail
-            else:
-                near = rest[k]
-                ends = jnp.zeros((256, 128), F32)
-                for s in range(2):
-                    top, total, acc = state[s]
-                    near_top = near[:, 512 + s : 513 + s]
-                    both_top = jnp.maximum(top, near_top)
-                    fade = jnp.exp2((top - both_top) * scale)
-                    near_fade = jnp.exp2((near_top - both_top) * scale)
-                    total = total * fade + near[:, 514 + s : 515 + s] * near_fade
-                    cols = slice(256 * s, 256 * s + 256)
-                    out_ref[:, cols] = acc * fade + near[:, cols] * near_fade
-                    ends = jnp.where(lane == s, both_top, ends)
-                    ends = jnp.where(lane == 2 + s, total, ends)
-                out_ref[:, 512:640] = ends
-
-
-def flash(meta, block, q_mine, q_other, kvs, far, states, us):
+            near = rest[k]
+            ends = jnp.zeros((256, 128), F32)
+            for s in range(2):
+                top, total, acc = state[s]
+                near_top = near[:, 512 + s : 513 + s]
+                both_top = jnp.maximum(top, near_top)
+                fade = jnp.exp2((top - both_top) * scale)
+                near_fade = jnp.exp2((near_top - both_top) * scale)
+                total = total * fade + near[:, 514 + s : 515 + s] * near_fade
+                cols = slice(256 * s, 256 * s + 256)
+                out_ref[:, cols] = acc * fade + near[:, cols] * near_fade
+                ends = jnp.where(lane == s, both_top, ends)
+                ends = jnp.where(lane == 2 + s, total, ends)
+            out_ref[:, 512:640] = ends
+
+
+def flash(meta, block, q_mine, q_other, kvs, states, us):
     scale = float(128**-0.5 * np.log2(np.e))
     kvs = [a.reshape(-1, 512) for a in kvs]
     return pl.pallas_call(
-        functools.partial(flash_kernel, block, far, scale),
-        grid=(2,),
+        functools.partial(flash_last_kernel if states else flash_first_kernel, block, scale),
+        grid=(2,) if states else (1,),
         in_specs=[pl.BlockSpec(memory_space=pltpu.SMEM)]
         + [pl.BlockSpec((256, 256), lambda i: (block, 0))] * 2
         + [whole(a.shape) for a in kvs]
@@ -544,7 +589,7 @@
     head = second.astype(jnp.int32)
 
     meta = meta_table(head, x, chip, core)
-    own, given = pack(meta, keys, values, queries)
+    own, given = pack(keys, values, queries)
     *kv_held, q_mine = thirds(own, chip_swap(given, STEP["yl"]))
     q_other = core_swap(q_mine)
 
@@ -557,8 +602,8 @@
         kv_far = [chip_swap(kv_held[t], STEP[KV_ORDERS[t][s]]) for t in range(3)]
         if s < 2:
             kv_held = join(kv_held, kv_far)
-    states_p = flash(meta, 1, q_mine, q_other, kv_held, 0, [], 5)
-    states_o = flash(meta, 0, after(q_mine, *states_p), q_other, kv_held, 0, [], 5)
+    states_p = flash(meta, 1, q_mine, q_other, kv_held, [], 5)
+    states_o = flash(meta, 0, after(q_mine, *states_p), q_other, kv_held, [], 5)
 
     def w_step(s, h, array):
         return chip_swap_by_core(array, [STEP[W_ORDERS[c][h][s]] for c in range(2)])
@@ -567,7 +612,7 @@
     w_held = join(w_held, w_far)
     w_far = [w_step(1, h, after(w_held[h], *states_p)) for h in range(2)]
 
-    kept, sent = flash(meta, 1, after(q_mine, *states_o), q_other, kv_far, 1, states_p, 5)
+    kept, sent = flash(meta, 1, after(q_mine, *states_o), q_other, kv_far, states_p, 5)
     came = core_swap(sent)
     w_held = join([after(w, sent) for w in w_held], w_far)
     w_far = [w_step(2, h, w_held[h]) for h in range(2)]
@@ -575,7 +620,7 @@
     pair_out = merge(meta, head_lambda, kept, came, head_gain[None])
     passed = chip_swap(pair_out, STEP["yl"])
     w_last0 = w_step(3, 0, after(w_held[0], pair_out))
-    kept, sent = flash(meta, 0, after(q_mine, pair_out), q_other, kv_far, 1, states_o, 5)
+    kept, sent = flash(meta, 0, after(q_mine, pair_out), q_other, kv_far, states_o, 5)
     came = core_swap(sent)
     block = merge_last(meta, head_lambda, kept, came, head_gain[None], passed)
     blocks = [block] + [shift_x(block, d) for d in (1, 2, 3)]

time: 211 us -> 209 us (level)
  waiting for transfers between devices: 98.4 us -> 102 us
  starting transfers between devices: 55 us -> 52.7 us
    pallas_call x5, Pallas kernels: 25.7 us -> 23.5 us  [the longest x4 21.4 us: flash(): pl.pallas_call(functools.partial(flash_last_kernel if states else flash_f...]
  transfers between devices with their start and end apart: 39 -> 39, of which waited for: 20 -> 21; matrix products, arithmetic and copies ran while one was open for 0% -> 0% of each run, Pallas kernels for 15% -> 14%
where the time goes in v2:
time: 209 us; the launch traced here: 208 us
  waiting for transfers between devices  102 us (49%)
  starting transfers between devices  52.7 us (25%)
  Pallas kernels  47.6 us (23%)
  local copies, waits for them, and re-layouts  3.94 us (2%)
    ppermute x9, waiting for transfers between devices, shift_x(): return lax.ppermute(array, 'tp', [(i, (i + d) % 4) for i in range(4)])  51.7 us
    ppermute x20, waiting for transfers between devices, chip_swap(): return lax.ppermute(array, 'sp', pairs)  31.6 us
    ppermute x20, starting transfers between devices, chip_swap(): return lax.ppermute(array, 'sp', pairs)  24.5 us
    pallas_call x4, Pallas kernels, flash(): pl.pallas_call(functools.partial(flash_last_kernel if states else flash_f...  21.4 us
    ppermute x10, waiting for transfers between devices, chip_swap_by_core(): return lax.ppermute(array, 'sp', pairs)  18.9 us
    ppermute x9, starting transfers between devices, shift_x(): return lax.ppermute(array, 'tp', [(i, (i + d) % 4) for i in range(4)])  14.8 us
    ppermute x10, starting transfers between devices, chip_swap_by_core(): return lax.ppermute(array, 'sp', pairs)  13.5 us
    pallas_call x1, Pallas kernels, ffn(): pl.pallas_call(ffn_kernel, in_specs=[pl.BlockSpec(memory_space=pltpu.SMEM...  9.1 us
  transfers between devices with their start and end apart: 39, of which 21 were waited for; matrix products, arithmetic and copies ran while one was open for 0% of the time, Pallas kernels for 14%

profile of v2, /device:TPU:0, one launch (start us, length us, event | category | flops | bytes accessed | tf_op | source)
XLA Modules:
  0.0 207.7 jit_solution(3213575294159561946)
XLA Ops:
  0.0 2.1 %pack.1 = (bf16[256,768]{1,0:T(8,128)(2,1)}, bf16[256,768]{1,0:T(8,128)(2,1)}) custom-call(bf16[256,512]{1,0:T(8,128)(2,1)} %keys.1, bf16[256,512]{1,0:T(8,128)(2,1)} %values.1, bf16[256,512]{1,0:T(8,128)(2,1)} %queries.1), custom_call_target="tpu_custom_call" | custom-call | flops 1000000000 | bytes 100000 | tf_op jit(solution)/shard_map/pack/pallas_call | solution.py:126
  3.9 9.3 %collective-permute-done.taken = bf16[256,768]{1,0:T(8,128)(2,1)S(1)} collective-permute-done((bf16[256,768]{1,0:T(8,128)(2,1)}, bf16[256,768]{1,0:T(8,128)(2,1)S(1)}, u32[]{:S(2)}, u32[]{:S(2)}) %collective-permute-start) | collective-permute-done | bytes 393248 | tf_op jit(solution)/shard_map/ppermute | solution.py:36
  14.3 2.2 %collective-permute-start.2 = (bf16[1,192,512]{2,1,0:T(8,128)(2,1)S(1)}, bf16[1,192,512]{2,1,0:T(8,128)(2,1)S(1)}, u32[]{:S(2)}, u32[]{:S(2)}) collective-permute-start(bf16[1,192,512]{2,1,0:T(8,128)(2,1)S(1)} %get-tuple-element.55.refs_0_), channel_id=1, source_target_pairs={{0,32},{4,36},{8,40},{12,44},{16,48},{20,52},{24,56},{28,60},{32,0... | collective-permute-start | bytes 589832 | tf_op jit(solution)/shard_map/ppermute | solution.py:36
  16.4 2.5 %collective-permute-start.3 = (bf16[1,160,512]{2,1,0:T(8,128)(2,1)S(1)}, bf16[1,160,512]{2,1,0:T(8,128)(2,1)S(1)}, u32[]{:S(2)}, u32[]{:S(2)}) collective-permute-start(bf16[1,160,512]{2,1,0:T(8,128)(2,1)S(1)} %get-tuple-element.56.refs_1_), channel_id=1, source_target_pairs={{0,96},{4,100},{8,104},{12,108},{16,112},{20,116},{24,120},{28,124... | collective-permute-start | bytes 491528 | tf_op jit(solution)/shard_map/ppermute | solution.py:36
  19.0 3.1 %collective-permute-start.4 = (bf16[1,160,512]{2,1,0:T(8,128)(2,1)S(1)}, bf16[1,160,512]{2,1,0:T(8,128)(2,1)S(1)}, u32[]{:S(2)}, u32[]{:S(2)}) collective-permute-start(bf16[1,160,512]{2,1,0:T(8,128)(2,1)S(1)} %get-tuple-element.57.refs_2_), channel_id=1, source_target_pairs={{0,24},{4,28},{8,16},{12,20},{16,8},{20,12},{24,0},{28,4},{32,56},... | collective-permute-start | bytes 491528 | tf_op jit(solution)/shard_map/ppermute | solution.py:36
  23.0 2.6 %collective-permute-done.4.refs_5_ = bf16[1,160,512]{2,1,0:T(8,128)(2,1)S(1)} collective-permute-done((bf16[1,160,512]{2,1,0:T(8,128)(2,1)S(1)}, bf16[1,160,512]{2,1,0:T(8,128)(2,1)S(1)}, u32[]{:S(2)}, u32[]{:S(2)}) %collective-permute-start.4) | collective-permute-done | bytes 163872 | tf_op jit(solution)/shard_map/ppermute | solution.py:36
  26.5 3.0 %collective-permute-start.6 = (bf16[2,160,512]{2,1,0:T(8,128)(2,1)S(1)}, bf16[2,160,512]{2,1,0:T(8,128)(2,1)S(1)}, u32[]{:S(2)}, u32[]{:S(2)}) collective-permute-start(bf16[2,160,512]{2,1,0:T(8,128)(2,1)S(1)} %get-tuple-element.59.refs_1_), channel_id=1, source_target_pairs={{0,24},{4,28},{8,16},{12,20},{16,8},{20,12},{24,0},{28,4},{32,56},... | collective-permute-start | bytes 983048 | tf_op jit(solution)/shard_map/ppermute | solution.py:36
  29.9 4.8 %collective-permute-done.6.refs_4_ = bf16[2,160,512]{2,1,0:T(8,128)(2,1)S(1)} collective-permute-done((bf16[2,160,512]{2,1,0:T(8,128)(2,1)S(1)}, bf16[2,160,512]{2,1,0:T(8,128)(2,1)S(1)}, u32[]{:S(2)}, u32[]{:S(2)}) %collective-permute-start.6) | collective-permute-done | bytes 327712 | tf_op jit(solution)/shard_map/ppermute | solution.py:36
  38.7 2.3 %collective-permute-start.10 = (bf16[4,160,512]{2,1,0:T(8,128)(2,1)S(1)}, bf16[4,160,512]{2,1,0:T(8,128)(2,1)S(1)}, u32[]{:S(2)}, u32[]{:S(2)}) collective-permute-start(bf16[4,160,512]{2,1,0:T(8,128)(2,1)S(1)} %get-tuple-element.63), channel_id=1, source_target_pairs={{0,96},{4,100},{8,104},{12,108},{16,112},{20,116},{24,120},{28,124... | collective-permute-start | bytes 1966088 | tf_op jit(solution)/shard_map/ppermute | solution.py:36
  41.0 4.3 %flash.4 = (f32[256,640]{1,0:T(8,128)S(1)}, f32[256,640]{1,0:T(8,128)S(1)}) custom-call(s32[86]{0:T(128)S(1)} %compare_select_fusion.1.meta.table, bf16[512,256]{1,0:T(8,128)(2,1)S(1)} %get-tuple-element.72.refs_0_, bf16[512,256]{1,0:T(8,128)(2,1)S(1)} %collective-permute-done.1.refs_1_, bf16[768,512]{1,0:T(8,128)(2,1)S(1)} %bitcast.11, ...), custom_call_target="tpu_custom_call" | custom-call | flops 5000000000 | bytes 100000 | tf_op jit(solution)/shard_map/flash/pallas_call | solution.py:361
  45.4 4.3 %flash.5 = (f32[256,640]{1,0:T(8,128)S(1)}, f32[256,640]{1,0:T(8,128)S(1)}) custom-call(s32[86]{0:T(128)S(1)} %compare_select_fusion.1.meta.table, bf16[512,256]{1,0:T(8,128)(2,1)S(1)} %get-tuple-element.72.refs_0_, bf16[512,256]{1,0:T(8,128)(2,1)S(1)} %collective-permute-done.1.refs_1_, bf16[768,512]{1,0:T(8,128)(2,1)S(1)} %bitcast.12, ...), custom_call_target="tpu_custom_call" | custom-call | flops 5000000000 | bytes 100000 | tf_op jit(solution)/shard_map/flash/pallas_call | solution.py:361
  53.6 6.8 %flash.6 = (f32[256,640]{1,0:T(8,128)S(1)}, f32[256,640]{1,0:T(8,128)}) custom-call(s32[86]{0:T(128)S(1)} %compare_select_fusion.1.meta.table, bf16[512,256]{1,0:T(8,128)(2,1)S(1)} %get-tuple-element.72.refs_0_, bf16[512,256]{1,0:T(8,128)(2,1)S(1)} %collective-permute-done.1.refs_1_, bf16[768,512]{1,0:T(8,128)(2,1)S(1)} %bitcast.9, ...), custom_call_target="tpu_custom_call" | custom-call | flops 5000000000 | bytes 100000 | tf_op jit(solution)/shard_map/flash/pallas_call | solution.py:361
  61.2 2.2 %weights.1 = (bf16[1,64,2176]{2,1,0:T(8,128)(2,1)}, bf16[1,64,2176]{2,1,0:T(8,128)(2,1)}) custom-call(s32[86]{0:T(128)} %copy-done, bf16[64,1408]{1,0:T(8,128)(2,1)} %gate.1, bf16[64,1408]{1,0:T(8,128)(2,1)} %up.1, bf16[64,1408]{1,0:T(8,128)(2,1)} %bitcast.24), custom_call_target="tpu_custom_call" | custom-call | flops 2000000000 | bytes 100000 | tf_op jit(solution)/shard_map/weights/pallas_call | solution.py:160
  65.5 3.2 %lines.1.refs_4_ = bf16[320,2048]{1,0:T(8,128)(2,1)} custom-call(s32[86]{0:T(128)} %copy-done, bf16[512,2048]{1,0:T(8,128)(2,1)} %refs_11_.1, bf16[64,2048]{1,0:T(8,128)(2,1)} %stream.1), custom_call_target="tpu_custom_call" | custom-call | flops 2000000000 | bytes 100000 | tf_op jit(solution)/shard_map/lines/pallas_call | solution.py:189
  70.3 2.7 %collective-permute-start.18 = (bf16[320,2048]{1,0:T(8,128)(2,1)}, bf16[320,2048]{1,0:T(8,128)(2,1)S(1)}, u32[]{:S(2)}, u32[]{:S(2)}) collective-permute-start(bf16[320,2048]{1,0:T(8,128)(2,1)} %lines.1.refs_4_), channel_id=1, source_target_pairs={{0,2},{1,3},{2,0},{3,1},{4,6},{5,7},{6,4},{7,5},{8,10},{9,11},{10,... | collective-permute-start | bytes 3932168 | tf_op jit(solution)/shard_map/ppermute | solution.py:49
  81.3 6.0 %flash.7 = (f32[256,640]{1,0:T(8,128)S(1)}, f32[256,640]{1,0:T(8,128)S(1)}) custom-call(s32[86]{0:T(128)S(1)} %copy-done.1, bf16[512,256]{1,0:T(8,128)(2,1)S(1)} %copy-done.10, bf16[512,256]{1,0:T(8,128)(2,1)S(1)} %copy-done.12, bf16[768,512]{1,0:T(8,128)(2,1)S(1)} %bitcast.10, bf16[640,512]{1,0:T(8,128)(2,1)S(1)} %bitcast.14, ...), custom_call_target="tpu_custom_call" | custom-call | flops 5000000000 | bytes 100000 | tf_op jit(solution)/shard_map/flash/pallas_call | solution.py:361
  89.4 5.3 %collective-permute-done.13.passed_ref = bf16[256,256]{1,0:T(8,128)(2,1)S(1)} collective-permute-done((bf16[256,256]{1,0:T(8,128)(2,1)S(1)}, bf16[256,256]{1,0:T(8,128)(2,1)S(1)}, u32[]{:S(2)}, u32[]{:S(2)}) %collective-permute-start.13) | collective-permute-done | bytes 131104 | tf_op jit(solution)/shard_map/ppermute | solution.py:36
  100.3 2.2 %collective-permute-start.20 = (bf16[320,2048]{1,0:T(8,128)(2,1)S(1)}, bf16[320,2048]{1,0:T(8,128)(2,1)S(1)}, u32[]{:S(2)}, u32[]{:S(2)}) collective-permute-start(bf16[320,2048]{1,0:T(8,128)(2,1)S(1)} %collective-permute-done.17.refs_5_), channel_id=1, source_target_pairs={{0,4},{4,0},{8,12},{12,8},{16,20},{20,16},{24,28},{28,24},{32,36},... | collective-permute-start | bytes 3932168 | tf_op jit(solution)/shard_map/ppermute | solution.py:36
  102.5 26.9 %collective-permute-done.18.refs_6_ = bf16[320,2048]{1,0:T(8,128)(2,1)S(1)} collective-permute-done((bf16[320,2048]{1,0:T(8,128)(2,1)}, bf16[320,2048]{1,0:T(8,128)(2,1)S(1)}, u32[]{:S(2)}, u32[]{:S(2)}) %collective-permute-start.18) | collective-permute-done | bytes 1310752 | tf_op jit(solution)/shard_map/ppermute | solution.py:49
  132.6 2.3 %collective-permute-start.15 = (bf16[256,512]{1,0:T(8,128)(2,1)S(1)}, bf16[256,512]{1,0:T(8,128)(2,1)S(1)}, u32[]{:S(2)}, u32[]{:S(2)}) collective-permute-start(bf16[256,512]{1,0:T(8,128)(2,1)S(1)} %merge_last.1.refs_0_), channel_id=1, source_target_pairs={{0,2},{1,3},{2,0},{3,1},{4,6},{5,7},{6,4},{7,5},{8,10},{9,11},{10,... | collective-permute-start | bytes 786440 | tf_op jit(solution)/shard_map/ppermute | solution.py:49
  135.0 5.7 %collective-permute-done.14.refs_1_ = bf16[256,512]{1,0:T(8,128)(2,1)S(1)} collective-permute-done((bf16[256,512]{1,0:T(8,128)(2,1)S(1)}, bf16[256,512]{1,0:T(8,128)(2,1)S(1)}, u32[]{:S(2)}, u32[]{:S(2)}) %collective-permute-start.14) | collective-permute-done | bytes 262176 | tf_op jit(solution)/shard_map/ppermute | solution.py:49
  142.7 4.5 %collective-permute-done.15.refs_2_ = bf16[256,512]{1,0:T(8,128)(2,1)S(1)} collective-permute-done((bf16[256,512]{1,0:T(8,128)(2,1)S(1)}, bf16[256,512]{1,0:T(8,128)(2,1)S(1)}, u32[]{:S(2)}, u32[]{:S(2)}) %collective-permute-start.15) | collective-permute-done | bytes 262176 | tf_op jit(solution)/shard_map/ppermute | solution.py:49
  147.2 2.5 %collective-permute-start.33 = (bf16[4,64,2176]{2,1,0:T(8,128)(2,1)S(1)}, bf16[4,64,2176]{2,1,0:T(8,128)(2,1)S(1)}, u32[]{:S(2)}, u32[]{:S(2)}) collective-permute-start(bf16[4,64,2176]{2,1,0:T(8,128)(2,1)S(1)} %get-tuple-element.90.refs_4_), channel_id=1, source_target_pairs={{0,96},{4,36},{8,104},{12,44},{16,112},{20,52},{24,120},{28,60},{3... | collective-permute-start | bytes 3342344 | tf_op jit(solution)/shard_map/ppermute | solution.py:41
  154.2 4.9 %middle.1 = (bf16[256,2048]{1,0:T(8,128)(2,1)S(1)}, f32[64,2048]{1,0:T(8,128)S(1)}) custom-call(s32[86]{0:T(128)S(1)} %copy-done.1, bf16[256,512]{1,0:T(8,128)(2,1)S(1)} %merge_last.1.refs_0_, bf16[256,512]{1,0:T(8,128)(2,1)S(1)} %collective-permute-done.14.refs_1_, bf16[256,512]{1,0:T(8,128)(2,1)S(1)} %collective-permute-done.15.refs_2_, ...), custom_call_target="tpu_custom_call" | custom-call | flops 4000000000 | bytes 100000 | tf_op jit(solution)/shard_map/middle/pallas_call | solution.py:469
  159.5 4.4 %collective-permute-done.33.refs_6_ = bf16[4,64,2176]{2,1,0:T(8,128)(2,1)S(1)} collective-permute-done((bf16[4,64,2176]{2,1,0:T(8,128)(2,1)S(1)}, bf16[4,64,2176]{2,1,0:T(8,128)(2,1)S(1)}, u32[]{:S(2)}, u32[]{:S(2)}) %collective-permute-start.33) | collective-permute-done | bytes 1114144 | tf_op jit(solution)/shard_map/ppermute | solution.py:41
  163.9 2.5 %collective-permute-done.30.refs_2_ = bf16[4,64,2176]{2,1,0:T(8,128)(2,1)S(1)} collective-permute-done((bf16[4,64,2176]{2,1,0:T(8,128)(2,1)S(1)}, bf16[4,64,2176]{2,1,0:T(8,128)(2,1)S(1)}, u32[]{:S(2)}, u32[]{:S(2)}) %collective-permute-start.30) | collective-permute-done | bytes 1114144 | tf_op jit(solution)/shard_map/ppermute | solution.py:41
  166.4 11.9 %collective-permute-done.31.refs_3_ = bf16[4,64,2176]{2,1,0:T(8,128)(2,1)S(1)} collective-permute-done((bf16[4,64,2176]{2,1,0:T(8,128)(2,1)S(1)}, bf16[4,64,2176]{2,1,0:T(8,128)(2,1)S(1)}, u32[]{:S(2)}, u32[]{:S(2)}) %collective-permute-start.31) | collective-permute-done | bytes 1114144 | tf_op jit(solution)/shard_map/ppermute | solution.py:41
  178.4 9.1 %ffn.1 = (f32[256,2048]{1,0:T(8,128)S(1)}, bf16[256,2048]{1,0:T(8,128)(2,1)S(1)}) custom-call(s32[86]{0:T(128)S(1)} %copy-done.1, bf16[256,2048]{1,0:T(8,128)(2,1)S(1)} %get-tuple-element.78.mine_ref, bf16[256,2048]{1,0:T(8,128)(2,1)S(1)} %collective-permute-done.23.other_ref, bf16[4,64,2176]{2,1,0:T(8,128)(2,1)S(1)} %get-tuple-element.88.refs_0_, ...), custom_call_target="tpu_custom_call" | custom-call | flops 8999999488 | bytes 100000 | tf_op jit(solution)/shard_map/ffn/pallas_call | solution.py:541
  187.5 2.6 %collective-permute-done.35.came_ref = bf16[256,2048]{1,0:T(8,128)(2,1)S(1)} collective-permute-done((bf16[256,2048]{1,0:T(8,128)(2,1)S(1)}, bf16[256,2048]{1,0:T(8,128)(2,1)S(1)}, u32[]{:S(2)}, u32[]{:S(2)}) %collective-permute-start.35) | collective-permute-done | bytes 1048608 | tf_op jit(solution)/shard_map/ppermute | solution.py:36
  193.3 6.4 %collective-permute-done.38 = bf16[64,2048]{1,0:T(8,128)(2,1)S(1)} collective-permute-done((bf16[64,2048]{1,0:T(8,128)(2,1)S(1)}, bf16[64,2048]{1,0:T(8,128)(2,1)S(1)}, u32[]{:S(2)}, u32[]{:S(2)}) %collective-permute-start.38) | collective-permute-done | bytes 262176 | tf_op jit(solution)/shard_map/ppermute | solution.py:49
  199.6 2.9 %collective-permute-done.37 = bf16[64,2048]{1,0:T(8,128)(2,1)S(1)} collective-permute-done((bf16[64,2048]{1,0:T(8,128)(2,1)S(1)}, bf16[64,2048]{1,0:T(8,128)(2,1)S(1)}, u32[]{:S(2)}, u32[]{:S(2)}) %collective-permute-start.37) | collective-permute-done | bytes 262176 | tf_op jit(solution)/shard_map/ppermute | solution.py:49
  202.5 4.3 %collective-permute-done.36 = bf16[64,2048]{1,0:T(8,128)(2,1)S(1)} collective-permute-done((bf16[64,2048]{1,0:T(8,128)(2,1)S(1)}, bf16[64,2048]{1,0:T(8,128)(2,1)S(1)}, u32[]{:S(2)}, u32[]{:S(2)}) %collective-permute-start.36) | collective-permute-done | bytes 262176 | tf_op jit(solution)/shard_map/ppermute | solution.py:49
  (121 shorter events, 47.2 us)
Async XLA Ops:
  2.1 11.1 %collective-permute-start = (bf16[256,768]{1,0:T(8,128)(2,1)}, bf16[256,768]{1,0:T(8,128)(2,1)S(1)}, u32[]{:S(2)}, u32[]{:S(2)}) collective-permute-start(bf16[256,768]{1,0:T(8,128)(2,1)} %get-tuple-element.53), channel_id=1, source_target_pairs={{0,8},{4,12},{8,0},{12,4},{16,24},{20,28},{24,16},{28,20},{32,40},... | collective-permute-start | bytes 1179656 | tf_op jit(solution)/shard_map/ppermute | solution.py:36
  14.3 11.3 %collective-permute-start.2 = (bf16[1,192,512]{2,1,0:T(8,128)(2,1)S(1)}, bf16[1,192,512]{2,1,0:T(8,128)(2,1)S(1)}, u32[]{:S(2)}, u32[]{:S(2)}) collective-permute-start(bf16[1,192,512]{2,1,0:T(8,128)(2,1)S(1)} %get-tuple-element.55.refs_0_), channel_id=1, source_target_pairs={{0,32},{4,36},{8,40},{12,44},{16,48},{20,52},{24,56},{28,60},{32,0... | collective-permute-start | bytes 589832 | tf_op jit(solution)/shard_map/ppermute | solution.py:36
  25.7 10.9 %collective-permute-start.5 = (bf16[2,192,512]{2,1,0:T(8,128)(2,1)S(1)}, bf16[2,192,512]{2,1,0:T(8,128)(2,1)S(1)}, u32[]{:S(2)}, u32[]{:S(2)}) collective-permute-start(bf16[2,192,512]{2,1,0:T(8,128)(2,1)S(1)} %get-tuple-element.58.refs_0_), channel_id=1, source_target_pairs={{0,96},{4,100},{8,104},{12,108},{16,112},{20,116},{24,120},{28,124... | collective-permute-start | bytes 1179656 | tf_op jit(solution)/shard_map/ppermute | solution.py:36
  29.9 11.2 %collective-permute-start.1 = (bf16[512,256]{1,0:T(8,128)(2,1)S(1)}, bf16[512,256]{1,0:T(8,128)(2,1)S(1)}, u32[]{:S(2)}, u32[]{:S(2)}) collective-permute-start(bf16[512,256]{1,0:T(8,128)(2,1)S(1)} %get-tuple-element.72.refs_0_), channel_id=1, source_target_pairs={{0,4},{4,0},{8,12},{12,8},{16,20},{20,16},{24,28},{28,24},{32,36},... | collective-permute-start | bytes 786440 | tf_op jit(solution)/shard_map/ppermute | solution.py:36
  36.7 16.9 %collective-permute-start.8 = (bf16[4,192,512]{2,1,0:T(8,128)(2,1)S(1)}, bf16[4,192,512]{2,1,0:T(8,128)(2,1)S(1)}, u32[]{:S(2)}, u32[]{:S(2)}) collective-permute-start(bf16[4,192,512]{2,1,0:T(8,128)(2,1)S(1)} %get-tuple-element.61), channel_id=1, source_target_pairs={{0,24},{4,28},{8,16},{12,20},{16,8},{20,12},{24,0},{28,4},{32,56},... | collective-permute-start | bytes 2359304 | tf_op jit(solution)/shard_map/ppermute | solution.py:36
  38.7 13.0 %collective-permute-start.9 = (bf16[4,160,512]{2,1,0:T(8,128)(2,1)S(1)}, bf16[4,160,512]{2,1,0:T(8,128)(2,1)S(1)}, u32[]{:S(2)}, u32[]{:S(2)}) collective-permute-start(bf16[4,160,512]{2,1,0:T(8,128)(2,1)S(1)} %get-tuple-element.62), channel_id=1, source_target_pairs={{0,32},{4,36},{8,40},{12,44},{16,48},{20,52},{24,56},{28,60},{32,0... | collective-permute-start | bytes 1966088 | tf_op jit(solution)/shard_map/ppermute | solution.py:36
  38.7 14.2 %collective-permute-start.10 = (bf16[4,160,512]{2,1,0:T(8,128)(2,1)S(1)}, bf16[4,160,512]{2,1,0:T(8,128)(2,1)S(1)}, u32[]{:S(2)}, u32[]{:S(2)}) collective-permute-start(bf16[4,160,512]{2,1,0:T(8,128)(2,1)S(1)} %get-tuple-element.63), channel_id=1, source_target_pairs={{0,96},{4,100},{8,104},{12,108},{16,112},{20,116},{24,120},{28,124... | collective-permute-start | bytes 1966088 | tf_op jit(solution)/shard_map/ppermute | solution.py:36
  61.2 17.5 %collective-permute-start.11 = (f32[256,640]{1,0:T(8,128)}, f32[256,640]{1,0:T(8,128)}, u32[]{:S(2)}, u32[]{:S(2)}) collective-permute-start(f32[256,640]{1,0:T(8,128)} %get-tuple-element.71), channel_id=1, source_target_pairs={{0,4},{4,0},{8,12},{12,8},{16,20},{20,16},{24,28},{28,24},{32,36},... | collective-permute-start | bytes 1966088 | tf_op jit(solution)/shard_map/ppermute | solution.py:36
  64.0 9.0 %collective-permute-start.25 = (bf16[1,64,2176]{2,1,0:T(8,128)(2,1)}, bf16[1,64,2176]{2,1,0:T(8,128)(2,1)}, u32[]{:S(2)}, u32[]{:S(2)}) collective-permute-start(bf16[1,64,2176]{2,1,0:T(8,128)(2,1)} %get-tuple-element.79.refs_0_), channel_id=1, source_target_pairs={{0,32},{4,100},{8,40},{12,108},{16,48},{20,116},{24,56},{28,124},{... | collective-permute-start | bytes 835592 | tf_op jit(solution)/shard_map/ppermute | solution.py:41
  65.5 9.0 %collective-permute-start.26 = (bf16[1,64,2176]{2,1,0:T(8,128)(2,1)}, bf16[1,64,2176]{2,1,0:T(8,128)(2,1)}, u32[]{:S(2)}, u32[]{:S(2)}) collective-permute-start(bf16[1,64,2176]{2,1,0:T(8,128)(2,1)} %collective-permute-done.24.refs_1_), channel_id=1, source_target_pairs={{0,8},{4,28},{8,0},{12,20},{16,24},{20,12},{24,16},{28,4},{32,40},... | collective-permute-start | bytes 835592 | tf_op jit(solution)/shard_map/ppermute | solution.py:41
  68.7 31.6 %collective-permute-start.17 = (bf16[320,2048]{1,0:T(8,128)(2,1)}, bf16[320,2048]{1,0:T(8,128)(2,1)S(1)}, u32[]{:S(2)}, u32[]{:S(2)}) collective-permute-start(bf16[320,2048]{1,0:T(8,128)(2,1)} %lines.1.refs_4_), channel_id=1, source_target_pairs={{0,1},{1,2},{2,3},{3,0},{4,5},{5,6},{6,7},{7,4},{8,9},{9,10},{10,1... | collective-permute-start | bytes 3932168 | tf_op jit(solution)/shard_map/ppermute | solution.py:49
  70.3 59.1 %collective-permute-start.18 = (bf16[320,2048]{1,0:T(8,128)(2,1)}, bf16[320,2048]{1,0:T(8,128)(2,1)S(1)}, u32[]{:S(2)}, u32[]{:S(2)}) collective-permute-start(bf16[320,2048]{1,0:T(8,128)(2,1)} %lines.1.refs_4_), channel_id=1, source_target_pairs={{0,2},{1,3},{2,0},{3,1},{4,6},{5,7},{6,4},{7,5},{8,10},{9,11},{10,... | collective-permute-start | bytes 3932168 | tf_op jit(solution)/shard_map/ppermute | solution.py:49
  73.0 57.7 %collective-permute-start.19 = (bf16[320,2048]{1,0:T(8,128)(2,1)}, bf16[320,2048]{1,0:T(8,128)(2,1)S(1)}, u32[]{:S(2)}, u32[]{:S(2)}) collective-permute-start(bf16[320,2048]{1,0:T(8,128)(2,1)} %lines.1.refs_4_), channel_id=1, source_target_pairs={{0,3},{1,0},{2,1},{3,2},{4,7},{5,4},{6,5},{7,6},{8,11},{9,8},{10,9... | collective-permute-start | bytes 3932168 | tf_op jit(solution)/shard_map/ppermute | solution.py:49
  76.7 10.6 %collective-permute-start.27 = (bf16[2,64,2176]{2,1,0:T(8,128)(2,1)S(1)}, bf16[2,64,2176]{2,1,0:T(8,128)(2,1)S(1)}, u32[]{:S(2)}, u32[]{:S(2)}) collective-permute-start(bf16[2,64,2176]{2,1,0:T(8,128)(2,1)S(1)} %get-tuple-element.85.refs_0_), channel_id=1, source_target_pairs={{0,8},{4,28},{8,0},{12,20},{16,24},{20,12},{24,16},{28,4},{32,40},... | collective-permute-start | bytes 1671176 | tf_op jit(solution)/shard_map/ppermute | solution.py:41
  78.8 10.5 %collective-permute-start.28 = (bf16[2,64,2176]{2,1,0:T(8,128)(2,1)S(1)}, bf16[2,64,2176]{2,1,0:T(8,128)(2,1)S(1)}, u32[]{:S(2)}, u32[]{:S(2)}) collective-permute-start(bf16[2,64,2176]{2,1,0:T(8,128)(2,1)S(1)} %get-tuple-element.86.refs_1_), channel_id=1, source_target_pairs={{0,32},{4,100},{8,40},{12,108},{16,48},{20,116},{24,56},{28,124},{... | collective-permute-start | bytes 1671176 | tf_op jit(solution)/shard_map/ppermute | solution.py:41
  87.3 9.4 %collective-permute-start.12 = (f32[256,640]{1,0:T(8,128)S(1)}, f32[256,640]{1,0:T(8,128)S(1)}, u32[]{:S(2)}, u32[]{:S(2)}) collective-permute-start(f32[256,640]{1,0:T(8,128)S(1)} %get-tuple-element.74), channel_id=1, source_target_pairs={{0,4},{4,0},{8,12},{12,8},{16,20},{20,16},{24,28},{28,24},{32,36},... | collective-permute-start | bytes 1966088 | tf_op jit(solution)/shard_map/ppermute | solution.py:36
  94.7 36.0 %collective-permute-start.29 = (bf16[4,64,2176]{2,1,0:T(8,128)(2,1)S(1)}, bf16[4,64,2176]{2,1,0:T(8,128)(2,1)S(1)}, u32[]{:S(2)}, u32[]{:S(2)}) collective-permute-start(bf16[4,64,2176]{2,1,0:T(8,128)(2,1)S(1)} %get-tuple-element.88.refs_0_), channel_id=1, source_target_pairs={{0,96},{4,36},{8,104},{12,44},{16,112},{20,52},{24,120},{28,60},{3... | collective-permute-start | bytes 3342344 | tf_op jit(solution)/shard_map/ppermute | solution.py:41
  96.7 36.0 %collective-permute-start.32 = (bf16[4,64,2176]{2,1,0:T(8,128)(2,1)S(1)}, bf16[4,64,2176]{2,1,0:T(8,128)(2,1)S(1)}, u32[]{:S(2)}, u32[]{:S(2)}) collective-permute-start(bf16[4,64,2176]{2,1,0:T(8,128)(2,1)S(1)} %get-tuple-element.90.refs_4_), channel_id=1, source_target_pairs={{0,24},{4,12},{8,16},{12,4},{16,8},{20,28},{24,0},{28,20},{32,56},... | collective-permute-start | bytes 3342344 | tf_op jit(solution)/shard_map/ppermute | solution.py:41
  100.3 50.9 %collective-permute-start.20 = (bf16[320,2048]{1,0:T(8,128)(2,1)S(1)}, bf16[320,2048]{1,0:T(8,128)(2,1)S(1)}, u32[]{:S(2)}, u32[]{:S(2)}) collective-permute-start(bf16[320,2048]{1,0:T(8,128)(2,1)S(1)} %collective-permute-done.17.refs_5_), channel_id=1, source_target_pairs={{0,4},{4,0},{8,12},{12,8},{16,20},{20,16},{24,28},{28,24},{32,36},... | collective-permute-start | bytes 3932168 | tf_op jit(solution)/shard_map/ppermute | solution.py:36
  129.4 23.6 %collective-permute-start.21 = (bf16[320,2048]{1,0:T(8,128)(2,1)S(1)}, bf16[320,2048]{1,0:T(8,128)(2,1)S(1)}, u32[]{:S(2)}, u32[]{:S(2)}) collective-permute-start(bf16[320,2048]{1,0:T(8,128)(2,1)S(1)} %collective-permute-done.18.refs_6_), channel_id=1, source_target_pairs={{0,4},{4,0},{8,12},{12,8},{16,20},{20,16},{24,28},{28,24},{32,36},... | collective-permute-start | bytes 3932168 | tf_op jit(solution)/shard_map/ppermute | solution.py:36
  130.7 23.4 %collective-permute-start.22 = (bf16[320,2048]{1,0:T(8,128)(2,1)S(1)}, bf16[320,2048]{1,0:T(8,128)(2,1)S(1)}, u32[]{:S(2)}, u32[]{:S(2)}) collective-permute-start(bf16[320,2048]{1,0:T(8,128)(2,1)S(1)} %collective-permute-done.19.refs_7_), channel_id=1, source_target_pairs={{0,4},{4,0},{8,12},{12,8},{16,20},{20,16},{24,28},{28,24},{32,36},... | collective-permute-start | bytes 3932168 | tf_op jit(solution)/shard_map/ppermute | solution.py:36
  130.8 9.9 %collective-permute-start.14 = (bf16[256,512]{1,0:T(8,128)(2,1)S(1)}, bf16[256,512]{1,0:T(8,128)(2,1)S(1)}, u32[]{:S(2)}, u32[]{:S(2)}) collective-permute-start(bf16[256,512]{1,0:T(8,128)(2,1)S(1)} %merge_last.1.refs_0_), channel_id=1, source_target_pairs={{0,1},{1,2},{2,3},{3,0},{4,5},{5,6},{6,7},{7,4},{8,9},{9,10},{10,1... | collective-permute-start | bytes 786440 | tf_op jit(solution)/shard_map/ppermute | solution.py:49
  132.6 14.5 %collective-permute-start.15 = (bf16[256,512]{1,0:T(8,128)(2,1)S(1)}, bf16[256,512]{1,0:T(8,128)(2,1)S(1)}, u32[]{:S(2)}, u32[]{:S(2)}) collective-permute-start(bf16[256,512]{1,0:T(8,128)(2,1)S(1)} %merge_last.1.refs_0_), channel_id=1, source_target_pairs={{0,2},{1,3},{2,0},{3,1},{4,6},{5,7},{6,4},{7,5},{8,10},{9,11},{10,... | collective-permute-start | bytes 786440 | tf_op jit(solution)/shard_map/ppermute | solution.py:49
  140.7 9.0 %collective-permute-start.16 = (bf16[256,512]{1,0:T(8,128)(2,1)S(1)}, bf16[256,512]{1,0:T(8,128)(2,1)S(1)}, u32[]{:S(2)}, u32[]{:S(2)}) collective-permute-start(bf16[256,512]{1,0:T(8,128)(2,1)S(1)} %merge_last.1.refs_0_), channel_id=1, source_target_pairs={{0,3},{1,0},{2,1},{3,2},{4,7},{5,4},{6,5},{7,6},{8,11},{9,8},{10,9... | collective-permute-start | bytes 786440 | tf_op jit(solution)/shard_map/ppermute | solution.py:49
  147.2 16.7 %collective-permute-start.33 = (bf16[4,64,2176]{2,1,0:T(8,128)(2,1)S(1)}, bf16[4,64,2176]{2,1,0:T(8,128)(2,1)S(1)}, u32[]{:S(2)}, u32[]{:S(2)}) collective-permute-start(bf16[4,64,2176]{2,1,0:T(8,128)(2,1)S(1)} %get-tuple-element.90.refs_4_), channel_id=1, source_target_pairs={{0,96},{4,36},{8,104},{12,44},{16,112},{20,52},{24,120},{28,60},{3... | collective-permute-start | bytes 3342344 | tf_op jit(solution)/shard_map/ppermute | solution.py:41
  149.7 16.7 %collective-permute-start.30 = (bf16[4,64,2176]{2,1,0:T(8,128)(2,1)S(1)}, bf16[4,64,2176]{2,1,0:T(8,128)(2,1)S(1)}, u32[]{:S(2)}, u32[]{:S(2)}) collective-permute-start(bf16[4,64,2176]{2,1,0:T(8,128)(2,1)S(1)} %get-tuple-element.88.refs_0_), channel_id=1, source_target_pairs={{0,24},{4,12},{8,16},{12,4},{16,8},{20,28},{24,0},{28,20},{32,56},... | collective-permute-start | bytes 3342344 | tf_op jit(solution)/shard_map/ppermute | solution.py:41
  151.2 27.2 %collective-permute-start.31 = (bf16[4,64,2176]{2,1,0:T(8,128)(2,1)S(1)}, bf16[4,64,2176]{2,1,0:T(8,128)(2,1)S(1)}, u32[]{:S(2)}, u32[]{:S(2)}) collective-permute-start(bf16[4,64,2176]{2,1,0:T(8,128)(2,1)S(1)} %collective-permute-done.29.refs_1_), channel_id=1, source_target_pairs={{0,24},{4,12},{8,16},{12,4},{16,8},{20,28},{24,0},{28,20},{32,56},... | collective-permute-start | bytes 3342344 | tf_op jit(solution)/shard_map/ppermute | solution.py:41
  152.9 25.4 %collective-permute-start.34 = (bf16[4,64,2176]{2,1,0:T(8,128)(2,1)S(1)}, bf16[4,64,2176]{2,1,0:T(8,128)(2,1)S(1)}, u32[]{:S(2)}, u32[]{:S(2)}) collective-permute-start(bf16[4,64,2176]{2,1,0:T(8,128)(2,1)S(1)} %collective-permute-done.32.refs_5_), channel_id=1, source_target_pairs={{0,96},{4,36},{8,104},{12,44},{16,112},{20,52},{24,120},{28,60},{3... | collective-permute-start | bytes 3342344 | tf_op jit(solution)/shard_map/ppermute | solution.py:41
  159.1 19.2 %collective-permute-start.23 = (bf16[256,2048]{1,0:T(8,128)(2,1)S(1)}, bf16[256,2048]{1,0:T(8,128)(2,1)S(1)}, u32[]{:S(2)}, u32[]{:S(2)}) collective-permute-start(bf16[256,2048]{1,0:T(8,128)(2,1)S(1)} %get-tuple-element.78.mine_ref), channel_id=1, source_target_pairs={{0,4},{4,0},{8,12},{12,8},{16,20},{20,16},{24,28},{28,24},{32,36},... | collective-permute-start | bytes 3145736 | tf_op jit(solution)/shard_map/ppermute | solution.py:36
  190.4 9.2 %collective-permute-start.38 = (bf16[64,2048]{1,0:T(8,128)(2,1)S(1)}, bf16[64,2048]{1,0:T(8,128)(2,1)S(1)}, u32[]{:S(2)}, u32[]{:S(2)}) collective-permute-start(bf16[64,2048]{1,0:T(8,128)(2,1)S(1)} %get-tuple-element.98), channel_id=1, source_target_pairs={{0,3},{1,0},{2,1},{3,2},{4,7},{5,4},{6,5},{7,6},{8,11},{9,8},{10,9... | collective-permute-start | bytes 786440 | tf_op jit(solution)/shard_map/ppermute | solution.py:49
  191.8 10.7 %collective-permute-start.37 = (bf16[64,2048]{1,0:T(8,128)(2,1)S(1)}, bf16[64,2048]{1,0:T(8,128)(2,1)S(1)}, u32[]{:S(2)}, u32[]{:S(2)}) collective-permute-start(bf16[64,2048]{1,0:T(8,128)(2,1)S(1)} %get-tuple-element.97), channel_id=1, source_target_pairs={{0,2},{1,3},{2,0},{3,1},{4,6},{5,7},{6,4},{7,5},{8,10},{9,11},{10,... | collective-permute-start | bytes 786440 | tf_op jit(solution)/shard_map/ppermute | solution.py:49
  191.9 14.9 %collective-permute-start.36 = (bf16[64,2048]{1,0:T(8,128)(2,1)S(1)}, bf16[64,2048]{1,0:T(8,128)(2,1)S(1)}, u32[]{:S(2)}, u32[]{:S(2)}) collective-permute-start(bf16[64,2048]{1,0:T(8,128)(2,1)S(1)} %get-tuple-element.96), channel_id=1, source_target_pairs={{0,1},{1,2},{2,3},{3,0},{4,5},{5,6},{6,7},{7,4},{8,9},{9,10},{10,1... | collective-permute-start | bytes 786440 | tf_op jit(solution)/shard_map/ppermute | solution.py:49
  (35 other events, 419.5 us)

commit v3 on v2

--- a/solution.py
+++ b/solution.py
@@ -488,8 +488,8 @@
 
 def ffn_kernel(table, mine_ref, other_ref, *refs):
     pieces = refs[:8]
-    keep_ref, send_ref = refs[8:10]
-    gu, down, both, hidden, sem = refs[10:]
+    send_ref, hidden, down = refs[8:11]
+    gu, both, sem = refs[11:]
     for k in range(8):
 
         def body(i, _, w=pieces[k], base=4 * k):
@@ -523,13 +523,19 @@
     lax.fori_loop(0, 4, activate, 0)
     pltpu.make_async_copy(down, down, sem.at[2]).wait()
 
+    project_rows(hidden, 0, down, send_ref)
+
+
+def project_rows(hidden, first, down, out_ref):
     def project(k, _):
         rows = pl.ds(pl.multiple_of(k * 512, 512), 512)
         part = lax.dot_general(
-            hidden[...], down[rows, :], (((1,), (1,)), ((), ())), preferred_element_type=F32
+            hidden[first : first + 256],
+            down[rows, :],
+            (((1,), (1,)), ((), ())),
+            preferred_element_type=F32,
         )
-        send_ref[:, rows] = part[:256].astype(BF16)
-        keep_ref[:, rows] = part[256:]
+        out_ref[:, rows] = part.astype(out_ref.dtype)
         return 0
 
     lax.fori_loop(0, 4, project, 0)
@@ -541,19 +547,38 @@
     return pl.pallas_call(
         ffn_kernel,
         in_specs=[pl.BlockSpec(memory_space=pltpu.SMEM), in_vmem, in_vmem] + [any_space] * 8,
-        out_specs=[in_vmem] * 2,
-        out_shape=[jax.ShapeDtypeStruct((256, 2048), F32), jax.ShapeDtypeStruct((256, 2048), BF16)],
+        out_specs=[in_vmem] * 3,
+        out_shape=[
+            jax.ShapeDtypeStruct((256, 2048), BF16),
+            jax.ShapeDtypeStruct((512, 768), BF16),
+            jax.ShapeDtypeStruct((2048, 768), BF16),
+        ],
         scratch_shapes=[
             pltpu.VMEM((2048, 1408), BF16),
-            pltpu.VMEM((2048, 768), BF16),
             pltpu.VMEM((512, 1408), F32),
-            pltpu.VMEM((512, 768), BF16),
             pltpu.SemaphoreType.DMA((3,)),
         ],
         compiler_params=vmem_params(28),
         cost_estimate=cost(9),
         name="ffn",
     )(table, mine, other, *pieces)
+
+
+def own_rows_kernel(hidden, down, out_ref):
+    project_rows(hidden, 256, down, out_ref)
+
+
+def own_rows(hidden, down):
+    in_vmem = pl.BlockSpec(memory_space=pltpu.VMEM)
+    return pl.pallas_call(
+        own_rows_kernel,
+        in_specs=[in_vmem] * 2,
+        out_specs=in_vmem,
+        out_shape=jax.ShapeDtypeStruct((256, 2048), F32),
+        compiler_params=vmem_params(),
+        cost_estimate=cost(2),
+        name="own_rows",
+    )(hidden, down)
 
 
 def add_kernel(mine_ref, came_ref, middle_ref, own_ref, *sent):
@@ -629,13 +654,15 @@
     w_last = [w_last0, w_last1]
     normed, middle = middle_call(meta, blocks, w_mines, w_others, w_out, norm_gain[None])
     other_normed = core_swap(normed)
-    kept_part, sent_part = ffn(
+    sent_part, hidden, down = ffn(
         meta,
         normed,
         other_normed,
         [w_held[0], w_far[0], w_last[0], w_tail[0], w_held[1], w_far[1], w_last[1], w_tail[1]],
     )
-    result, *parts = add_parts(kept_part, core_swap(sent_part), middle)
+    came_part = core_swap(sent_part)
+    kept_part = own_rows(hidden, down)
+    result, *parts = add_parts(kept_part, came_part, middle)
     for d in (1, 2, 3):
         result = result + shift_x(parts[d - 1], d).astype(F32)
     return result.astype(BF16)

time: 209 us -> 208 us (level)
  transfers between devices with their start and end apart: 39 -> 39, of which waited for: 21 -> 21; matrix products, arithmetic and copies ran while one was open for 0% -> 0% of each run, Pallas kernels for 14% -> 15%
where the time goes in v3:
time: 208 us; the launch traced here: 207 us
  waiting for transfers between devices  101 us (49%)
  starting transfers between devices  52.7 us (25%)
  Pallas kernels  48.4 us (23%)
  local copies, waits for them, and re-layouts  3.94 us (2%)
    ppermute x9, waiting for transfers between devices, shift_x(): return lax.ppermute(array, 'tp', [(i, (i + d) % 4) for i in range(4)])  51.7 us
    ppermute x20, waiting for transfers between devices, chip_swap(): return lax.ppermute(array, 'sp', pairs)  30 us
    ppermute x20, starting transfers between devices, chip_swap(): return lax.ppermute(array, 'sp', pairs)  24.5 us
    pallas_call x4, Pallas kernels, flash(): pl.pallas_call(functools.partial(flash_last_kernel if states else flash_f...  21.4 us
    ppermute x10, waiting for transfers between devices, chip_swap_by_core(): return lax.ppermute(array, 'sp', pairs)  18.9 us
    ppermute x9, starting transfers between devices, shift_x(): return lax.ppermute(array, 'tp', [(i, (i + d) % 4) for i in range(4)])  14.8 us
    ppermute x10, starting transfers between devices, chip_swap_by_core(): return lax.ppermute(array, 'sp', pairs)  13.5 us
    pallas_call x1, Pallas kernels, ffn(): pl.pallas_call(ffn_kernel, in_specs=[pl.BlockSpec(memory_space=pltpu.SMEM...  8.29 us
  transfers between devices with their start and end apart: 39, of which 21 were waited for; matrix products, arithmetic and copies ran while one was open for 0% of the time, Pallas kernels for 15%

profile of v3, /device:TPU:0, one launch (start us, length us, event | category | flops | bytes accessed | tf_op | source)
XLA Modules:
  0.0 206.8 jit_solution(12040718682372969211)
XLA Ops:
  0.0 2.1 %pack.1 = (bf16[256,768]{1,0:T(8,128)(2,1)}, bf16[256,768]{1,0:T(8,128)(2,1)}) custom-call(bf16[256,512]{1,0:T(8,128)(2,1)} %keys.1, bf16[256,512]{1,0:T(8,128)(2,1)} %values.1, bf16[256,512]{1,0:T(8,128)(2,1)} %queries.1), custom_call_target="tpu_custom_call" | custom-call | flops 1000000000 | bytes 100000 | tf_op jit(solution)/shard_map/pack/pallas_call | solution.py:126
  3.9 9.3 %collective-permute-done.taken = bf16[256,768]{1,0:T(8,128)(2,1)S(1)} collective-permute-done((bf16[256,768]{1,0:T(8,128)(2,1)}, bf16[256,768]{1,0:T(8,128)(2,1)S(1)}, u32[]{:S(2)}, u32[]{:S(2)}) %collective-permute-start) | collective-permute-done | bytes 393248 | tf_op jit(solution)/shard_map/ppermute | solution.py:36
  14.3 2.2 %collective-permute-start.2 = (bf16[1,192,512]{2,1,0:T(8,128)(2,1)S(1)}, bf16[1,192,512]{2,1,0:T(8,128)(2,1)S(1)}, u32[]{:S(2)}, u32[]{:S(2)}) collective-permute-start(bf16[1,192,512]{2,1,0:T(8,128)(2,1)S(1)} %get-tuple-element.56.refs_0_), channel_id=1, source_target_pairs={{0,32},{4,36},{8,40},{12,44},{16,48},{20,52},{24,56},{28,60},{32,0... | collective-permute-start | bytes 589832 | tf_op jit(solution)/shard_map/ppermute | solution.py:36
  16.4 2.5 %collective-permute-start.3 = (bf16[1,160,512]{2,1,0:T(8,128)(2,1)S(1)}, bf16[1,160,512]{2,1,0:T(8,128)(2,1)S(1)}, u32[]{:S(2)}, u32[]{:S(2)}) collective-permute-start(bf16[1,160,512]{2,1,0:T(8,128)(2,1)S(1)} %get-tuple-element.57.refs_1_), channel_id=1, source_target_pairs={{0,96},{4,100},{8,104},{12,108},{16,112},{20,116},{24,120},{28,124... | collective-permute-start | bytes 491528 | tf_op jit(solution)/shard_map/ppermute | solution.py:36
  19.0 3.1 %collective-permute-start.4 = (bf16[1,160,512]{2,1,0:T(8,128)(2,1)S(1)}, bf16[1,160,512]{2,1,0:T(8,128)(2,1)S(1)}, u32[]{:S(2)}, u32[]{:S(2)}) collective-permute-start(bf16[1,160,512]{2,1,0:T(8,128)(2,1)S(1)} %get-tuple-element.58.refs_2_), channel_id=1, source_target_pairs={{0,24},{4,28},{8,16},{12,20},{16,8},{20,12},{24,0},{28,4},{32,56},... | collective-permute-start | bytes 491528 | tf_op jit(solution)/shard_map/ppermute | solution.py:36
  23.0 2.6 %collective-permute-done.4.refs_5_ = bf16[1,160,512]{2,1,0:T(8,128)(2,1)S(1)} collective-permute-done((bf16[1,160,512]{2,1,0:T(8,128)(2,1)S(1)}, bf16[1,160,512]{2,1,0:T(8,128)(2,1)S(1)}, u32[]{:S(2)}, u32[]{:S(2)}) %collective-permute-start.4) | collective-permute-done | bytes 163872 | tf_op jit(solution)/shard_map/ppermute | solution.py:36
  26.5 3.0 %collective-permute-start.6 = (bf16[2,160,512]{2,1,0:T(8,128)(2,1)S(1)}, bf16[2,160,512]{2,1,0:T(8,128)(2,1)S(1)}, u32[]{:S(2)}, u32[]{:S(2)}) collective-permute-start(bf16[2,160,512]{2,1,0:T(8,128)(2,1)S(1)} %get-tuple-element.60.refs_1_), channel_id=1, source_target_pairs={{0,24},{4,28},{8,16},{12,20},{16,8},{20,12},{24,0},{28,4},{32,56},... | collective-permute-start | bytes 983048 | tf_op jit(solution)/shard_map/ppermute | solution.py:36
  29.9 4.8 %collective-permute-done.6.refs_4_ = bf16[2,160,512]{2,1,0:T(8,128)(2,1)S(1)} collective-permute-done((bf16[2,160,512]{2,1,0:T(8,128)(2,1)S(1)}, bf16[2,160,512]{2,1,0:T(8,128)(2,1)S(1)}, u32[]{:S(2)}, u32[]{:S(2)}) %collective-permute-start.6) | collective-permute-done | bytes 327712 | tf_op jit(solution)/shard_map/ppermute | solution.py:36
  38.7 2.3 %collective-permute-start.10 = (bf16[4,160,512]{2,1,0:T(8,128)(2,1)S(1)}, bf16[4,160,512]{2,1,0:T(8,128)(2,1)S(1)}, u32[]{:S(2)}, u32[]{:S(2)}) collective-permute-start(bf16[4,160,512]{2,1,0:T(8,128)(2,1)S(1)} %get-tuple-element.64), channel_id=1, source_target_pairs={{0,96},{4,100},{8,104},{12,108},{16,112},{20,116},{24,120},{28,124... | collective-permute-start | bytes 1966088 | tf_op jit(solution)/shard_map/ppermute | solution.py:36
  41.0 4.3 %flash.4 = (f32[256,640]{1,0:T(8,128)S(1)}, f32[256,640]{1,0:T(8,128)S(1)}) custom-call(s32[86]{0:T(128)S(1)} %compare_select_fusion.1.meta.table, bf16[512,256]{1,0:T(8,128)(2,1)S(1)} %get-tuple-element.73.refs_0_, bf16[512,256]{1,0:T(8,128)(2,1)S(1)} %collective-permute-done.1.refs_1_, bf16[768,512]{1,0:T(8,128)(2,1)S(1)} %bitcast.11, ...), custom_call_target="tpu_custom_call" | custom-call | flops 5000000000 | bytes 100000 | tf_op jit(solution)/shard_map/flash/pallas_call | solution.py:361
  45.4 4.3 %flash.5 = (f32[256,640]{1,0:T(8,128)S(1)}, f32[256,640]{1,0:T(8,128)S(1)}) custom-call(s32[86]{0:T(128)S(1)} %compare_select_fusion.1.meta.table, bf16[512,256]{1,0:T(8,128)(2,1)S(1)} %get-tuple-element.73.refs_0_, bf16[512,256]{1,0:T(8,128)(2,1)S(1)} %collective-permute-done.1.refs_1_, bf16[768,512]{1,0:T(8,128)(2,1)S(1)} %bitcast.12, ...), custom_call_target="tpu_custom_call" | custom-call | flops 5000000000 | bytes 100000 | tf_op jit(solution)/shard_map/flash/pallas_call | solution.py:361
  53.6 6.8 %flash.6 = (f32[256,640]{1,0:T(8,128)S(1)}, f32[256,640]{1,0:T(8,128)}) custom-call(s32[86]{0:T(128)S(1)} %compare_select_fusion.1.meta.table, bf16[512,256]{1,0:T(8,128)(2,1)S(1)} %get-tuple-element.73.refs_0_, bf16[512,256]{1,0:T(8,128)(2,1)S(1)} %collective-permute-done.1.refs_1_, bf16[768,512]{1,0:T(8,128)(2,1)S(1)} %bitcast.9, ...), custom_call_target="tpu_custom_call" | custom-call | flops 5000000000 | bytes 100000 | tf_op jit(solution)/shard_map/flash/pallas_call | solution.py:361
  61.2 2.2 %weights.1 = (bf16[1,64,2176]{2,1,0:T(8,128)(2,1)}, bf16[1,64,2176]{2,1,0:T(8,128)(2,1)}) custom-call(s32[86]{0:T(128)} %copy-done, bf16[64,1408]{1,0:T(8,128)(2,1)} %gate.1, bf16[64,1408]{1,0:T(8,128)(2,1)} %up.1, bf16[64,1408]{1,0:T(8,128)(2,1)} %bitcast.24), custom_call_target="tpu_custom_call" | custom-call | flops 2000000000 | bytes 100000 | tf_op jit(solution)/shard_map/weights/pallas_call | solution.py:160
  65.5 3.2 %lines.1.refs_4_ = bf16[320,2048]{1,0:T(8,128)(2,1)} custom-call(s32[86]{0:T(128)} %copy-done, bf16[512,2048]{1,0:T(8,128)(2,1)} %refs_11_.1, bf16[64,2048]{1,0:T(8,128)(2,1)} %stream.1), custom_call_target="tpu_custom_call" | custom-call | flops 2000000000 | bytes 100000 | tf_op jit(solution)/shard_map/lines/pallas_call | solution.py:189
  70.3 2.7 %collective-permute-start.18 = (bf16[320,2048]{1,0:T(8,128)(2,1)}, bf16[320,2048]{1,0:T(8,128)(2,1)S(1)}, u32[]{:S(2)}, u32[]{:S(2)}) collective-permute-start(bf16[320,2048]{1,0:T(8,128)(2,1)} %lines.1.refs_4_), channel_id=1, source_target_pairs={{0,2},{1,3},{2,0},{3,1},{4,6},{5,7},{6,4},{7,5},{8,10},{9,11},{10,... | collective-permute-start | bytes 3932168 | tf_op jit(solution)/shard_map/ppermute | solution.py:49
  76.7 2.1 %collective-permute-start.27 = (bf16[2,64,2176]{2,1,0:T(8,128)(2,1)S(1)}, bf16[2,64,2176]{2,1,0:T(8,128)(2,1)S(1)}, u32[]{:S(2)}, u32[]{:S(2)}) collective-permute-start(bf16[2,64,2176]{2,1,0:T(8,128)(2,1)S(1)} %get-tuple-element.86.refs_0_), channel_id=1, source_target_pairs={{0,8},{4,28},{8,0},{12,20},{16,24},{20,12},{24,16},{28,4},{32,40},... | collective-permute-start | bytes 1671176 | tf_op jit(solution)/shard_map/ppermute | solution.py:41
  81.3 6.0 %flash.7 = (f32[256,640]{1,0:T(8,128)S(1)}, f32[256,640]{1,0:T(8,128)S(1)}) custom-call(s32[86]{0:T(128)S(1)} %copy-done.1, bf16[512,256]{1,0:T(8,128)(2,1)S(1)} %copy-done.10, bf16[512,256]{1,0:T(8,128)(2,1)S(1)} %copy-done.12, bf16[768,512]{1,0:T(8,128)(2,1)S(1)} %bitcast.10, bf16[640,512]{1,0:T(8,128)(2,1)S(1)} %bitcast.14, ...), custom_call_target="tpu_custom_call" | custom-call | flops 5000000000 | bytes 100000 | tf_op jit(solution)/shard_map/flash/pallas_call | solution.py:361
  89.4 5.3 %collective-permute-done.13.passed_ref = bf16[256,256]{1,0:T(8,128)(2,1)S(1)} collective-permute-done((bf16[256,256]{1,0:T(8,128)(2,1)S(1)}, bf16[256,256]{1,0:T(8,128)(2,1)S(1)}, u32[]{:S(2)}, u32[]{:S(2)}) %collective-permute-start.13) | collective-permute-done | bytes 131104 | tf_op jit(solution)/shard_map/ppermute | solution.py:36
  100.3 2.2 %collective-permute-start.20 = (bf16[320,2048]{1,0:T(8,128)(2,1)S(1)}, bf16[320,2048]{1,0:T(8,128)(2,1)S(1)}, u32[]{:S(2)}, u32[]{:S(2)}) collective-permute-start(bf16[320,2048]{1,0:T(8,128)(2,1)S(1)} %collective-permute-done.17.refs_5_), channel_id=1, source_target_pairs={{0,4},{4,0},{8,12},{12,8},{16,20},{20,16},{24,28},{28,24},{32,36},... | collective-permute-start | bytes 3932168 | tf_op jit(solution)/shard_map/ppermute | solution.py:36
  102.5 26.9 %collective-permute-done.18.refs_6_ = bf16[320,2048]{1,0:T(8,128)(2,1)S(1)} collective-permute-done((bf16[320,2048]{1,0:T(8,128)(2,1)}, bf16[320,2048]{1,0:T(8,128)(2,1)S(1)}, u32[]{:S(2)}, u32[]{:S(2)}) %collective-permute-start.18) | collective-permute-done | bytes 1310752 | tf_op jit(solution)/shard_map/ppermute | solution.py:49
  132.6 2.3 %collective-permute-start.15 = (bf16[256,512]{1,0:T(8,128)(2,1)S(1)}, bf16[256,512]{1,0:T(8,128)(2,1)S(1)}, u32[]{:S(2)}, u32[]{:S(2)}) collective-permute-start(bf16[256,512]{1,0:T(8,128)(2,1)S(1)} %merge_last.1.refs_0_), channel_id=1, source_target_pairs={{0,2},{1,3},{2,0},{3,1},{4,6},{5,7},{6,4},{7,5},{8,10},{9,11},{10,... | collective-permute-start | bytes 786440 | tf_op jit(solution)/shard_map/ppermute | solution.py:49
  135.0 5.7 %collective-permute-done.14.refs_1_ = bf16[256,512]{1,0:T(8,128)(2,1)S(1)} collective-permute-done((bf16[256,512]{1,0:T(8,128)(2,1)S(1)}, bf16[256,512]{1,0:T(8,128)(2,1)S(1)}, u32[]{:S(2)}, u32[]{:S(2)}) %collective-permute-start.14) | collective-permute-done | bytes 262176 | tf_op jit(solution)/shard_map/ppermute | solution.py:49
  142.7 4.5 %collective-permute-done.15.refs_2_ = bf16[256,512]{1,0:T(8,128)(2,1)S(1)} collective-permute-done((bf16[256,512]{1,0:T(8,128)(2,1)S(1)}, bf16[256,512]{1,0:T(8,128)(2,1)S(1)}, u32[]{:S(2)}, u32[]{:S(2)}) %collective-permute-start.15) | collective-permute-done | bytes 262176 | tf_op jit(solution)/shard_map/ppermute | solution.py:49
  147.2 2.5 %collective-permute-start.33 = (bf16[4,64,2176]{2,1,0:T(8,128)(2,1)S(1)}, bf16[4,64,2176]{2,1,0:T(8,128)(2,1)S(1)}, u32[]{:S(2)}, u32[]{:S(2)}) collective-permute-start(bf16[4,64,2176]{2,1,0:T(8,128)(2,1)S(1)} %get-tuple-element.91.refs_4_), channel_id=1, source_target_pairs={{0,96},{4,36},{8,104},{12,44},{16,112},{20,52},{24,120},{28,60},{3... | collective-permute-start | bytes 3342344 | tf_op jit(solution)/shard_map/ppermute | solution.py:41
  154.2 4.9 %middle.1 = (bf16[256,2048]{1,0:T(8,128)(2,1)S(1)}, f32[64,2048]{1,0:T(8,128)S(1)}) custom-call(s32[86]{0:T(128)S(1)} %copy-done.1, bf16[256,512]{1,0:T(8,128)(2,1)S(1)} %merge_last.1.refs_0_, bf16[256,512]{1,0:T(8,128)(2,1)S(1)} %collective-permute-done.14.refs_1_, bf16[256,512]{1,0:T(8,128)(2,1)S(1)} %collective-permute-done.15.refs_2_, ...), custom_call_target="tpu_custom_call" | custom-call | flops 4000000000 | bytes 100000 | tf_op jit(solution)/shard_map/middle/pallas_call | solution.py:469
  159.5 4.4 %collective-permute-done.33.refs_6_ = bf16[4,64,2176]{2,1,0:T(8,128)(2,1)S(1)} collective-permute-done((bf16[4,64,2176]{2,1,0:T(8,128)(2,1)S(1)}, bf16[4,64,2176]{2,1,0:T(8,128)(2,1)S(1)}, u32[]{:S(2)}, u32[]{:S(2)}) %collective-permute-start.33) | collective-permute-done | bytes 1114144 | tf_op jit(solution)/shard_map/ppermute | solution.py:41
  163.9 2.5 %collective-permute-done.30.refs_2_ = bf16[4,64,2176]{2,1,0:T(8,128)(2,1)S(1)} collective-permute-done((bf16[4,64,2176]{2,1,0:T(8,128)(2,1)S(1)}, bf16[4,64,2176]{2,1,0:T(8,128)(2,1)S(1)}, u32[]{:S(2)}, u32[]{:S(2)}) %collective-permute-start.30) | collective-permute-done | bytes 1114144 | tf_op jit(solution)/shard_map/ppermute | solution.py:41
  166.4 11.9 %collective-permute-done.31.refs_3_ = bf16[4,64,2176]{2,1,0:T(8,128)(2,1)S(1)} collective-permute-done((bf16[4,64,2176]{2,1,0:T(8,128)(2,1)S(1)}, bf16[4,64,2176]{2,1,0:T(8,128)(2,1)S(1)}, u32[]{:S(2)}, u32[]{:S(2)}) %collective-permute-start.31) | collective-permute-done | bytes 1114144 | tf_op jit(solution)/shard_map/ppermute | solution.py:41
  178.4 8.3 %ffn.1 = (bf16[256,2048]{1,0:T(8,128)(2,1)S(1)}, bf16[512,768]{1,0:T(8,128)(2,1)S(1)}, bf16[2048,768]{1,0:T(8,128)(2,1)S(1)}) custom-call(s32[86]{0:T(128)S(1)} %copy-done.1, bf16[256,2048]{1,0:T(8,128)(2,1)S(1)} %get-tuple-element.79.mine_ref, bf16[256,2048]{1,0:T(8,128)(2,1)S(1)} %collective-permute-done.23.other_ref, ...), custom_call_target="tpu_custom_call" | custom-call | flops 8999999488 | bytes 100000 | tf_op jit(solution)/shard_map/ffn/pallas_call | solution.py:547
  192.4 6.4 %collective-permute-done.38 = bf16[64,2048]{1,0:T(8,128)(2,1)S(1)} collective-permute-done((bf16[64,2048]{1,0:T(8,128)(2,1)S(1)}, bf16[64,2048]{1,0:T(8,128)(2,1)S(1)}, u32[]{:S(2)}, u32[]{:S(2)}) %collective-permute-start.38) | collective-permute-done | bytes 262176 | tf_op jit(solution)/shard_map/ppermute | solution.py:49
  198.8 2.9 %collective-permute-done.37 = bf16[64,2048]{1,0:T(8,128)(2,1)S(1)} collective-permute-done((bf16[64,2048]{1,0:T(8,128)(2,1)S(1)}, bf16[64,2048]{1,0:T(8,128)(2,1)S(1)}, u32[]{:S(2)}, u32[]{:S(2)}) %collective-permute-start.37) | collective-permute-done | bytes 262176 | tf_op jit(solution)/shard_map/ppermute | solution.py:49
  201.7 4.3 %collective-permute-done.36 = bf16[64,2048]{1,0:T(8,128)(2,1)S(1)} collective-permute-done((bf16[64,2048]{1,0:T(8,128)(2,1)S(1)}, bf16[64,2048]{1,0:T(8,128)(2,1)S(1)}, u32[]{:S(2)}, u32[]{:S(2)}) %collective-permute-start.36) | collective-permute-done | bytes 262176 | tf_op jit(solution)/shard_map/ppermute | solution.py:49
  (122 shorter events, 47.7 us)
Async XLA Ops:
  2.1 11.1 %collective-permute-start = (bf16[256,768]{1,0:T(8,128)(2,1)}, bf16[256,768]{1,0:T(8,128)(2,1)S(1)}, u32[]{:S(2)}, u32[]{:S(2)}) collective-permute-start(bf16[256,768]{1,0:T(8,128)(2,1)} %get-tuple-element.54), channel_id=1, source_target_pairs={{0,8},{4,12},{8,0},{12,4},{16,24},{20,28},{24,16},{28,20},{32,40},... | collective-permute-start | bytes 1179656 | tf_op jit(solution)/shard_map/ppermute | solution.py:36
  14.3 11.3 %collective-permute-start.2 = (bf16[1,192,512]{2,1,0:T(8,128)(2,1)S(1)}, bf16[1,192,512]{2,1,0:T(8,128)(2,1)S(1)}, u32[]{:S(2)}, u32[]{:S(2)}) collective-permute-start(bf16[1,192,512]{2,1,0:T(8,128)(2,1)S(1)} %get-tuple-element.56.refs_0_), channel_id=1, source_target_pairs={{0,32},{4,36},{8,40},{12,44},{16,48},{20,52},{24,56},{28,60},{32,0... | collective-permute-start | bytes 589832 | tf_op jit(solution)/shard_map/ppermute | solution.py:36
  25.7 10.9 %collective-permute-start.5 = (bf16[2,192,512]{2,1,0:T(8,128)(2,1)S(1)}, bf16[2,192,512]{2,1,0:T(8,128)(2,1)S(1)}, u32[]{:S(2)}, u32[]{:S(2)}) collective-permute-start(bf16[2,192,512]{2,1,0:T(8,128)(2,1)S(1)} %get-tuple-element.59.refs_0_), channel_id=1, source_target_pairs={{0,96},{4,100},{8,104},{12,108},{16,112},{20,116},{24,120},{28,124... | collective-permute-start | bytes 1179656 | tf_op jit(solution)/shard_map/ppermute | solution.py:36
  29.9 11.2 %collective-permute-start.1 = (bf16[512,256]{1,0:T(8,128)(2,1)S(1)}, bf16[512,256]{1,0:T(8,128)(2,1)S(1)}, u32[]{:S(2)}, u32[]{:S(2)}) collective-permute-start(bf16[512,256]{1,0:T(8,128)(2,1)S(1)} %get-tuple-element.73.refs_0_), channel_id=1, source_target_pairs={{0,4},{4,0},{8,12},{12,8},{16,20},{20,16},{24,28},{28,24},{32,36},... | collective-permute-start | bytes 786440 | tf_op jit(solution)/shard_map/ppermute | solution.py:36
  36.7 16.9 %collective-permute-start.8 = (bf16[4,192,512]{2,1,0:T(8,128)(2,1)S(1)}, bf16[4,192,512]{2,1,0:T(8,128)(2,1)S(1)}, u32[]{:S(2)}, u32[]{:S(2)}) collective-permute-start(bf16[4,192,512]{2,1,0:T(8,128)(2,1)S(1)} %get-tuple-element.62), channel_id=1, source_target_pairs={{0,24},{4,28},{8,16},{12,20},{16,8},{20,12},{24,0},{28,4},{32,56},... | collective-permute-start | bytes 2359304 | tf_op jit(solution)/shard_map/ppermute | solution.py:36
  38.7 13.0 %collective-permute-start.9 = (bf16[4,160,512]{2,1,0:T(8,128)(2,1)S(1)}, bf16[4,160,512]{2,1,0:T(8,128)(2,1)S(1)}, u32[]{:S(2)}, u32[]{:S(2)}) collective-permute-start(bf16[4,160,512]{2,1,0:T(8,128)(2,1)S(1)} %get-tuple-element.63), channel_id=1, source_target_pairs={{0,32},{4,36},{8,40},{12,44},{16,48},{20,52},{24,56},{28,60},{32,0... | collective-permute-start | bytes 1966088 | tf_op jit(solution)/shard_map/ppermute | solution.py:36
  38.7 14.2 %collective-permute-start.10 = (bf16[4,160,512]{2,1,0:T(8,128)(2,1)S(1)}, bf16[4,160,512]{2,1,0:T(8,128)(2,1)S(1)}, u32[]{:S(2)}, u32[]{:S(2)}) collective-permute-start(bf16[4,160,512]{2,1,0:T(8,128)(2,1)S(1)} %get-tuple-element.64), channel_id=1, source_target_pairs={{0,96},{4,100},{8,104},{12,108},{16,112},{20,116},{24,120},{28,124... | collective-permute-start | bytes 1966088 | tf_op jit(solution)/shard_map/ppermute | solution.py:36
  61.2 17.5 %collective-permute-start.11 = (f32[256,640]{1,0:T(8,128)}, f32[256,640]{1,0:T(8,128)}, u32[]{:S(2)}, u32[]{:S(2)}) collective-permute-start(f32[256,640]{1,0:T(8,128)} %get-tuple-element.72), channel_id=1, source_target_pairs={{0,4},{4,0},{8,12},{12,8},{16,20},{20,16},{24,28},{28,24},{32,36},... | collective-permute-start | bytes 1966088 | tf_op jit(solution)/shard_map/ppermute | solution.py:36
  64.0 9.0 %collective-permute-start.25 = (bf16[1,64,2176]{2,1,0:T(8,128)(2,1)}, bf16[1,64,2176]{2,1,0:T(8,128)(2,1)}, u32[]{:S(2)}, u32[]{:S(2)}) collective-permute-start(bf16[1,64,2176]{2,1,0:T(8,128)(2,1)} %get-tuple-element.80.refs_0_), channel_id=1, source_target_pairs={{0,32},{4,100},{8,40},{12,108},{16,48},{20,116},{24,56},{28,124},{... | collective-permute-start | bytes 835592 | tf_op jit(solution)/shard_map/ppermute | solution.py:41
  65.5 9.0 %collective-permute-start.26 = (bf16[1,64,2176]{2,1,0:T(8,128)(2,1)}, bf16[1,64,2176]{2,1,0:T(8,128)(2,1)}, u32[]{:S(2)}, u32[]{:S(2)}) collective-permute-start(bf16[1,64,2176]{2,1,0:T(8,128)(2,1)} %collective-permute-done.24.refs_1_), channel_id=1, source_target_pairs={{0,8},{4,28},{8,0},{12,20},{16,24},{20,12},{24,16},{28,4},{32,40},... | collective-permute-start | bytes 835592 | tf_op jit(solution)/shard_map/ppermute | solution.py:41
  68.7 31.6 %collective-permute-start.17 = (bf16[320,2048]{1,0:T(8,128)(2,1)}, bf16[320,2048]{1,0:T(8,128)(2,1)S(1)}, u32[]{:S(2)}, u32[]{:S(2)}) collective-permute-start(bf16[320,2048]{1,0:T(8,128)(2,1)} %lines.1.refs_4_), channel_id=1, source_target_pairs={{0,1},{1,2},{2,3},{3,0},{4,5},{5,6},{6,7},{7,4},{8,9},{9,10},{10,1... | collective-permute-start | bytes 3932168 | tf_op jit(solution)/shard_map/ppermute | solution.py:49
  70.3 59.1 %collective-permute-start.18 = (bf16[320,2048]{1,0:T(8,128)(2,1)}, bf16[320,2048]{1,0:T(8,128)(2,1)S(1)}, u32[]{:S(2)}, u32[]{:S(2)}) collective-permute-start(bf16[320,2048]{1,0:T(8,128)(2,1)} %lines.1.refs_4_), channel_id=1, source_target_pairs={{0,2},{1,3},{2,0},{3,1},{4,6},{5,7},{6,4},{7,5},{8,10},{9,11},{10,... | collective-permute-start | bytes 3932168 | tf_op jit(solution)/shard_map/ppermute | solution.py:49
  73.0 57.7 %collective-permute-start.19 = (bf16[320,2048]{1,0:T(8,128)(2,1)}, bf16[320,2048]{1,0:T(8,128)(2,1)S(1)}, u32[]{:S(2)}, u32[]{:S(2)}) collective-permute-start(bf16[320,2048]{1,0:T(8,128)(2,1)} %lines.1.refs_4_), channel_id=1, source_target_pairs={{0,3},{1,0},{2,1},{3,2},{4,7},{5,4},{6,5},{7,6},{8,11},{9,8},{10,9... | collective-permute-start | bytes 3932168 | tf_op jit(solution)/shard_map/ppermute | solution.py:49
  76.7 10.6 %collective-permute-start.27 = (bf16[2,64,2176]{2,1,0:T(8,128)(2,1)S(1)}, bf16[2,64,2176]{2,1,0:T(8,128)(2,1)S(1)}, u32[]{:S(2)}, u32[]{:S(2)}) collective-permute-start(bf16[2,64,2176]{2,1,0:T(8,128)(2,1)S(1)} %get-tuple-element.86.refs_0_), channel_id=1, source_target_pairs={{0,8},{4,28},{8,0},{12,20},{16,24},{20,12},{24,16},{28,4},{32,40},... | collective-permute-start | bytes 1671176 | tf_op jit(solution)/shard_map/ppermute | solution.py:41
  78.8 10.5 %collective-permute-start.28 = (bf16[2,64,2176]{2,1,0:T(8,128)(2,1)S(1)}, bf16[2,64,2176]{2,1,0:T(8,128)(2,1)S(1)}, u32[]{:S(2)}, u32[]{:S(2)}) collective-permute-start(bf16[2,64,2176]{2,1,0:T(8,128)(2,1)S(1)} %get-tuple-element.87.refs_1_), channel_id=1, source_target_pairs={{0,32},{4,100},{8,40},{12,108},{16,48},{20,116},{24,56},{28,124},{... | collective-permute-start | bytes 1671176 | tf_op jit(solution)/shard_map/ppermute | solution.py:41
  87.3 9.4 %collective-permute-start.12 = (f32[256,640]{1,0:T(8,128)S(1)}, f32[256,640]{1,0:T(8,128)S(1)}, u32[]{:S(2)}, u32[]{:S(2)}) collective-permute-start(f32[256,640]{1,0:T(8,128)S(1)} %get-tuple-element.75), channel_id=1, source_target_pairs={{0,4},{4,0},{8,12},{12,8},{16,20},{20,16},{24,28},{28,24},{32,36},... | collective-permute-start | bytes 1966088 | tf_op jit(solution)/shard_map/ppermute | solution.py:36
  94.7 36.0 %collective-permute-start.29 = (bf16[4,64,2176]{2,1,0:T(8,128)(2,1)S(1)}, bf16[4,64,2176]{2,1,0:T(8,128)(2,1)S(1)}, u32[]{:S(2)}, u32[]{:S(2)}) collective-permute-start(bf16[4,64,2176]{2,1,0:T(8,128)(2,1)S(1)} %get-tuple-element.89.refs_0_), channel_id=1, source_target_pairs={{0,96},{4,36},{8,104},{12,44},{16,112},{20,52},{24,120},{28,60},{3... | collective-permute-start | bytes 3342344 | tf_op jit(solution)/shard_map/ppermute | solution.py:41
  96.7 36.0 %collective-permute-start.32 = (bf16[4,64,2176]{2,1,0:T(8,128)(2,1)S(1)}, bf16[4,64,2176]{2,1,0:T(8,128)(2,1)S(1)}, u32[]{:S(2)}, u32[]{:S(2)}) collective-permute-start(bf16[4,64,2176]{2,1,0:T(8,128)(2,1)S(1)} %get-tuple-element.91.refs_4_), channel_id=1, source_target_pairs={{0,24},{4,12},{8,16},{12,4},{16,8},{20,28},{24,0},{28,20},{32,56},... | collective-permute-start | bytes 3342344 | tf_op jit(solution)/shard_map/ppermute | solution.py:41
  100.3 50.9 %collective-permute-start.20 = (bf16[320,2048]{1,0:T(8,128)(2,1)S(1)}, bf16[320,2048]{1,0:T(8,128)(2,1)S(1)}, u32[]{:S(2)}, u32[]{:S(2)}) collective-permute-start(bf16[320,2048]{1,0:T(8,128)(2,1)S(1)} %collective-permute-done.17.refs_5_), channel_id=1, source_target_pairs={{0,4},{4,0},{8,12},{12,8},{16,20},{20,16},{24,28},{28,24},{32,36},... | collective-permute-start | bytes 3932168 | tf_op jit(solution)/shard_map/ppermute | solution.py:36
  129.4 23.6 %collective-permute-start.21 = (bf16[320,2048]{1,0:T(8,128)(2,1)S(1)}, bf16[320,2048]{1,0:T(8,128)(2,1)S(1)}, u32[]{:S(2)}, u32[]{:S(2)}) collective-permute-start(bf16[320,2048]{1,0:T(8,128)(2,1)S(1)} %collective-permute-done.18.refs_6_), channel_id=1, source_target_pairs={{0,4},{4,0},{8,12},{12,8},{16,20},{20,16},{24,28},{28,24},{32,36},... | collective-permute-start | bytes 3932168 | tf_op jit(solution)/shard_map/ppermute | solution.py:36
  130.7 23.4 %collective-permute-start.22 = (bf16[320,2048]{1,0:T(8,128)(2,1)S(1)}, bf16[320,2048]{1,0:T(8,128)(2,1)S(1)}, u32[]{:S(2)}, u32[]{:S(2)}) collective-permute-start(bf16[320,2048]{1,0:T(8,128)(2,1)S(1)} %collective-permute-done.19.refs_7_), channel_id=1, source_target_pairs={{0,4},{4,0},{8,12},{12,8},{16,20},{20,16},{24,28},{28,24},{32,36},... | collective-permute-start | bytes 3932168 | tf_op jit(solution)/shard_map/ppermute | solution.py:36
  130.8 9.9 %collective-permute-start.14 = (bf16[256,512]{1,0:T(8,128)(2,1)S(1)}, bf16[256,512]{1,0:T(8,128)(2,1)S(1)}, u32[]{:S(2)}, u32[]{:S(2)}) collective-permute-start(bf16[256,512]{1,0:T(8,128)(2,1)S(1)} %merge_last.1.refs_0_), channel_id=1, source_target_pairs={{0,1},{1,2},{2,3},{3,0},{4,5},{5,6},{6,7},{7,4},{8,9},{9,10},{10,1... | collective-permute-start | bytes 786440 | tf_op jit(solution)/shard_map/ppermute | solution.py:49
  132.6 14.5 %collective-permute-start.15 = (bf16[256,512]{1,0:T(8,128)(2,1)S(1)}, bf16[256,512]{1,0:T(8,128)(2,1)S(1)}, u32[]{:S(2)}, u32[]{:S(2)}) collective-permute-start(bf16[256,512]{1,0:T(8,128)(2,1)S(1)} %merge_last.1.refs_0_), channel_id=1, source_target_pairs={{0,2},{1,3},{2,0},{3,1},{4,6},{5,7},{6,4},{7,5},{8,10},{9,11},{10,... | collective-permute-start | bytes 786440 | tf_op jit(solution)/shard_map/ppermute | solution.py:49
  140.7 9.0 %collective-permute-start.16 = (bf16[256,512]{1,0:T(8,128)(2,1)S(1)}, bf16[256,512]{1,0:T(8,128)(2,1)S(1)}, u32[]{:S(2)}, u32[]{:S(2)}) collective-permute-start(bf16[256,512]{1,0:T(8,128)(2,1)S(1)} %merge_last.1.refs_0_), channel_id=1, source_target_pairs={{0,3},{1,0},{2,1},{3,2},{4,7},{5,4},{6,5},{7,6},{8,11},{9,8},{10,9... | collective-permute-start | bytes 786440 | tf_op jit(solution)/shard_map/ppermute | solution.py:49
  147.2 16.7 %collective-permute-start.33 = (bf16[4,64,2176]{2,1,0:T(8,128)(2,1)S(1)}, bf16[4,64,2176]{2,1,0:T(8,128)(2,1)S(1)}, u32[]{:S(2)}, u32[]{:S(2)}) collective-permute-start(bf16[4,64,2176]{2,1,0:T(8,128)(2,1)S(1)} %get-tuple-element.91.refs_4_), channel_id=1, source_target_pairs={{0,96},{4,36},{8,104},{12,44},{16,112},{20,52},{24,120},{28,60},{3... | collective-permute-start | bytes 3342344 | tf_op jit(solution)/shard_map/ppermute | solution.py:41
  149.7 16.7 %collective-permute-start.30 = (bf16[4,64,2176]{2,1,0:T(8,128)(2,1)S(1)}, bf16[4,64,2176]{2,1,0:T(8,128)(2,1)S(1)}, u32[]{:S(2)}, u32[]{:S(2)}) collective-permute-start(bf16[4,64,2176]{2,1,0:T(8,128)(2,1)S(1)} %get-tuple-element.89.refs_0_), channel_id=1, source_target_pairs={{0,24},{4,12},{8,16},{12,4},{16,8},{20,28},{24,0},{28,20},{32,56},... | collective-permute-start | bytes 3342344 | tf_op jit(solution)/shard_map/ppermute | solution.py:41
  151.2 27.2 %collective-permute-start.31 = (bf16[4,64,2176]{2,1,0:T(8,128)(2,1)S(1)}, bf16[4,64,2176]{2,1,0:T(8,128)(2,1)S(1)}, u32[]{:S(2)}, u32[]{:S(2)}) collective-permute-start(bf16[4,64,2176]{2,1,0:T(8,128)(2,1)S(1)} %collective-permute-done.29.refs_1_), channel_id=1, source_target_pairs={{0,24},{4,12},{8,16},{12,4},{16,8},{20,28},{24,0},{28,20},{32,56},... | collective-permute-start | bytes 3342344 | tf_op jit(solution)/shard_map/ppermute | solution.py:41
  152.9 25.4 %collective-permute-start.34 = (bf16[4,64,2176]{2,1,0:T(8,128)(2,1)S(1)}, bf16[4,64,2176]{2,1,0:T(8,128)(2,1)S(1)}, u32[]{:S(2)}, u32[]{:S(2)}) collective-permute-start(bf16[4,64,2176]{2,1,0:T(8,128)(2,1)S(1)} %collective-permute-done.32.refs_5_), channel_id=1, source_target_pairs={{0,96},{4,36},{8,104},{12,44},{16,112},{20,52},{24,120},{28,60},{3... | collective-permute-start | bytes 3342344 | tf_op jit(solution)/shard_map/ppermute | solution.py:41
  159.1 19.2 %collective-permute-start.23 = (bf16[256,2048]{1,0:T(8,128)(2,1)S(1)}, bf16[256,2048]{1,0:T(8,128)(2,1)S(1)}, u32[]{:S(2)}, u32[]{:S(2)}) collective-permute-start(bf16[256,2048]{1,0:T(8,128)(2,1)S(1)} %get-tuple-element.79.mine_ref), channel_id=1, source_target_pairs={{0,4},{4,0},{8,12},{12,8},{16,20},{20,16},{24,28},{28,24},{32,36},... | collective-permute-start | bytes 3145736 | tf_op jit(solution)/shard_map/ppermute | solution.py:36
  189.6 9.2 %collective-permute-start.38 = (bf16[64,2048]{1,0:T(8,128)(2,1)S(1)}, bf16[64,2048]{1,0:T(8,128)(2,1)S(1)}, u32[]{:S(2)}, u32[]{:S(2)}) collective-permute-start(bf16[64,2048]{1,0:T(8,128)(2,1)S(1)} %get-tuple-element.100), channel_id=1, source_target_pairs={{0,3},{1,0},{2,1},{3,2},{4,7},{5,4},{6,5},{7,6},{8,11},{9,8},{10,9... | collective-permute-start | bytes 786440 | tf_op jit(solution)/shard_map/ppermute | solution.py:49
  191.0 10.7 %collective-permute-start.37 = (bf16[64,2048]{1,0:T(8,128)(2,1)S(1)}, bf16[64,2048]{1,0:T(8,128)(2,1)S(1)}, u32[]{:S(2)}, u32[]{:S(2)}) collective-permute-start(bf16[64,2048]{1,0:T(8,128)(2,1)S(1)} %get-tuple-element.99), channel_id=1, source_target_pairs={{0,2},{1,3},{2,0},{3,1},{4,6},{5,7},{6,4},{7,5},{8,10},{9,11},{10,... | collective-permute-start | bytes 786440 | tf_op jit(solution)/shard_map/ppermute | solution.py:49
  191.1 14.9 %collective-permute-start.36 = (bf16[64,2048]{1,0:T(8,128)(2,1)S(1)}, bf16[64,2048]{1,0:T(8,128)(2,1)S(1)}, u32[]{:S(2)}, u32[]{:S(2)}) collective-permute-start(bf16[64,2048]{1,0:T(8,128)(2,1)S(1)} %get-tuple-element.98), channel_id=1, source_target_pairs={{0,1},{1,2},{2,3},{3,0},{4,5},{5,6},{6,7},{7,4},{8,9},{9,10},{10,1... | collective-permute-start | bytes 786440 | tf_op jit(solution)/shard_map/ppermute | solution.py:49
  (35 other events, 419.5 us)
